TPU v7x, 256 devices: a 4x2x16 block of a 4x16x16 slice. The times are simulated.
256 devices in a mesh: grp: 2 (over y), st: 32 (over z, core), tp: 4 (over x).
Axes of the slice: x: 4, y: 2, z: 16, core: 2. Of those that a mesh axis runs over, the one named last changes fastest.
The devices are a block of a 4x16x16 slice.
Arguments:
- tokens: bfloat16 [65536, 2048], P(('grp', 'st'), 'tp'), parts along dimension 0, may hold values from -6 to 6
- norm_gain: float32 [2048], replicated, may hold values from 0.1 to 1.9
- pool_weight: bfloat16 [4, 512, 512], P('tp'), may hold values from -0.25 to 0.25
- pool_scale: float32 [2048], P('tp'), may hold values from 0.1 to 1.9
- query_weight: bfloat16 [2048, 1024], P(None, 'tp'), may hold values from -3 to 3
- gate_weight: bfloat16 [2048, 8], replicated, may hold values from -0.125 to 0.125
- key_weight: bfloat16 [2048, 1024], P(None, 'tp'), may hold values from -0.125 to 0.125
- value_weight: bfloat16 [2048, 1024], P(None, 'tp'), may hold values from -0.125 to 0.125
- out_weight: bfloat16 [1024, 2048], P(None, 'tp'), may hold values from -0.1875 to 0.1875
- passage_gain: float32 [2048], replicated, may hold values from 0.1 to 1.9
- passage_store: bfloat16 [1536, 64, 2048], P(('grp', 'st')), parts along dimension 0, may hold values from -6 to 6
- passage_ids: int32 [512, 4], P(('grp', 'st')), parts along dimension 0, may hold values from 0 to 767, as said below
Outputs:
- mixed: bfloat16 [65536, 2048], P(('grp', 'st'), 'tp'), parts along dimension 0
There are 2 independent parts, one for each index of `grp`. A program takes and returns all parts, laid end to end along the dimension named above; an argument that names none is the same for every part. Nothing has to cross between parts.
Inputs may be any that keep to these rules, and one draw needn't show every extreme that they name: `passage_ids`: the ids of the blocks of one index of st name at most 2 passages held by any one index of st, and exactly 2 held by some index.
All inputs are finite; a program needn't handle non-finite values.
Results may differ from a plain program's by a relative error of at most 0.009.
Values may be sent and summed in bfloat16 or wider, within the bound.
No kernel may reach another device: no remote copies, remote signals or barrier semaphores. Data moves between devices by JAX's collectives and lax.ppermute only.
A program may use at most 128 MiB of HBM per device.

v0:
```python
import jax
import jax.numpy as jnp
from jax import lax
from jax.sharding import PartitionSpec as P

HD = 128
GROUPS = 4
SEQ_LEN = 256
BLK = 128
NPB = 4
PLEN = 64
P_DEV = 24


epsilon = 1e-06


def in_order(pieces, dim):
    lengths = list(pieces.shape[1:])
    lengths[dim] *= pieces.shape[0]
    return jnp.moveaxis(pieces, 0, dim).reshape(lengths)


def copy_for_each(value, axis):
    copies = jnp.broadcast_to(value, (lax.axis_size(axis), *value.shape))
    return lax.all_to_all(copies, axis, split_axis=0, concat_axis=0, tiled=True)


def gather_directly(value, axis, dim):
    return in_order(copy_for_each(value, axis), dim)


def normalize_rows(fetched, passage_gain):
    wide_rows = fetched.astype(jnp.float32)
    inverse = lax.rsqrt(jnp.mean(wide_rows * wide_rows, axis=-1, keepdims=True) + epsilon)
    return (wide_rows * inverse * passage_gain).astype(jnp.bfloat16)


def project_rows(fetched, passage_gain, both_weights):
    count_rows = fetched.shape[0]
    flat_rows = normalize_rows(fetched.reshape(count_rows * PLEN, fetched.shape[2]), passage_gain)
    projected = jnp.dot(flat_rows, both_weights, preferred_element_type=jnp.float32).astype(
        jnp.bfloat16
    )
    return projected.reshape(count_rows, PLEN, both_weights.shape[1])


def per_device(
    tokens,
    norm_gain,
    pool_weight,
    pool_scale,
    query_weight,
    gate_weight,
    key_weight,
    value_weight,
    out_weight,
    passage_gain,
    passage_store,
    passage_ids,
):
    head_index = lax.axis_index("tp")
    tok_rows, width_local = tokens.shape
    full_width = width_local * lax.axis_size("tp")
    local_heads = query_weight.shape[1] // HD
    head_width = local_heads * HD
    wide_tokens = tokens.astype(jnp.float32)
    square_sums = lax.psum(jnp.sum(wide_tokens * wide_tokens, axis=1), "tp")
    inverse = lax.rsqrt(square_sums / full_width + epsilon)
    gain_local = lax.dynamic_slice_in_dim(norm_gain, head_index * width_local, width_local)
    normed = (wide_tokens * inverse[:, None] * gain_local[None, :]).astype(jnp.bfloat16)
    sequences = tok_rows // SEQ_LEN
    widest = 2**GROUPS
    window = jnp.left_shift(jnp.int32(2), head_index)
    grouped = normed.astype(jnp.float32).reshape(sequences, SEQ_LEN, width_local)
    running = jnp.cumsum(grouped, axis=1)
    padded = jnp.concatenate(
        [jnp.zeros((sequences, widest, width_local), jnp.float32), running], axis=1
    )
    lagged = lax.dynamic_slice_in_dim(padded, widest - window, SEQ_LEN, axis=1)
    position = jnp.arange(SEQ_LEN, dtype=jnp.int32)
    divisor = jnp.minimum(position + 1, window).astype(jnp.float32)
    pooled = (
        ((running - lagged) / divisor[None, :, None] - grouped)
        .astype(jnp.bfloat16)
        .reshape(tok_rows, width_local)
    )
    mixing = (
        jnp.dot(pooled, pool_weight[0], preferred_element_type=jnp.float32) * pool_scale[None, :]
    )
    gate_columns = lax.dynamic_slice_in_dim(
        gate_weight, head_index * local_heads, local_heads, axis=1
    )
    columns = lax.all_gather(normed, "tp", axis=1, tiled=True)
    query_sum = jnp.dot(columns, query_weight, preferred_element_type=jnp.float32)
    gate_sum = jnp.dot(columns, gate_columns, preferred_element_type=jnp.float32)
    queries = query_sum.astype(jnp.bfloat16)
    gating = jax.nn.sigmoid(gate_sum)
    flat_ids = passage_ids.reshape(-1)
    asked_count = flat_ids.shape[0]
    st_count = lax.axis_size("st")
    capacity = max(2, (asked_count + st_count - 1) // st_count)
    owners = flat_ids // P_DEV
    local_index = flat_ids % P_DEV
    order_index = jnp.arange(asked_count, dtype=jnp.int32)
    earlier = (owners[None, :] == owners[:, None]) & (order_index[None, :] < order_index[:, None])
    slot_index = jnp.sum(earlier.astype(jnp.int32), axis=1)
    position_flat = owners * capacity + slot_index
    slot_range = jnp.arange(st_count * capacity, dtype=jnp.int32)
    request_table = jnp.sum(
        jnp.where(position_flat[None, :] == slot_range[:, None], local_index[None, :], 0), axis=1
    )
    request_table = request_table.reshape(st_count, capacity)
    asked = lax.all_to_all(request_table, "st", split_axis=0, concat_axis=0, tiled=True)
    both_weights = jnp.concatenate([key_weight, value_weight], axis=1)
    projected_store = project_rows(passage_store, passage_gain, both_weights)
    projected = jnp.take(projected_store, asked.reshape(-1), axis=0)
    returned = lax.all_to_all(
        projected.reshape(st_count, capacity * PLEN, 2 * head_width),
        "st",
        split_axis=0,
        concat_axis=0,
        tiled=True,
    )
    key_values = jnp.take(
        returned.reshape(st_count * capacity, PLEN, 2 * head_width), position_flat, axis=0
    )
    block_count = tok_rows // BLK
    key_values = key_values.reshape(block_count, NPB * PLEN, 2 * head_width)
    key_rows = key_values[:, :, :head_width].reshape(block_count, NPB * PLEN, local_heads, HD)
    values = key_values[:, :, head_width:].reshape(block_count, NPB * PLEN, local_heads, HD)
    query_blocks = queries.reshape(block_count, BLK, local_heads, HD)
    scores = jnp.einsum(
        "bqhd,bkhd->bhqk", query_blocks, key_rows, preferred_element_type=jnp.float32
    ) * HD ** (-0.5)
    row_max = jnp.max(scores, axis=-1, keepdims=True)
    weights = jnp.exp(scores - row_max)
    probabilities = (weights / jnp.sum(weights, axis=-1, keepdims=True)).astype(jnp.bfloat16)
    attended = jnp.einsum(
        "bhqk,bkhd->bqhd", probabilities, values, preferred_element_type=jnp.float32
    ).reshape(tok_rows, local_heads, HD)
    head_out = (attended * gating[:, :, None]).astype(jnp.bfloat16).reshape(tok_rows, head_width)
    crossed = jnp.dot(
        gather_directly(head_out, "tp", 1), out_weight, preferred_element_type=jnp.float32
    )
    return (mixing + crossed).astype(jnp.bfloat16)


def solution(mesh):
    in_specs = (
        P(("grp", "st"), "tp"),
        P(),
        P("tp", None, None),
        P("tp"),
        P(None, "tp"),
        P(),
        P(None, "tp"),
        P(None, "tp"),
        P(None, "tp"),
        P(),
        P(("grp", "st"), None, None),
        P(("grp", "st"), None),
    )
    out_specs = P(("grp", "st"), "tp")
    return jax.shard_map(
        per_device, mesh=mesh, in_specs=in_specs, out_specs=out_specs, check_vma=False
    )
```

profile of v0, /device:TPU:160, one launch (start us, length us, event | category | flops | bytes accessed | tf_op | source)
XLA Modules:
  0.0 315.7 jit_solution(15482940754100980256)
XLA Ops:
  6.6 0.8 copy.47
  8.7 23.3 %all-to-all-start = ((s32[32,1,2]{2,1,0:T(1,128)}), s32[32,1,2]{2,1,0:T(1,128)S(1)}, u32[]{:S(2)}, u32[]{:S(2)}) async-start(s32[32,1,2]{2,1,0:T(1,128)} %bitcast.9), calls=%async_computation | async-start | bytes 32768 | tf_op jit(solution)/shard_map/all_to_all | solution.py:114
  32.0 4.1 %multiply_reduce_fusion = f32[24,64]{1,0:T(8,128)S(1)} fusion(bf16[24,64,2048]{2,1,0:T(8,128)(2,1)} %param.22), kind=kLoop, calls=%fused_computation.6 | loop fusion | flops 9435648 | bytes 6297600 | tf_op jit(solution)/shard_map/reduce_sum | solution.py:35
  36.2 4.4 %fusion.2 = bf16[1536,2048]{1,0:T(8,128)(2,1)S(1)} fusion(f32[2048]{0:T(1024)S(1)} %copy-done.5, f32[1536]{0:T(1024)S(1)} %rsqrt.16, bf16[24,64,2048]{2,1,0:T(8,128)(2,1)} %param.22), kind=kLoop, calls=%fused_computation.5 | loop fusion | flops 12582912 | bytes 12597248 | tf_op jit(solution)/shard_map/convert_element_type | solution.py:36
  40.6 3.5 %convolution_convert_fusion = bf16[1536,512]{1,0:T(8,128)(2,1)S(1)} fusion(bf16[1536,2048]{1,0:T(8,128)(2,1)S(1)} %fusion.2, bf16[2048,256]{1,0:T(8,128)(2,1)S(1)} %copy-done.7, bf16[2048,256]{1,0:T(8,128)(2,1)S(1)} %copy-done.8), kind=kOutput, calls=%fused_computation.8 | convolution fusion | flops 3226206208 | bytes 9961472 | tf_op jit(solution)/shard_map/dot_general | solution.py:42
  45.9 2.8 gather_fusion
  48.7 3.9 %bitcast_select_fusion = bf16[32,128,512]{2,1,0:T(8,128)(2,1)} fusion(pred[32,128]{1,0:T(8,128)(4,1)S(1)} %broadcast_in_dim.66, bf16[32,128,512]{2,1,0:T(8,128)(2,1)} %bitcast.68), kind=kLoop, calls=%fused_computation.7 | loop fusion | flops 2097152 | bytes 8392704 | tf_op jit(solution)/shard_map/jit(_take)/select_n | solution.py:117
  52.6 12.6 %all-to-all-start.1 = ((bf16[32,128,512]{2,1,0:T(8,128)(2,1)}), bf16[32,128,512]{2,1,0:T(8,128)(2,1)}, u32[]{:S(2)}, u32[]{:S(2)}) async-start(bf16[32,128,512]{2,1,0:T(8,128)(2,1)} %bitcast_select_fusion), calls=%async_computation.1 | async-start | bytes 8388608 | tf_op jit(solution)/shard_map/all_to_all | solution.py:118
  65.2 0.8 dynamic_slice.9
  66.3 10.9 %psum.7 = f32[1024]{0:T(1024)S(1)} all-reduce(f32[1024]{0:T(1024)S(1)} %fusion.6), channel_id=1, replica_groups=mesh['grp'=2,'st'=32,'tp'=4] {'tp'}, use_global_device_ids=true, to_apply=%region_1.0 | all-reduce | flops 1024 | bytes 8192 | tf_op jit(solution)/shard_map/psum | solution.py:68
  77.2 1.4 fusion.8
  79.1 53.2 %all-gather.2.cloned.1.call-done = bf16[1024,2048]{1,0:T(8,128)(2,1)} async-done(((bf16[1024,512]{1,0:T(8,128)(2,1)}), bf16[1024,2048]{1,0:T(8,128)(2,1)}) %all-gather.2.cloned.1.call-update) | async-done | bytes 4194320 | tf_op jit(solution)/shard_map/all_gather | solution.py:94
  132.3 3.7 %convolution_convert_fusion.1 = bf16[1024,256]{1,0:T(8,128)(2,1)S(1)} fusion(bf16[1024,2048]{1,0:T(8,128)(2,1)} %all-gather.2.cloned.1.call-done, bf16[2048,256]{1,0:T(8,128)(2,1)} %param.16), kind=kOutput, calls=%fused_computation.31 | convolution fusion | flops 1074003968 | bytes 5767168 | tf_op jit(solution)/shard_map/dot_general | solution.py:95
  136.1 0.9 reshape.273
  137.0 3.4 %fusion.18 = f32[1024,2]{0,1:T(2,128)S(1)} fusion(bf16[1024,2048]{1,0:T(8,128)(2,1)} %all-gather.2.cloned.1.call-done, bf16[2048,8]{0,1:T(8,128)(2,1)} %param.17, s32[]{:T(128)S(6)} %select_n.109), kind=kOutput, calls=%fused_computation.35 | convolution fusion | flops 8394752 | bytes 4210692 | tf_op jit(solution)/shard_map/dot_general | solution.py:96
  140.4 113.7 %all-to-all-done.1 = bf16[32,128,512]{2,1,0:T(8,128)(2,1)} async-done(((bf16[32,128,512]{2,1,0:T(8,128)(2,1)}), bf16[32,128,512]{2,1,0:T(8,128)(2,1)}, u32[]{:S(2)}, u32[]{:S(2)}) %all-to-all-start.1) | async-done | bytes 4194336 | tf_op jit(solution)/shard_map/all_to_all | solution.py:118
  254.1 2.9 gather_fusion.1
  257.4 1.2 fusion.46
  258.6 1.5 copy.54
  260.1 2.0 fusion.47
  262.1 2.8 fusion.22
  265.5 5.3 %convolution_bitcast_fusion = f32[8,128,2,128]{1,3,2,0:T(8,128)S(1)} fusion(bf16[8,256,2,128]{1,3,2,0:T(8,128)(2,1)S(1)} %bitcast.77, f32[8,2,128]{2,1,0:T(2,128)S(1)} %fusion.47, f32[8,2,128,256]{3,2,1,0:T(8,128)} %fusion.22), kind=kOutput, calls=%fused_computation.30 | convolution fusion | flops 136317184 | bytes 4202496 | tf_op jit(solution)/shard_map/bhqk,bkhd->bqhd/dot_general | solution.py:139
  271.6 1.6 broadcast_in_dim.70
  273.2 4.9 %all-to-all-start.2 = ((bf16[4,1024,256]{1,2,0:T(8,128)(2,1)}), bf16[4,1024,256]{1,2,0:T(8,128)(2,1)}, u32[]{:S(2)}, u32[]{:S(2)}) async-start(bf16[4,1024,256]{1,2,0:T(8,128)(2,1)} %broadcast_in_dim.70), calls=%async_computation.2 | async-start | bytes 4194304 | tf_op jit(solution)/shard_map/all_to_all | solution.py:26
  278.4 1.6 fusion.12
  280.1 1.3 copy-done.2
  281.5 2.3 broadcast_add_fusion
  283.8 1.7 copy.46
  285.5 3.1 fusion.14
  288.6 15.6 %all-to-all-done.2 = bf16[4,1024,256]{1,2,0:T(8,128)(2,1)} async-done(((bf16[4,1024,256]{1,2,0:T(8,128)(2,1)}), bf16[4,1024,256]{1,2,0:T(8,128)(2,1)}, u32[]{:S(2)}, u32[]{:S(2)}) %all-to-all-start.2) | async-done | bytes 2097184 | tf_op jit(solution)/shard_map/all_to_all | solution.py:26
  304.2 2.9 fusion.50
  307.1 1.7 add_convert_fusion
  (61 shorter events, 6.1 us)
Async XLA Ops:
  6.5 297.6 %copy-start = (bf16[1024,512]{1,0:T(8,128)(2,1)S(1)}, bf16[1024,512]{1,0:T(8,128)(2,1)}, u32[]{:S(2)}) copy-start(bf16[1024,512]{1,0:T(8,128)(2,1)} %param.20) | copy-start | bytes 3145732
  8.7 35.5 %all-to-all-start = ((s32[32,1,2]{2,1,0:T(1,128)}), s32[32,1,2]{2,1,0:T(1,128)S(1)}, u32[]{:S(2)}, u32[]{:S(2)}) async-start(s32[32,1,2]{2,1,0:T(1,128)} %bitcast.9), calls=%async_computation | async-start | bytes 32768 | tf_op jit(solution)/shard_map/all_to_all | solution.py:114
  32.0 4.2 %copy-start.5 = (f32[2048]{0:T(1024)S(1)}, f32[2048]{0:T(1024)}, u32[]{:S(2)}) copy-start(f32[2048]{0:T(1024)} %param.21) | copy-start | bytes 24580
  36.2 4.4 %copy-start.7 = (bf16[2048,256]{1,0:T(8,128)(2,1)S(1)}, bf16[2048,256]{1,0:T(8,128)(2,1)}, u32[]{:S(2)}) copy-start(bf16[2048,256]{1,0:T(8,128)(2,1)} %param.19) | copy-start | bytes 3145732
  36.2 4.5 %copy-start.8 = (bf16[2048,256]{1,0:T(8,128)(2,1)S(1)}, bf16[2048,256]{1,0:T(8,128)(2,1)}, u32[]{:S(2)}) copy-start(bf16[2048,256]{1,0:T(8,128)(2,1)} %param.18) | copy-start | bytes 3145732
  52.6 13.4 %copy-start.3 = (bf16[1024,512]{1,0:T(8,128)(2,1)S(1)}, bf16[1024,512]{1,0:T(8,128)(2,1)}, u32[]{:S(2)}) copy-start(bf16[1024,512]{1,0:T(8,128)(2,1)} %param.12) | copy-start | bytes 3145732
  52.6 201.5 %all-to-all-start.1 = ((bf16[32,128,512]{2,1,0:T(8,128)(2,1)}), bf16[32,128,512]{2,1,0:T(8,128)(2,1)}, u32[]{:S(2)}, u32[]{:S(2)}) async-start(bf16[32,128,512]{2,1,0:T(8,128)(2,1)} %bitcast_select_fusion), calls=%async_computation.1 | async-start | bytes 8388608 | tf_op jit(solution)/shard_map/all_to_all | solution.py:118
  65.1 67.2 %all-gather.2.cloned.1.call-start = ((), (), s32[]{:S(2)}) async-start(), calls=%async_computation.3 | async-start | bytes 5242880 | tf_op jit(solution)/shard_map/all_gather | solution.py:94
  273.2 4.9 %copy-start.1 = (bf16[1024,512]{1,0:T(8,128)(2,1)S(1)}, bf16[1024,512]{1,0:T(8,128)(2,1)}, u32[]{:S(2)}) copy-start(bf16[1024,512]{1,0:T(8,128)(2,1)} %fusion.8) | copy-start | bytes 3145732
  273.2 30.9 %all-to-all-start.2 = ((bf16[4,1024,256]{1,2,0:T(8,128)(2,1)}), bf16[4,1024,256]{1,2,0:T(8,128)(2,1)}, u32[]{:S(2)}, u32[]{:S(2)}) async-start(bf16[4,1024,256]{1,2,0:T(8,128)(2,1)} %broadcast_in_dim.70), calls=%async_computation.2 | async-start | bytes 4194304 | tf_op jit(solution)/shard_map/all_to_all | solution.py:26
  280.1 1.3 copy-start.2
  304.2 2.9 copy-start.4
  304.2 2.9 copy-start.6
Sparse Core Ops, SparseCore 0:
  78.8 53.5 all-gather.1
where the time goes:
time: 316 us
  waiting for transfers between devices  183 us (58%)
  starting transfers between devices  40.8 us (13%)
  matrix products  25.5 us (8%)
  other arithmetic  23.1 us (7%)
  local copies, waits for them, and re-layouts  19.1 us (6%)
  between operations  13.7 us (4%)
  blocking collectives  10.9 us (3%)
    all_to_all x1, waiting for transfers between devices, per_device(): lax.all_to_all(projected.reshape(st_count, capacity * PLEN, 2 * head_widt...  114 us
    all_gather x1, waiting for transfers between devices, per_device(): columns = lax.all_gather(normed, 'tp', axis=1, tiled=True)  53.2 us
    all_to_all x1, starting transfers between devices, per_device(): lax.all_to_all(request_table, 'st', split_axis=0, concat_axis=0, tiled=True)  23.3 us
    all_to_all x1, waiting for transfers between devices, copy_for_each(): return lax.all_to_all(copies, axis, split_axis=0, concat_axis=0, tiled=True)  15.6 us
    all_to_all x1, starting transfers between devices, per_device(): lax.all_to_all(projected.reshape(st_count, capacity * PLEN, 2 * head_widt...  12.6 us
    psum x1, blocking collectives, per_device(): square_sums = lax.psum(jnp.sum(wide_tokens * wide_tokens, axis=1), 'tp')  10.9 us
  transfers between devices with their start and end apart: 4, of which 3 were waited for; matrix products, arithmetic and copies ran while one was open for 10% of the time, Pallas kernels for 0%

commit v1 on v0

v1 whole, which is shorter than its diff:
```python
import jax
import jax.numpy as jnp
from jax import lax
from jax.experimental import pallas as pl
from jax.experimental.pallas import tpu as pltpu
from jax.sharding import PartitionSpec as P

HD = 128
GROUPS = 4
SEQ_LEN = 256
BLK = 128
NPB = 4
PLEN = 64
P_DEV = 24

epsilon = 1e-06
PROJ_ROWS = 256
PACK_SLOTS = 16
OUT_ROWS = 256


def project_kernel(store_ref, gain_ref, key_ref, value_ref, out_ref):
    wide = store_ref[...].astype(jnp.float32)
    inverse = lax.rsqrt(jnp.mean(wide * wide, axis=-1, keepdims=True) + epsilon)
    rows = (wide * inverse * gain_ref[...]).astype(jnp.bfloat16)
    half = key_ref.shape[1]
    keys = jnp.dot(rows, key_ref[...], preferred_element_type=jnp.float32)
    values = jnp.dot(rows, value_ref[...], preferred_element_type=jnp.float32)
    out_ref[:, :half] = keys.astype(jnp.bfloat16)
    out_ref[:, half:] = values.astype(jnp.bfloat16)


def project_store(store, gain, key_weight, value_weight):
    rows, width = store.shape
    head_width = key_weight.shape[1]
    return pl.pallas_call(
        project_kernel,
        grid=(rows // PROJ_ROWS,),
        in_specs=[
            pl.BlockSpec((PROJ_ROWS, width), lambda i: (i, 0)),
            pl.BlockSpec((1, width), lambda i: (0, 0)),
            pl.BlockSpec((width, head_width), lambda i: (0, 0)),
            pl.BlockSpec((width, head_width), lambda i: (0, 0)),
        ],
        out_specs=pl.BlockSpec((PROJ_ROWS, 2 * head_width), lambda i: (i, 0)),
        out_shape=jax.ShapeDtypeStruct((rows, 2 * head_width), jnp.bfloat16),
        name="project_store",
    )(store, gain.reshape(1, width), key_weight, value_weight)


def pack_kernel(index_ref, store_ref, out_ref):
    count = out_ref.shape[0]
    first = pl.program_id(0) * count
    for slot in range(count):
        out_ref[slot] = store_ref[index_ref[first + slot]]


def pack_slots(index, store):
    slots = index.shape[0]
    _, rows, width = store.shape
    return pl.pallas_call(
        pack_kernel,
        grid_spec=pltpu.PrefetchScalarGridSpec(
            num_scalar_prefetch=1,
            grid=(slots // PACK_SLOTS,),
            in_specs=[pl.BlockSpec(store.shape, lambda i, s: (0, 0, 0))],
            out_specs=pl.BlockSpec((PACK_SLOTS, rows, width), lambda i, s: (i, 0, 0)),
        ),
        out_shape=jax.ShapeDtypeStruct((slots, rows, width), jnp.bfloat16),
        name="pack_slots",
    )(index, store)


def attend_kernel(first, index_ref, query_ref, gate_ref, table_ref, out_ref):
    blocks = out_ref.shape[0] // BLK
    width = query_ref.shape[1]
    for block in range(blocks):
        rows = slice(block * BLK, (block + 1) * BLK)
        slots = [index_ref[(first + block) * NPB + part] for part in range(NPB)]
        for head in range(width // HD):
            cols = slice(head * HD, (head + 1) * HD)
            late = slice(width + head * HD, width + (head + 1) * HD)
            keys = jnp.concatenate([table_ref[slot, :, cols] for slot in slots], axis=0)
            values = jnp.concatenate([table_ref[slot, :, late] for slot in slots], axis=0)
            scores = lax.dot_general(
                query_ref[rows, cols],
                keys,
                (((1,), (1,)), ((), ())),
                preferred_element_type=jnp.float32,
            ) * HD ** (-0.5)
            weights = jnp.exp(scores - jnp.max(scores, axis=-1, keepdims=True))
            total = jnp.sum(weights, axis=-1, keepdims=True)
            probabilities = (weights / total).astype(jnp.bfloat16)
            attended = jnp.dot(probabilities, values, preferred_element_type=jnp.float32)
            out_ref[rows, cols] = (attended * gate_ref[rows, head : head + 1]).astype(jnp.bfloat16)


def attend(index, queries, gates, table, half):
    rows, width = queries.shape
    rows = rows // 2
    first = half * rows // BLK
    return pl.pallas_call(
        lambda *refs: attend_kernel(first, *refs),
        grid_spec=pltpu.PrefetchScalarGridSpec(
            num_scalar_prefetch=1,
            grid=(1,),
            in_specs=[
                pl.BlockSpec((rows, width), lambda i, s: (half, 0)),
                pl.BlockSpec((rows, gates.shape[1]), lambda i, s: (half, 0)),
                pl.BlockSpec(table.shape, lambda i, s: (0, 0, 0)),
            ],
            out_specs=pl.BlockSpec((rows, width), lambda i, s: (0, 0)),
        ),
        out_shape=jax.ShapeDtypeStruct((rows, width), jnp.bfloat16),
        name="attend",
    )(index, queries, gates, table)


def add_products_kernel(*refs):
    base_ref, out_ref = refs[0], refs[-1]
    pairs = refs[1:-1]
    count = len(pairs) // 2
    total = base_ref[...]
    for k in range(count):
        total = total + jnp.dot(
            pairs[k][...], pairs[count + k][...], preferred_element_type=jnp.float32
        )
    out_ref[...] = total.astype(out_ref.dtype)


def add_products(base, pieces, weights, dtype):
    rows, width = base.shape
    steps = rows // OUT_ROWS
    narrow = pieces[0].shape[1]
    return pl.pallas_call(
        add_products_kernel,
        grid=(steps,),
        in_specs=[pl.BlockSpec((OUT_ROWS, width), lambda i: (i, 0))]
        + [pl.BlockSpec((OUT_ROWS, narrow), lambda i: (i, 0))] * len(pieces)
        + [pl.BlockSpec((narrow, width), lambda i: (0, 0))] * len(weights),
        out_specs=pl.BlockSpec((OUT_ROWS, width), lambda i: (i, 0)),
        out_shape=jax.ShapeDtypeStruct((rows, width), dtype),
        name="add_products",
    )(base, *pieces, *weights)


def per_device(
    tokens,
    norm_gain,
    pool_weight,
    pool_scale,
    query_weight,
    gate_weight,
    key_weight,
    value_weight,
    out_weight,
    passage_gain,
    passage_store,
    passage_ids,
):
    head_index = lax.axis_index("tp")
    tp_count = lax.axis_size("tp")
    tok_rows, width_local = tokens.shape
    full_width = width_local * tp_count
    local_heads = query_weight.shape[1] // HD
    store_rows = passage_store.shape[0] * PLEN

    flat_ids = passage_ids.reshape(-1)
    asked_count = flat_ids.shape[0]
    st_count = lax.axis_size("st")
    capacity = max(2, (asked_count + st_count - 1) // st_count)
    owners = flat_ids // P_DEV
    local_index = flat_ids % P_DEV
    order_index = jnp.arange(asked_count, dtype=jnp.int32)
    earlier = (owners[None, :] == owners[:, None]) & (order_index[None, :] < order_index[:, None])
    slot_index = jnp.sum(earlier.astype(jnp.int32), axis=1)
    position_flat = owners * capacity + slot_index
    slot_range = jnp.arange(st_count * capacity, dtype=jnp.int32)
    request_table = jnp.sum(
        jnp.where(position_flat[None, :] == slot_range[:, None], local_index[None, :], 0), axis=1
    )
    request_table = request_table.reshape(st_count, capacity)
    asked = lax.all_to_all(request_table, "st", split_axis=0, concat_axis=0, tiled=True)

    projected = project_store(
        passage_store.reshape(store_rows, full_width), passage_gain, key_weight, value_weight
    )
    width_both = projected.shape[1]
    packed = pack_slots(asked.reshape(-1), projected.reshape(-1, PLEN, width_both))
    returned = lax.all_to_all(
        packed.reshape(st_count, capacity * PLEN, width_both),
        "st",
        split_axis=0,
        concat_axis=0,
        tiled=True,
    ).reshape(st_count * capacity, PLEN, width_both)

    wide_tokens = tokens.astype(jnp.float32)
    square_sums = lax.psum(jnp.sum(wide_tokens * wide_tokens, axis=1), "tp")
    inverse = lax.rsqrt(square_sums / full_width + epsilon)
    gain_local = lax.dynamic_slice_in_dim(norm_gain, head_index * width_local, width_local)
    normed = (wide_tokens * inverse[:, None] * gain_local[None, :]).astype(jnp.bfloat16)
    columns = lax.all_gather(normed, "tp", axis=1, tiled=True)

    sequences = tok_rows // SEQ_LEN
    window = jnp.left_shift(jnp.int32(2), head_index)
    grouped = normed.astype(jnp.float32).reshape(sequences, SEQ_LEN, width_local)
    total = grouped
    for level in range(GROUPS):
        shift = 2**level
        moved = jnp.pad(total, ((0, 0), (shift, 0), (0, 0)))[:, :SEQ_LEN]
        total = jnp.where(level <= head_index, total + moved, total)
    position = jnp.arange(SEQ_LEN, dtype=jnp.int32)
    divisor = jnp.minimum(position + 1, window).astype(jnp.float32)
    pooled = (
        (total / divisor[None, :, None] - grouped)
        .astype(jnp.bfloat16)
        .reshape(tok_rows, width_local)
    )
    base = (
        jnp.dot(pooled, pool_weight[0], preferred_element_type=jnp.float32) * pool_scale[None, :]
    )

    gate_columns = lax.dynamic_slice_in_dim(
        gate_weight, head_index * local_heads, local_heads, axis=1
    )
    query_sum = jnp.dot(columns, query_weight, preferred_element_type=jnp.float32)
    gate_sum = jnp.dot(columns, gate_columns, preferred_element_type=jnp.float32)
    queries = query_sum.astype(jnp.bfloat16)
    gating = jax.nn.sigmoid(gate_sum)

    rows_of = out_weight.reshape(tp_count, local_heads * HD, width_local)
    weights = [
        lax.dynamic_index_in_dim(rows_of, (head_index + place) % tp_count, 0, keepdims=False)
        for place in (0, tp_count - 1, 1, 2)
    ]
    queries, gating, base, weights = lax.optimization_barrier((queries, gating, base, weights))

    up = [(i, (i + 1) % tp_count) for i in range(tp_count)]
    down = [(i, (i - 1) % tp_count) for i in range(tp_count)]
    low = attend(position_flat, queries, gating, returned, 0)
    low_before = lax.ppermute(low, "tp", up)
    high = attend(position_flat, queries, gating, returned, 1)
    high_after = lax.ppermute(high, "tp", down)
    high_before = lax.ppermute(high, "tp", up)
    low_after = lax.ppermute(low, "tp", down)
    low_far = lax.ppermute(low_before, "tp", up)
    high_far = lax.ppermute(high_after, "tp", down)
    half = tok_rows // 2
    sides = ((low, low_before, low_after, low_far), (high, high_before, high_after, high_far))
    outs = []
    for side, (own, before, after, far) in enumerate(sides):
        part = base[side * half : (side + 1) * half]
        part = add_products(part, (own, before, after), weights[:3], jnp.float32)
        outs.append(add_products(part, (far,), weights[3:], jnp.bfloat16))
    return jnp.concatenate(outs, axis=0)


def solution(mesh):
    in_specs = (
        P(("grp", "st"), "tp"),
        P(),
        P("tp", None, None),
        P("tp"),
        P(None, "tp"),
        P(),
        P(None, "tp"),
        P(None, "tp"),
        P(None, "tp"),
        P(),
        P(("grp", "st"), None, None),
        P(("grp", "st"), None),
    )
    out_specs = P(("grp", "st"), "tp")
    return jax.shard_map(
        per_device, mesh=mesh, in_specs=in_specs, out_specs=out_specs, check_vma=False
    )
```

time: 316 us -> 298 us (0.943)
  Pallas kernels: 0 us -> 34.5 us
  matrix products: 25.5 us -> 7.16 us
  other arithmetic: 23.1 us -> 9.12 us
  waiting for transfers between devices: 183 us -> 170 us
  local copies, waits for them, and re-layouts: 19.1 us -> 8.94 us
    pallas_call x0 -> x8, Pallas kernels: none -> 34.5 us  [the longest x4 10.8 us: add_products(): pl.pallas_call(add_products_kernel, grid=(steps,), in_specs=[pl.BlockSpec...]
    dot_general x4 -> x0, matrix products: 14.6 us -> none  [the longest x1 5.31 us: per_device(): jnp.einsum('bhqk,bkhd->bqhd', probabilities, values, preferred_element_ty...]
    all_to_all x2 -> x1, waiting for transfers between devices: 129 us -> 115 us  [per_device(): lax.all_to_all(packed.reshape(st_count, capacity * PLEN, width_both), 'st...]
    ppermute x0 -> x6, starting transfers between devices: none -> 8.63 us  [the longest x1 2.94 us: per_device(): high_far = lax.ppermute(high_after, 'tp', down)]
    convert_element_type x3 -> x1, other arithmetic: 7.72 us -> 0.56 us  [per_device(): pooled = (total / divisor[None, :, None] - grouped).astype(jnp.bfloat16)....]
    all_gather x1, waiting for transfers between devices: 53.2 us -> 46.2 us  [per_device(): columns = lax.all_gather(normed, 'tp', axis=1, tiled=True)]
    all_to_all x2 -> x1, starting transfers between devices: 17.4 us -> 10.8 us  [per_device(): lax.all_to_all(packed.reshape(st_count, capacity * PLEN, width_both), 'st...]
    ppermute x0 -> x6, waiting for transfers between devices: none -> 6.5 us  [the longest x1 5.43 us: per_device(): high_after = lax.ppermute(high, 'tp', down)]
  transfers between devices with their start and end apart: 4 -> 9, of which waited for: 3 -> 5; matrix products, arithmetic and copies ran while one was open for 10% -> 5% of each run, Pallas kernels for 0% -> 8%
where the time goes in v1:
time: 298 us; the launch traced here: 297 us
  waiting for transfers between devices  170 us (57%)
  starting transfers between devices  42.8 us (14%)
  Pallas kernels  34.5 us (12%)
  between operations  13.7 us (5%)
  blocking collectives  11 us (4%)
  other arithmetic  9.12 us (3%)
  local copies, waits for them, and re-layouts  8.94 us (3%)
  matrix products  7.16 us (2%)
    all_to_all x1, waiting for transfers between devices, per_device(): lax.all_to_all(packed.reshape(st_count, capacity * PLEN, width_both), 'st...  115 us
    all_gather x1, waiting for transfers between devices, per_device(): columns = lax.all_gather(normed, 'tp', axis=1, tiled=True)  46.2 us
    all_to_all x1, starting transfers between devices, per_device(): lax.all_to_all(request_table, 'st', split_axis=0, concat_axis=0, tiled=True)  23.3 us
    psum x1, blocking collectives, per_device(): square_sums = lax.psum(jnp.sum(wide_tokens * wide_tokens, axis=1), 'tp')  11 us
    pallas_call x4, Pallas kernels, add_products(): pl.pallas_call(add_products_kernel, grid=(steps,), in_specs=[pl.BlockSpec...  10.8 us
    all_to_all x1, starting transfers between devices, per_device(): lax.all_to_all(packed.reshape(st_count, capacity * PLEN, width_both), 'st...  10.8 us
    pallas_call x2, Pallas kernels, attend(): pl.pallas_call(lambda *refs: attend_kernel(first, *refs), grid_spec=pltpu...  9.94 us
    pallas_call x1, Pallas kernels, project_store(): pl.pallas_call(project_kernel, grid=(rows // PROJ_ROWS,), in_specs=[pl.Bl...  9.16 us
  transfers between devices with their start and end apart: 9, of which 5 were waited for; matrix products, arithmetic and copies ran while one was open for 5% of the time, Pallas kernels for 8%

profile of v1, /device:TPU:160, one launch (start us, length us, event | category | flops | bytes accessed | tf_op | source)
XLA Modules:
  0.0 297.0 jit_solution(11058901144201570690)
XLA Ops:
  6.6 0.8 sign_compare_fusion
  8.8 0.7 all_to_all.9
  9.6 23.3 %all-to-all-start = ((s32[32,1,2]{2,1,0:T(1,128)}), s32[32,1,2]{2,1,0:T(1,128)S(1)}, u32[]{:S(2)}, u32[]{:S(2)}) async-start(s32[32,1,2]{2,1,0:T(1,128)} %bitcast.9), calls=%async_computation | async-start | bytes 32768 | tf_op jit(solution)/shard_map/all_to_all | solution.py:183
  32.9 9.2 %project_store.1 = bf16[1536,512]{1,0:T(8,128)(2,1)} custom-call(bf16[1536,2048]{1,0:T(8,128)(2,1)} %bitcast.28, f32[1,2048]{1,0:T(1,128)} %bitcast.32, bf16[2048,256]{1,0:T(8,128)(2,1)} %key_ref.1, bf16[2048,256]{1,0:T(8,128)(2,1)} %value_ref.1), custom_call_target="tpu_custom_call" | custom-call | tf_op jit(solution)/shard_map/project_store/pallas_call | solution.py:36
  42.0 1.8 all-to-all-done
  45.6 4.6 %pack_slots.1 = bf16[64,64,512]{2,1,0:T(8,128)(2,1)} custom-call(s32[64]{0:T(128)} %reshape.110.index_ref, bf16[24,64,512]{2,1,0:T(8,128)(2,1)} %bitcast.29), custom_call_target="tpu_custom_call" | custom-call | tf_op jit(solution)/shard_map/pack_slots/pallas_call | solution.py:61
  50.2 10.8 %all-to-all-start.1 = ((bf16[32,128,512]{2,1,0:T(8,128)(2,1)}), bf16[32,128,512]{2,1,0:T(8,128)(2,1)}, u32[]{:S(2)}, u32[]{:S(2)}) async-start(bf16[32,128,512]{2,1,0:T(8,128)(2,1)} %bitcast.27), calls=%async_computation.1 | async-start | bytes 8388608 | tf_op jit(solution)/shard_map/all_to_all | solution.py:190
  61.1 0.8 dynamic_slice.19
  62.1 11.0 %psum.7 = f32[1024]{0:T(1024)S(1)} all-reduce(f32[1024]{0:T(1024)S(1)} %fusion), channel_id=1, replica_groups=mesh['grp'=2,'st'=32,'tp'=4] {'tp'}, use_global_device_ids=true, to_apply=%region_1.2 | all-reduce | flops 1024 | bytes 8192 | tf_op jit(solution)/shard_map/psum | solution.py:199
  73.1 1.3 fusion.2
  74.5 1.5 convert.1
  76.0 2.2 dynamic-slice_bitcast_fusion
  79.2 0.9 copy-done.1
  81.9 46.2 %all-gather.2.cloned.1.call-done = bf16[1024,2048]{1,0:T(8,128)(2,1)} async-done(((bf16[1024,512]{1,0:T(8,128)(2,1)}), bf16[1024,2048]{1,0:T(8,128)(2,1)}) %all-gather.2.cloned.1.call-update) | async-done | bytes 4194320 | tf_op jit(solution)/shard_map/all_gather | solution.py:203
  128.1 4.4 %fusion.8.refs_2_ = f32[1024,2]{1,0:T(8,128)} fusion(bf16[1024,2048]{1,0:T(8,128)(2,1)} %all-gather.2.cloned.1.call-done, bf16[2048,8]{0,1:T(8,128)(2,1)} %param.17, s32[]{:T(128)S(6)} %select_n.95), kind=kOutput, calls=%fused_computation.21 | convolution fusion | flops 8394752 | bytes 4210692 | tf_op jit(solution)/shard_map/dot_general | solution.py:228
  132.5 2.1 convolution_convert_fusion.refs_1_
  134.6 115.3 %all-to-all-done.1 = bf16[32,128,512]{2,1,0:T(8,128)(2,1)} async-done(((bf16[32,128,512]{2,1,0:T(8,128)(2,1)}), bf16[32,128,512]{2,1,0:T(8,128)(2,1)}, u32[]{:S(2)}, u32[]{:S(2)}) %all-to-all-start.1) | async-done | bytes 4194336 | tf_op jit(solution)/shard_map/all_to_all | solution.py:190
  249.9 5.0 %attend.2.refs_1_ = bf16[512,256]{1,0:T(8,128)(2,1)} custom-call(s32[32]{0:T(128)} %copy-done.8, bf16[1024,256]{1,0:T(8,128)(2,1)} %convolution_convert_fusion.refs_1_, f32[1024,2]{1,0:T(8,128)} %fusion.8.refs_2_, bf16[64,64,512]{2,1,0:T(8,128)(2,1)} %bitcast.14.refs_3_), custom_call_target="tpu_custom_call" | custom-call | tf_op jit(solution)/shard_map/attend/pallas_call | solution.py:102
  254.9 1.6 collective-permute-start
  256.5 5.0 %attend.3.refs_1_ = bf16[512,256]{1,0:T(8,128)(2,1)} custom-call(s32[32]{0:T(128)} %copy-done.8, bf16[1024,256]{1,0:T(8,128)(2,1)} %convolution_convert_fusion.refs_1_, f32[1024,2]{1,0:T(8,128)} %fusion.8.refs_2_, bf16[64,64,512]{2,1,0:T(8,128)(2,1)} %bitcast.14.refs_3_), custom_call_target="tpu_custom_call" | custom-call | tf_op jit(solution)/shard_map/attend/pallas_call | solution.py:102
  261.5 1.7 collective-permute-start.4
  263.2 1.8 collective-permute-start.1
  265.6 5.4 %collective-permute-done.4.refs_3_ = bf16[512,256]{1,0:T(8,128)(2,1)} collective-permute-done((bf16[512,256]{1,0:T(8,128)(2,1)}, bf16[512,256]{1,0:T(8,128)(2,1)}, u32[]{:S(2)}, u32[]{:S(2)}) %collective-permute-start.4) | collective-permute-done | bytes 262176 | tf_op jit(solution)/shard_map/ppermute | solution.py:244
  271.0 2.9 collective-permute-start.5
  273.9 1.5 fusion.13
  275.4 1.1 collective-permute-done.1.refs_3_
  276.5 0.7 copy-done.6
  277.2 3.0 %add_products.4.refs_0_ = f32[512,512]{1,0:T(8,128)} custom-call(f32[512,512]{1,0:T(8,128)} %get-tuple-element.19.refs_0_, bf16[512,256]{1,0:T(8,128)(2,1)} %attend.2.refs_1_, bf16[512,256]{1,0:T(8,128)(2,1)} %collective-permute-done.refs_2_, bf16[512,256]{1,0:T(8,128)(2,1)} %copy-done.6, bf16[256,512]{1,0:T(8,128)(2,1)} %get-tuple-element.15.refs_4_, ...), custom_call_target="tpu_custom_call" | custom-call | tf_op jit(solution)/shard_map/add_products/pallas_call | solution.py:135
  280.2 3.1 %add_products.6.refs_0_ = f32[512,512]{1,0:T(8,128)} custom-call(f32[512,512]{1,0:T(8,128)} %get-tuple-element.20.refs_0_, bf16[512,256]{1,0:T(8,128)(2,1)} %attend.3.refs_1_, bf16[512,256]{1,0:T(8,128)(2,1)} %collective-permute-done.3.refs_2_, bf16[512,256]{1,0:T(8,128)(2,1)} %collective-permute-done.4.refs_3_, bf16[256,512]{1,0:T(8,128)(2,1)} %get-tuple-element.15.refs_4_, ...), custom_call_target="tpu_custom_call" | custom-call | tf_op jit(solution)/shard_map/add_products/pallas_call | solution.py:135
  283.3 2.3 add_products.5
  285.6 2.4 add_products.7
  288.1 2.1 pad_maximum_fusion
  (48 shorter events, 6.9 us)
Async XLA Ops:
  6.5 126.0 %copy-start = (bf16[2048,256]{1,0:T(8,128)(2,1)S(1)}, bf16[2048,256]{1,0:T(8,128)(2,1)}, u32[]{:S(2)}) copy-start(bf16[2048,256]{1,0:T(8,128)(2,1)} %param.16) | copy-start | bytes 3145732
  8.7 33.3 %copy-start.8 = (s32[32]{0:T(128)}, s32[32]{0:T(128)S(1)}, u32[]{:S(2)}) copy-start(s32[32]{0:T(128)S(1)} %multiply_add_fusion.refs_0_) | copy-start | bytes 388
  9.6 34.3 %all-to-all-start = ((s32[32,1,2]{2,1,0:T(1,128)}), s32[32,1,2]{2,1,0:T(1,128)S(1)}, u32[]{:S(2)}, u32[]{:S(2)}) async-start(s32[32,1,2]{2,1,0:T(1,128)} %bitcast.9), calls=%async_computation | async-start | bytes 32768 | tf_op jit(solution)/shard_map/all_to_all | solution.py:183
  50.2 11.6 %copy-start.2 = (bf16[1024,512]{1,0:T(8,128)(2,1)S(1)}, bf16[1024,512]{1,0:T(8,128)(2,1)}, u32[]{:S(2)}) copy-start(bf16[1024,512]{1,0:T(8,128)(2,1)} %param.12) | copy-start | bytes 3145732
  50.2 199.7 %all-to-all-start.1 = ((bf16[32,128,512]{2,1,0:T(8,128)(2,1)}), bf16[32,128,512]{2,1,0:T(8,128)(2,1)}, u32[]{:S(2)}, u32[]{:S(2)}) async-start(bf16[32,128,512]{2,1,0:T(8,128)(2,1)} %bitcast.27), calls=%async_computation.1 | async-start | bytes 8388608 | tf_op jit(solution)/shard_map/all_to_all | solution.py:190
  61.0 67.1 %all-gather.2.cloned.1.call-start = ((), (), s32[]{:S(2)}) async-start(), calls=%async_computation.2 | async-start | bytes 5242880 | tf_op jit(solution)/shard_map/all_gather | solution.py:203
  78.9 1.2 copy-start.1
  80.1 1.0 copy-start.5
  80.1 1.0 copy-start.7
  128.1 4.4 %copy-start.9 = (bf16[1024,2048]{1,0:T(8,128)(2,1)S(1)}, bf16[1024,2048]{1,0:T(8,128)(2,1)}, u32[]{:S(2)}) copy-start(bf16[1024,2048]{1,0:T(8,128)(2,1)} %all-gather.2.cloned.1.call-done) | copy-start | bytes 12582916
  254.9 8.3 %copy-start.4 = (bf16[512,256]{1,0:T(8,128)(2,1)S(1)}, bf16[512,256]{1,0:T(8,128)(2,1)}, u32[]{:S(2)}) copy-start(bf16[512,256]{1,0:T(8,128)(2,1)} %attend.2.refs_1_) | copy-start | bytes 786436
  254.9 10.4 %collective-permute-start = (bf16[512,256]{1,0:T(8,128)(2,1)}, bf16[512,256]{1,0:T(8,128)(2,1)}, u32[]{:S(2)}, u32[]{:S(2)}) collective-permute-start(bf16[512,256]{1,0:T(8,128)(2,1)} %attend.2.refs_1_), channel_id=1, source_target_pairs={{0,1},{1,2},{2,3},{3,0},{4,5},{5,6},{6,7},{7,4},{8,9},{9,10},{10,1... | collective-permute-start | bytes 786440 | tf_op jit(solution)/shard_map/ppermute | solution.py:242
  261.5 9.5 %collective-permute-start.4 = (bf16[512,256]{1,0:T(8,128)(2,1)}, bf16[512,256]{1,0:T(8,128)(2,1)}, u32[]{:S(2)}, u32[]{:S(2)}) collective-permute-start(bf16[512,256]{1,0:T(8,128)(2,1)} %attend.3.refs_1_), channel_id=1, source_target_pairs={{0,3},{1,0},{2,1},{3,2},{4,7},{5,4},{6,5},{7,6},{8,11},{9,8},{10,9... | collective-permute-start | bytes 786440 | tf_op jit(solution)/shard_map/ppermute | solution.py:244
  263.2 13.3 %collective-permute-start.1 = (bf16[512,256]{1,0:T(8,128)(2,1)S(1)}, bf16[512,256]{1,0:T(8,128)(2,1)S(1)}, u32[]{:S(2)}, u32[]{:S(2)}) collective-permute-start(bf16[512,256]{1,0:T(8,128)(2,1)S(1)} %copy-done.4), channel_id=1, source_target_pairs={{0,3},{1,0},{2,1},{3,2},{4,7},{5,4},{6,5},{7,6},{8,11},{9,8},{10,9... | collective-permute-start | bytes 786440 | tf_op jit(solution)/shard_map/ppermute | solution.py:246
  265.1 15.2 %collective-permute-start.3 = (bf16[512,256]{1,0:T(8,128)(2,1)}, bf16[512,256]{1,0:T(8,128)(2,1)}, u32[]{:S(2)}, u32[]{:S(2)}) collective-permute-start(bf16[512,256]{1,0:T(8,128)(2,1)} %attend.3.refs_1_), channel_id=1, source_target_pairs={{0,1},{1,2},{2,3},{3,0},{4,5},{5,6},{6,7},{7,4},{8,9},{9,10},{10,1... | collective-permute-start | bytes 786440 | tf_op jit(solution)/shard_map/ppermute | solution.py:245
  265.3 18.0 %collective-permute-start.2 = (bf16[512,256]{1,0:T(8,128)(2,1)}, bf16[512,256]{1,0:T(8,128)(2,1)}, u32[]{:S(2)}, u32[]{:S(2)}) collective-permute-start(bf16[512,256]{1,0:T(8,128)(2,1)} %collective-permute-done.refs_2_), channel_id=1, source_target_pairs={{0,1},{1,2},{2,3},{3,0},{4,5},{5,6},{6,7},{7,4},{8,9},{9,10},{10,1... | collective-permute-start | bytes 786440 | tf_op jit(solution)/shard_map/ppermute | solution.py:247
  271.0 14.7 %collective-permute-start.5 = (bf16[512,256]{1,0:T(8,128)(2,1)}, bf16[512,256]{1,0:T(8,128)(2,1)}, u32[]{:S(2)}, u32[]{:S(2)}) collective-permute-start(bf16[512,256]{1,0:T(8,128)(2,1)} %collective-permute-done.4.refs_3_), channel_id=1, source_target_pairs={{0,3},{1,0},{2,1},{3,2},{4,7},{5,4},{6,5},{7,6},{8,11},{9,8},{10,9... | collective-permute-start | bytes 786440 | tf_op jit(solution)/shard_map/ppermute | solution.py:248
  276.5 0.7 copy-start.6
  285.6 2.4 copy-start.3
Sparse Core Ops, SparseCore 0:
  74.5 53.5 all-gather.1

commit v2 on v0

v2 whole, which is shorter than its diff:
```python
import jax
import jax.numpy as jnp
from jax import lax
from jax.experimental import pallas as pl
from jax.experimental.pallas import tpu as pltpu
from jax.sharding import PartitionSpec as P

HD = 128
GROUPS = 4
SEQ_LEN = 256
BLK = 128
NPB = 4
PLEN = 64

epsilon = 1e-06
TILE = 8
SELECT_READERS = 4
OUT_ROWS = 256


def spread_kernel(store_ref, gain_ref, key_ref, value_ref, order_ref, out_ref):
    passages, tile, width = store_ref.shape
    wide = store_ref[...].astype(jnp.float32).reshape(passages * tile, width)
    inverse = lax.rsqrt(jnp.mean(wide * wide, axis=-1, keepdims=True) + epsilon)
    rows = (wide * gain_ref[...]).astype(jnp.bfloat16)
    half = key_ref.shape[1]
    for part, weight_ref in enumerate((key_ref, value_ref)):
        product = jnp.dot(rows, weight_ref[...], preferred_element_type=jnp.float32)
        product = (product * inverse).astype(jnp.bfloat16)
        turned = jnp.dot(order_ref[...], product, preferred_element_type=jnp.float32)
        turned = turned.reshape(tile, passages, half).astype(jnp.bfloat16)
        out_ref[:, :, part * half : (part + 1) * half] = turned


def spread_store(store, gain, key_weight, value_weight, holders):
    passages, length, width = store.shape
    head_width = key_weight.shape[1]
    rows = passages * TILE
    spot = jnp.arange(rows, dtype=jnp.int32)
    wanted = (spot % passages) * TILE + spot // passages
    order = (wanted[:, None] == spot[None, :]).astype(jnp.bfloat16)
    groups = holders // TILE
    return pl.pallas_call(
        spread_kernel,
        grid=(length // TILE,),
        in_specs=[
            pl.BlockSpec((passages, TILE, width), lambda i: (0, i, 0)),
            pl.BlockSpec((1, width), lambda i: (0, 0)),
            pl.BlockSpec((width, head_width), lambda i: (0, 0)),
            pl.BlockSpec((width, head_width), lambda i: (0, 0)),
            pl.BlockSpec((rows, rows), lambda i: (0, 0)),
        ],
        out_specs=pl.BlockSpec(
            (TILE, passages, 2 * head_width), lambda i: (i % groups, i // groups, 0)
        ),
        out_shape=jax.ShapeDtypeStruct(
            (holders, passages * length // holders, 2 * head_width), jnp.bfloat16
        ),
        name="spread_store",
    )(store, gain.reshape(1, width), key_weight, value_weight, order)


def select_kernel(wanted_ref, table_ref, out_ref):
    count = wanted_ref.shape[0]
    spot = lax.broadcasted_iota(jnp.int32, (count, table_ref.shape[0]), 1)
    chosen = jnp.where(spot == wanted_ref[...], 1.0, 0.0).astype(jnp.bfloat16)
    out_ref[...] = jnp.dot(chosen, table_ref[...], preferred_element_type=jnp.float32).astype(
        jnp.bfloat16
    )


def select_rows(wanted, table, step_rows):
    rows = wanted.shape[0]
    width = table.shape[1]
    return pl.pallas_call(
        select_kernel,
        grid=(rows // step_rows,),
        in_specs=[
            pl.BlockSpec((step_rows, 1), lambda i: (i, 0)),
            pl.BlockSpec(table.shape, lambda i: (0, 0)),
        ],
        out_specs=pl.BlockSpec((step_rows, width), lambda i: (i, 0)),
        out_shape=jax.ShapeDtypeStruct((rows, width), jnp.bfloat16),
        name="select_rows",
    )(wanted, table)


def attend_kernel(query_ref, gate_ref, table_ref, out_ref):
    holders, tile, both = table_ref.shape
    width = query_ref.shape[1]
    table = table_ref[...].astype(jnp.float32).reshape(holders * tile, both)
    table = table.astype(jnp.bfloat16)
    for head in range(width // HD):
        cols = slice(head * HD, (head + 1) * HD)
        late = slice(width + head * HD, width + (head + 1) * HD)
        scores = lax.dot_general(
            query_ref[:, cols],
            table[:, cols],
            (((1,), (1,)), ((), ())),
            preferred_element_type=jnp.float32,
        ) * HD ** (-0.5)
        weights = jnp.exp(scores - jnp.max(scores, axis=-1, keepdims=True))
        total = jnp.sum(weights, axis=-1, keepdims=True)
        probabilities = (weights / total).astype(jnp.bfloat16)
        attended = jnp.dot(probabilities, table[:, late], preferred_element_type=jnp.float32)
        out_ref[:, cols] = (attended * gate_ref[:, head : head + 1]).astype(jnp.bfloat16)


def attend(queries, gates, table, half):
    rows, width = queries.shape
    rows = rows // 2
    blocks = rows // BLK
    first = half * blocks
    holders, _, both = table.shape
    return pl.pallas_call(
        attend_kernel,
        grid=(blocks,),
        in_specs=[
            pl.BlockSpec((BLK, width), lambda i: (first + i, 0)),
            pl.BlockSpec((BLK, gates.shape[1]), lambda i: (first + i, 0)),
            pl.BlockSpec((holders, TILE, both), lambda i: (0, first + i, 0)),
        ],
        out_specs=pl.BlockSpec((BLK, width), lambda i: (i, 0)),
        out_shape=jax.ShapeDtypeStruct((rows, width), jnp.bfloat16),
        name="attend",
    )(queries, gates, table)


def finish_kernel(halves, weight_ref, base_ref, *refs):
    out_ref = refs[-1]
    pieces = refs[:-1]
    count = len(pieces) // halves
    step = pl.program_id(0)
    each = pl.num_programs(0) // halves
    for half in range(halves):

        @pl.when(step // each == half)
        def _():
            total = base_ref[...]
            for k in range(count):
                total = total + jnp.dot(
                    pieces[half * count + k][...], weight_ref[k], preferred_element_type=jnp.float32
                )
            out_ref[...] = total.astype(out_ref.dtype)


def finish(base, sides, weights):
    rows, width = base.shape
    halves = len(sides)
    each = rows // OUT_ROWS // halves
    narrow = sides[0][0].shape[1]

    def spec(half):
        return pl.BlockSpec(
            (OUT_ROWS, narrow), lambda i: (jnp.clip(i - half * each, 0, each - 1), 0)
        )

    return pl.pallas_call(
        lambda *refs: finish_kernel(halves, *refs),
        grid=(each * halves,),
        in_specs=[
            pl.BlockSpec(weights.shape, lambda i: (0, 0, 0)),
            pl.BlockSpec((OUT_ROWS, width), lambda i: (i, 0)),
        ]
        + [spec(half) for half in range(halves) for _ in sides[half]],
        out_specs=pl.BlockSpec((OUT_ROWS, width), lambda i: (i, 0)),
        out_shape=jax.ShapeDtypeStruct((rows, width), jnp.bfloat16),
        name="finish",
    )(weights, base, *[piece for side in sides for piece in side])


def per_device(
    tokens,
    norm_gain,
    pool_weight,
    pool_scale,
    query_weight,
    gate_weight,
    key_weight,
    value_weight,
    out_weight,
    passage_gain,
    passage_store,
    passage_ids,
):
    head_index = lax.axis_index("tp")
    tp_count = lax.axis_size("tp")
    tok_rows, width_local = tokens.shape
    full_width = width_local * tp_count
    local_heads = query_weight.shape[1] // HD
    st_count = lax.axis_size("st")
    passages = passage_store.shape[0]
    shares = PLEN // st_count
    spread = spread_store(passage_store, passage_gain, key_weight, value_weight, st_count)
    width_both = spread.shape[2]
    held = lax.all_to_all(spread, "st", split_axis=0, concat_axis=0, tiled=True)

    all_ids = lax.all_gather(passage_ids.reshape(-1), "st", axis=0)
    all_ids = all_ids.reshape(st_count, -1, 1, NPB)
    owners = lax.div(all_ids, jnp.int32(passages))
    share = jnp.arange(shares, dtype=jnp.int32)[None, None, :, None]
    wanted = owners * (shares * passages) + share * passages + (all_ids - owners * passages)
    packed = select_rows(
        wanted.reshape(-1, 1),
        held.reshape(-1, width_both),
        SELECT_READERS * NPB * shares * (tok_rows // BLK),
    )
    returned = lax.all_to_all(
        packed.reshape(st_count, -1, width_both), "st", split_axis=0, concat_axis=0, tiled=True
    )

    wide_tokens = tokens.astype(jnp.float32)
    square_sums = lax.psum(jnp.sum(wide_tokens * wide_tokens, axis=1), "tp")
    inverse = lax.rsqrt(square_sums / full_width + epsilon)
    gain_local = lax.dynamic_slice_in_dim(norm_gain, head_index * width_local, width_local)
    normed = (wide_tokens * inverse[:, None] * gain_local[None, :]).astype(jnp.bfloat16)
    columns = lax.all_gather(normed, "tp", axis=1, tiled=True)

    sequences = tok_rows // SEQ_LEN
    window = jnp.left_shift(jnp.int32(2), head_index)
    grouped = normed.astype(jnp.float32).reshape(sequences, SEQ_LEN, width_local)
    total = grouped
    for level in range(GROUPS):
        shift = 2**level
        moved = jnp.pad(total, ((0, 0), (shift, 0), (0, 0)))[:, :SEQ_LEN]
        total = jnp.where(level <= head_index, total + moved, total)
    position = jnp.arange(SEQ_LEN, dtype=jnp.int32)
    divisor = jnp.minimum(position + 1, window).astype(jnp.float32)
    pooled = (
        (total / divisor[None, :, None] - grouped)
        .astype(jnp.bfloat16)
        .reshape(tok_rows, width_local)
    )
    base = (
        jnp.dot(pooled, pool_weight[0], preferred_element_type=jnp.float32) * pool_scale[None, :]
    )

    gate_columns = lax.dynamic_slice_in_dim(
        gate_weight, head_index * local_heads, local_heads, axis=1
    )
    query_sum = jnp.dot(columns, query_weight, preferred_element_type=jnp.float32)
    gate_sum = jnp.dot(columns, gate_columns, preferred_element_type=jnp.float32)
    queries = query_sum.astype(jnp.bfloat16)
    gating = jax.nn.sigmoid(gate_sum)

    rows_of = out_weight.reshape(tp_count, local_heads * HD, width_local)
    turned = (head_index + jnp.array([0, tp_count - 1, 1, 2], dtype=jnp.int32)) % tp_count
    weights = jnp.take(rows_of, turned, axis=0, mode="clip")
    queries, gating, base, weights = lax.optimization_barrier((queries, gating, base, weights))

    up = [(i, (i + 1) % tp_count) for i in range(tp_count)]
    down = [(i, (i - 1) % tp_count) for i in range(tp_count)]
    low = attend(queries, gating, returned, 0)
    low_before = lax.ppermute(low, "tp", up)
    low_after = lax.ppermute(low, "tp", down)
    high = attend(queries, gating, returned, 1)
    high_before = lax.ppermute(high, "tp", up)
    high_after = lax.ppermute(high, "tp", down)
    low_far = lax.ppermute(low_before, "tp", up)
    high_far = lax.ppermute(high_after, "tp", down)
    sides = ((low, low_before, low_after, low_far), (high, high_before, high_after, high_far))
    return finish(base, sides, weights)


def solution(mesh):
    in_specs = (
        P(("grp", "st"), "tp"),
        P(),
        P("tp", None, None),
        P("tp"),
        P(None, "tp"),
        P(),
        P(None, "tp"),
        P(None, "tp"),
        P(None, "tp"),
        P(),
        P(("grp", "st"), None, None),
        P(("grp", "st"), None),
    )
    out_specs = P(("grp", "st"), "tp")
    return jax.shard_map(
        per_device, mesh=mesh, in_specs=in_specs, out_specs=out_specs, check_vma=False
    )
```

time: 316 us -> 306 us (0.968); the launches traced: 316 us -> 301 us
  waiting for transfers between devices: 183 us -> 74.5 us
  blocking collectives: 10.9 us -> 102 us
  Pallas kernels: 0 us -> 37.6 us
  matrix products: 25.5 us -> 8.47 us
  other arithmetic: 23.1 us -> 11.8 us
  local copies, waits for them, and re-layouts: 19.1 us -> 9 us
  starting transfers between devices: 40.8 us -> 44.1 us
    all_to_all x3 -> x2, waiting for transfers between devices: 129 us -> 23.6 us  [the longest x1 23.6 us: per_device(): lax.all_to_all(packed.reshape(st_count, -1, width_both), 'st', split_axis...]
    all_gather x0 -> x1, blocking collectives: none -> 91.4 us  [per_device(): all_ids = lax.all_gather(passage_ids.reshape(-1), 'st', axis=0)]
    pallas_call x0 -> x5, Pallas kernels: none -> 37.6 us  [the longest x1 13.2 us: spread_store(): pl.pallas_call(spread_kernel, grid=(length // TILE,), in_specs=[pl.BlockS...]
    dot_general x4 -> x0, matrix products: 14.6 us -> none  [the longest x1 5.31 us: per_device(): jnp.einsum('bhqk,bkhd->bqhd', probabilities, values, preferred_element_ty...]
    all_gather x1, waiting for transfers between devices: 53.2 us -> 41.7 us  [per_device(): columns = lax.all_gather(normed, 'tp', axis=1, tiled=True)]
    ppermute x0 -> x6, waiting for transfers between devices: none -> 9.21 us  [the longest x1 5.33 us: per_device(): high_after = lax.ppermute(high, 'tp', down)]
    ppermute x0 -> x6, starting transfers between devices: none -> 8.5 us  [the longest x1 2.83 us: per_device(): high_far = lax.ppermute(high_after, 'tp', down)]
    convert_element_type x3 -> x2, other arithmetic: 7.72 us -> 1.3 us  [the longest x1 0.74 us: spread_store(): order = (wanted[:, None] == spot[None, :]).astype(jnp.bfloat16)]
  transfers between devices with their start and end apart: 4 -> 9, of which waited for: 3 -> 6; matrix products, arithmetic and copies ran while one was open for 10% -> 8% of each run, Pallas kernels for 0% -> 2%
where the time goes in v2:
time: 306 us; the launch traced here: 301 us
  blocking collectives  102 us (33%)
  waiting for transfers between devices  74.5 us (24%)
  starting transfers between devices  44.1 us (14%)
  Pallas kernels  37.6 us (12%)
  between operations  13.6 us (4%)
  other arithmetic  11.8 us (4%)
  local copies, waits for them, and re-layouts  9 us (3%)
  matrix products  8.47 us (3%)
    all_gather x1, blocking collectives, per_device(): all_ids = lax.all_gather(passage_ids.reshape(-1), 'st', axis=0)  91.4 us
    all_gather x1, waiting for transfers between devices, per_device(): columns = lax.all_gather(normed, 'tp', axis=1, tiled=True)  41.7 us
    all_to_all x1, waiting for transfers between devices, per_device(): lax.all_to_all(packed.reshape(st_count, -1, width_both), 'st', split_axis...  23.6 us
    all_to_all x1, starting transfers between devices, per_device(): held = lax.all_to_all(spread, 'st', split_axis=0, concat_axis=0, tiled=True)  23.4 us
    pallas_call x1, Pallas kernels, spread_store(): pl.pallas_call(spread_kernel, grid=(length // TILE,), in_specs=[pl.BlockS...  13.2 us
    all_to_all x1, starting transfers between devices, per_device(): lax.all_to_all(packed.reshape(st_count, -1, width_both), 'st', split_axis...  12.1 us
    psum x1, blocking collectives, per_device(): square_sums = lax.psum(jnp.sum(wide_tokens * wide_tokens, axis=1), 'tp')  10.9 us
    pallas_call x2, Pallas kernels, attend(): pl.pallas_call(attend_kernel, grid=(blocks,), in_specs=[pl.BlockSpec((BLK...  10.4 us
  transfers between devices with their start and end apart: 9, of which 6 were waited for; matrix products, arithmetic and copies ran while one was open for 8% of the time, Pallas kernels for 2%

profile of v2, /device:TPU:160, one launch (start us, length us, event | category | flops | bytes accessed | tf_op | source)
XLA Modules:
  0.0 301.4 jit_solution(11963021612522023348)
XLA Ops:
  7.3 13.2 %spread_store.1 = bf16[32,48,512]{2,1,0:T(8,128)(2,1)} custom-call(bf16[24,64,2048]{2,1,0:T(8,128)(2,1)} %store_ref.1, f32[1,2048]{1,0:T(1,128)} %bitcast.22, bf16[2048,256]{1,0:T(8,128)(2,1)} %key_ref.1, bf16[2048,256]{1,0:T(8,128)(2,1)} %value_ref.1, bf16[192,192]{1,0:T(8,128)(2,1)} %fusion.10.order_ref), custom_call_target="tpu_custom_call" | custom-call | tf_op jit(solution)/shard_map/spread_store/pallas_call | solution.py:43
  20.5 23.4 %all-to-all-start = ((bf16[32,48,512]{2,1,0:T(8,128)(2,1)}), bf16[32,48,512]{2,1,0:T(8,128)(2,1)S(1)}, u32[]{:S(2)}, u32[]{:S(2)}) async-start(bf16[32,48,512]{2,1,0:T(8,128)(2,1)} %spread_store.1), calls=%async_computation | async-start | bytes 3145728 | tf_op jit(solution)/shard_map/all_to_all | solution.py:196
  44.1 91.4 %all-gather = s32[32,1,32]{2,1,0:T(1,128)S(1)} all-gather(s32[1,1,32]{2,1,0:T(1,128)S(1)} %reshape.133), channel_id=1, replica_groups=mesh['grp'=2,'st'=32,'tp'=4] {'st'}, dimensions={0}, use_global_device_ids=true | all-gather | bytes 4224 | tf_op jit(solution)/shard_map/all_gather | solution.py:198
  136.1 1.4 add.142.wanted_ref
  137.6 1.2 copy-done.3
  138.7 8.5 %select_rows.1 = bf16[2048,512]{1,0:T(8,128)(2,1)} custom-call(s32[2048,1]{1,0:T(8,128)} %add.142.wanted_ref, bf16[1536,512]{1,0:T(8,128)(2,1)} %bitcast.19), custom_call_target="tpu_custom_call" | custom-call | tf_op jit(solution)/shard_map/select_rows/pallas_call | solution.py:75
  147.2 12.1 %all-to-all-start.1 = ((bf16[32,64,512]{2,1,0:T(8,128)(2,1)}), bf16[32,64,512]{2,1,0:T(8,128)(2,1)S(1)}, u32[]{:S(2)}, u32[]{:S(2)}) async-start(bf16[32,64,512]{2,1,0:T(8,128)(2,1)} %bitcast.18), calls=%async_computation.1 | async-start | bytes 4194304 | tf_op jit(solution)/shard_map/all_to_all | solution.py:208
  159.4 0.8 dynamic_slice.6
  160.2 1.5 fusion
  161.7 10.9 %psum.7 = f32[1024]{0:T(1024)S(1)} all-reduce(f32[1024]{0:T(1024)S(1)} %fusion), channel_id=1, replica_groups=mesh['grp'=2,'st'=32,'tp'=4] {'tp'}, use_global_device_ids=true, to_apply=%region_1.2 | all-reduce | flops 1024 | bytes 8192 | tf_op jit(solution)/shard_map/psum | solution.py:213
  172.7 2.5 fusion.2
  175.2 2.9 convert.1
  178.1 1.7 gather_fusion
  179.8 2.7 add_select_fusion.3
  183.3 0.9 copy-done.2
  185.2 2.1 convolution_multiply_fusion.refs_1_
  187.3 41.7 %all-gather.3.cloned.1.call-done = bf16[1024,2048]{1,0:T(8,128)(2,1)} async-done(((bf16[1024,512]{1,0:T(8,128)(2,1)}), bf16[1024,2048]{1,0:T(8,128)(2,1)}) %all-gather.3.cloned.1.call-update) | async-done | bytes 4194320 | tf_op jit(solution)/shard_map/all_gather | solution.py:217
  228.9 4.4 %fusion.8.gate_ref = f32[1024,2]{1,0:T(8,128)} fusion(bf16[1024,2048]{1,0:T(8,128)(2,1)} %all-gather.3.cloned.1.call-done, bf16[2048,8]{0,1:T(8,128)(2,1)} %param.18, s32[]{:T(128)S(6)} %select_n.59), kind=kOutput, calls=%fused_computation.22 | convolution fusion | flops 8394752 | bytes 4210692 | tf_op jit(solution)/shard_map/dot_general | solution.py:242
  233.3 2.0 convolution_convert_fusion.query_ref
  235.3 23.6 %all-to-all-done.1.table_ref = bf16[32,64,512]{2,1,0:T(8,128)(2,1)S(1)} async-done(((bf16[32,64,512]{2,1,0:T(8,128)(2,1)}), bf16[32,64,512]{2,1,0:T(8,128)(2,1)S(1)}, u32[]{:S(2)}, u32[]{:S(2)}) %all-to-all-start.1) | async-done | bytes 2097184 | tf_op jit(solution)/shard_map/all_to_all | solution.py:208
  258.9 1.3 copy-done.1
  260.3 5.2 %attend.2.refs_2_ = bf16[512,256]{1,0:T(8,128)(2,1)} custom-call(bf16[1024,256]{1,0:T(8,128)(2,1)} %convolution_convert_fusion.query_ref, f32[1024,2]{1,0:T(8,128)} %fusion.8.gate_ref, bf16[32,64,512]{2,1,0:T(8,128)(2,1)} %copy-done.1), custom_call_target="tpu_custom_call" | custom-call | tf_op jit(solution)/shard_map/attend/pallas_call | solution.py:115
  265.5 1.6 collective-permute-start
  267.1 5.2 %attend.3.refs_6_ = bf16[512,256]{1,0:T(8,128)(2,1)} custom-call(bf16[1024,256]{1,0:T(8,128)(2,1)} %convolution_convert_fusion.query_ref, f32[1024,2]{1,0:T(8,128)} %fusion.8.gate_ref, bf16[32,64,512]{2,1,0:T(8,128)(2,1)} %copy-done.1), custom_call_target="tpu_custom_call" | custom-call | tf_op jit(solution)/shard_map/attend/pallas_call | solution.py:115
  272.3 1.6 collective-permute-start.4
  274.0 2.0 collective-permute-start.1
  276.4 5.3 %collective-permute-done.4.refs_8_ = bf16[512,256]{1,0:T(8,128)(2,1)S(1)} collective-permute-done((bf16[512,256]{1,0:T(8,128)(2,1)}, bf16[512,256]{1,0:T(8,128)(2,1)S(1)}, u32[]{:S(2)}, u32[]{:S(2)}) %collective-permute-start.4) | collective-permute-done | bytes 262176 | tf_op jit(solution)/shard_map/ppermute | solution.py:258
  281.7 2.8 collective-permute-start.5
  284.6 1.0 collective-permute-done.1.refs_4_
  285.6 1.4 collective-permute-done.2.refs_5_
  287.0 1.4 collective-permute-done.5.refs_9_
  289.2 5.4 %finish.1 = bf16[1024,512]{1,0:T(8,128)(2,1)} custom-call(bf16[4,256,512]{2,1,0:T(8,128)(2,1)} %gather_fusion, f32[1024,512]{1,0:T(8,128)} %convolution_multiply_fusion.refs_1_, bf16[512,256]{1,0:T(8,128)(2,1)} %attend.2.refs_2_, bf16[512,256]{1,0:T(8,128)(2,1)} %copy-done.6, bf16[512,256]{1,0:T(8,128)(2,1)} %copy-done.8, bf16[512,256]{1,0:T(8,128)(2,1)} %copy-done.10, ...), custom_call_target="tpu_custom_call" | custom-call | tf_op jit(solution)/shard_map/finish/pallas_call | solution.py:158
  (55 shorter events, 4.6 us)
Async XLA Ops:
  6.5 171.6 %copy-start = (bf16[1024,512]{1,0:T(8,128)(2,1)S(1)}, bf16[1024,512]{1,0:T(8,128)(2,1)}, u32[]{:S(2)}) copy-start(bf16[1024,512]{1,0:T(8,128)(2,1)} %param.21) | copy-start | bytes 3145732
  20.5 23.4 %copy-start.13 = (s32[8,4]{0,1:T(4,128)S(1)}, s32[8,4]{0,1:T(4,128)}, u32[]{:S(2)}) copy-start(s32[8,4]{0,1:T(4,128)} %param.24) | copy-start | bytes 388
  20.5 117.0 %all-to-all-start = ((bf16[32,48,512]{2,1,0:T(8,128)(2,1)}), bf16[32,48,512]{2,1,0:T(8,128)(2,1)S(1)}, u32[]{:S(2)}, u32[]{:S(2)}) async-start(bf16[32,48,512]{2,1,0:T(8,128)(2,1)} %spread_store.1), calls=%async_computation | async-start | bytes 3145728 | tf_op jit(solution)/shard_map/all_to_all | solution.py:196
  137.6 1.2 copy-start.3
  147.2 111.7 %all-to-all-start.1 = ((bf16[32,64,512]{2,1,0:T(8,128)(2,1)}), bf16[32,64,512]{2,1,0:T(8,128)(2,1)S(1)}, u32[]{:S(2)}, u32[]{:S(2)}) async-start(bf16[32,64,512]{2,1,0:T(8,128)(2,1)} %bitcast.18), calls=%async_computation.1 | async-start | bytes 4194304 | tf_op jit(solution)/shard_map/all_to_all | solution.py:208
  159.4 69.6 %all-gather.3.cloned.1.call-start = ((), (), s32[]{:S(2)}) async-start(), calls=%async_computation.2 | async-start | bytes 5242880 | tf_op jit(solution)/shard_map/all_gather | solution.py:217
  175.2 2.9 copy-start.16
  182.9 1.2 copy-start.2
  184.2 1.0 copy-start.5
  184.2 1.0 copy-start.12
  228.9 4.4 %copy-start.14 = (bf16[1024,2048]{1,0:T(8,128)(2,1)S(1)}, bf16[1024,2048]{1,0:T(8,128)(2,1)}, u32[]{:S(2)}) copy-start(bf16[1024,2048]{1,0:T(8,128)(2,1)} %all-gather.3.cloned.1.call-done) | copy-start | bytes 12582916
  228.9 4.4 %copy-start.15 = (bf16[2048,256]{1,0:T(8,128)(2,1)S(1)}, bf16[2048,256]{1,0:T(8,128)(2,1)}, u32[]{:S(2)}) copy-start(bf16[2048,256]{1,0:T(8,128)(2,1)} %param.17) | copy-start | bytes 3145732
  258.9 1.3 copy-start.1
  265.5 8.5 %copy-start.4 = (bf16[512,256]{1,0:T(8,128)(2,1)S(1)}, bf16[512,256]{1,0:T(8,128)(2,1)}, u32[]{:S(2)}) copy-start(bf16[512,256]{1,0:T(8,128)(2,1)} %attend.2.refs_2_) | copy-start | bytes 786436
  265.5 10.5 %collective-permute-start = (bf16[512,256]{1,0:T(8,128)(2,1)}, bf16[512,256]{1,0:T(8,128)(2,1)S(1)}, u32[]{:S(2)}, u32[]{:S(2)}) collective-permute-start(bf16[512,256]{1,0:T(8,128)(2,1)} %attend.2.refs_2_), channel_id=1, source_target_pairs={{0,1},{1,2},{2,3},{3,0},{4,5},{5,6},{6,7},{7,4},{8,9},{9,10},{10,1... | collective-permute-start | bytes 786440 | tf_op jit(solution)/shard_map/ppermute | solution.py:254
  272.3 9.4 %collective-permute-start.4 = (bf16[512,256]{1,0:T(8,128)(2,1)}, bf16[512,256]{1,0:T(8,128)(2,1)S(1)}, u32[]{:S(2)}, u32[]{:S(2)}) collective-permute-start(bf16[512,256]{1,0:T(8,128)(2,1)} %attend.3.refs_6_), channel_id=1, source_target_pairs={{0,3},{1,0},{2,1},{3,2},{4,7},{5,4},{6,5},{7,6},{8,11},{9,8},{10,9... | collective-permute-start | bytes 786440 | tf_op jit(solution)/shard_map/ppermute | solution.py:258
  274.0 11.6 %collective-permute-start.1 = (bf16[512,256]{1,0:T(8,128)(2,1)S(1)}, bf16[512,256]{1,0:T(8,128)(2,1)S(1)}, u32[]{:S(2)}, u32[]{:S(2)}) collective-permute-start(bf16[512,256]{1,0:T(8,128)(2,1)S(1)} %copy-done.4), channel_id=1, source_target_pairs={{0,3},{1,0},{2,1},{3,2},{4,7},{5,4},{6,5},{7,6},{8,11},{9,8},{10,9... | collective-permute-start | bytes 786440 | tf_op jit(solution)/shard_map/ppermute | solution.py:255
  275.9 9.7 %collective-permute-start.3 = (bf16[512,256]{1,0:T(8,128)(2,1)}, bf16[512,256]{1,0:T(8,128)(2,1)S(1)}, u32[]{:S(2)}, u32[]{:S(2)}) collective-permute-start(bf16[512,256]{1,0:T(8,128)(2,1)} %attend.3.refs_6_), channel_id=1, source_target_pairs={{0,1},{1,2},{2,3},{3,0},{4,5},{5,6},{6,7},{7,4},{8,9},{9,10},{10,1... | collective-permute-start | bytes 786440 | tf_op jit(solution)/shard_map/ppermute | solution.py:257
  276.0 12.5 %copy-start.6 = (bf16[512,256]{1,0:T(8,128)(2,1)}, bf16[512,256]{1,0:T(8,128)(2,1)S(1)}, u32[]{:S(2)}) copy-start(bf16[512,256]{1,0:T(8,128)(2,1)S(1)} %collective-permute-done.refs_3_) | copy-start | bytes 786436
  276.0 11.0 %collective-permute-start.2 = (bf16[512,256]{1,0:T(8,128)(2,1)S(1)}, bf16[512,256]{1,0:T(8,128)(2,1)S(1)}, u32[]{:S(2)}, u32[]{:S(2)}) collective-permute-start(bf16[512,256]{1,0:T(8,128)(2,1)S(1)} %collective-permute-done.refs_3_), channel_id=1, source_target_pairs={{0,1},{1,2},{2,3},{3,0},{4,5},{5,6},{6,7},{7,4},{8,9},{9,10},{10,1... | collective-permute-start | bytes 786440 | tf_op jit(solution)/shard_map/ppermute | solution.py:259
  281.7 6.7 %copy-start.7 = (bf16[512,256]{1,0:T(8,128)(2,1)}, bf16[512,256]{1,0:T(8,128)(2,1)S(1)}, u32[]{:S(2)}) copy-start(bf16[512,256]{1,0:T(8,128)(2,1)S(1)} %collective-permute-done.4.refs_8_) | copy-start | bytes 786436
  281.7 6.7 %collective-permute-start.5 = (bf16[512,256]{1,0:T(8,128)(2,1)S(1)}, bf16[512,256]{1,0:T(8,128)(2,1)S(1)}, u32[]{:S(2)}, u32[]{:S(2)}) collective-permute-start(bf16[512,256]{1,0:T(8,128)(2,1)S(1)} %collective-permute-done.4.refs_8_), channel_id=1, source_target_pairs={{0,3},{1,0},{2,1},{3,2},{4,7},{5,4},{6,5},{7,6},{8,11},{9,8},{10,9... | collective-permute-start | bytes 786440 | tf_op jit(solution)/shard_map/ppermute | solution.py:260
  285.6 2.9 copy-start.8
  285.6 2.9 copy-start.9
  287.0 1.5 copy-start.10
  288.5 0.7 copy-start.11
Sparse Core Ops, SparseCore 0:
  175.3 53.5 all-gather.2

commit v3 on v2

v3 whole, which is shorter than its diff:
```python
import jax
import jax.numpy as jnp
from jax import lax
from jax.experimental import pallas as pl
from jax.experimental.pallas import tpu as pltpu
from jax.sharding import PartitionSpec as P

HD = 128
GROUPS = 4
SEQ_LEN = 256
BLK = 128
NPB = 4
PLEN = 64

epsilon = 1e-06
LANES = 128
TILE = 8
SHARE_ROWS = 16
SELECT_READERS = 8
OUT_ROWS = 256
whole = pl.BlockSpec(memory_space=pltpu.VMEM)


def spread_kernel(ids_ref, store_ref, gain_ref, key_ref, value_ref, out_ref, order_ref):
    step = pl.program_id(0)
    passages, span, width = store_ref.shape
    rows = passages * span
    holders = out_ref.shape[0]
    groups = holders // span
    shares = pl.num_programs(0) // groups
    body = shares * passages

    @pl.when(step == 0)
    def _():
        spot = lax.broadcasted_iota(jnp.int32, (rows, rows), 0)
        holder = lax.div(spot, jnp.int32(passages))
        wanted = (spot - holder * passages) * span + holder
        other = lax.broadcasted_iota(jnp.int32, (rows, rows), 1)
        order_ref[...] = jnp.where(wanted == other, 1.0, 0.0).astype(jnp.bfloat16)
        line = lax.broadcasted_iota(jnp.int32, (TILE, LANES), 0)
        lane = lax.broadcasted_iota(jnp.int32, (TILE, LANES), 1)
        share = lax.shift_right_logical(line, 2)
        part_of = line - share * NPB
        blocks = ids_ref.shape[0]
        tile = jnp.zeros((TILE, LANES), jnp.int32)
        for block in range(blocks):
            for part in range(NPB):
                name = ids_ref[block, part]
                owner = lax.div(name, jnp.int32(passages))
                inside = name - owner * passages
                here = part_of == part
                tile = jnp.where(here & (lane == block), owner, tile)
                tile = jnp.where(here & (lane == blocks + block), inside + share * passages, tile)
        tile = tile.astype(jnp.float32).astype(jnp.bfloat16)
        out_ref[:, out_ref.shape[1] - TILE :, :] = jnp.broadcast_to(tile, (holders, TILE, LANES))

    wide = store_ref[...].astype(jnp.float32).reshape(rows, width)
    inverse = lax.rsqrt(jnp.mean(wide * wide, axis=-1, keepdims=True) + epsilon)
    scaled = (wide * gain_ref[...]).astype(jnp.bfloat16)
    first = pl.multiple_of((step % groups) * span, span)
    offset = (step // groups) * passages
    chunks = key_ref.shape[1] // LANES
    for half, weight_ref in enumerate((key_ref, value_ref)):
        product = jnp.dot(scaled, weight_ref[...], preferred_element_type=jnp.float32)
        product = (product * inverse).astype(jnp.bfloat16)
        turned = jnp.dot(order_ref[...], product, preferred_element_type=jnp.float32)
        turned = turned.reshape(span, passages, chunks * LANES).astype(jnp.bfloat16)
        for chunk in range(chunks):
            start = pl.multiple_of((half * chunks + chunk) * body + offset, TILE)
            out_ref[pl.ds(first, span), pl.ds(start, passages), :] = turned[
                :, :, chunk * LANES : (chunk + 1) * LANES
            ]


def spread_store(ids, store, gain, key_weight, value_weight, holders):
    passages, length, width = store.shape
    head_width = key_weight.shape[1]
    rows = passages * SHARE_ROWS
    per_holder = passages * length // holders * (2 * head_width // LANES) + TILE
    return pl.pallas_call(
        spread_kernel,
        grid_spec=pltpu.PrefetchScalarGridSpec(
            num_scalar_prefetch=1,
            grid=(length // SHARE_ROWS,),
            in_specs=[
                pl.BlockSpec((passages, SHARE_ROWS, width), lambda i, s: (0, i, 0)),
                pl.BlockSpec((1, width), lambda i, s: (0, 0)),
                pl.BlockSpec((width, head_width), lambda i, s: (0, 0)),
                pl.BlockSpec((width, head_width), lambda i, s: (0, 0)),
            ],
            out_specs=pl.BlockSpec((holders, per_holder, LANES), lambda i, s: (0, 0, 0)),
            scratch_shapes=[pltpu.VMEM((rows, rows), jnp.bfloat16)],
        ),
        out_shape=jax.ShapeDtypeStruct((holders, per_holder, LANES), jnp.bfloat16),
        name="spread_store",
    )(ids, store, gain.reshape(1, width), key_weight, value_weight)


def select_kernel(blocks, held_ref, out_ref, table_ref):
    step = pl.program_id(0)
    owners = held_ref.shape[0]
    chunks = table_ref.shape[1] // LANES
    body = table_ref.shape[0] // owners

    @pl.when(step == 0)
    def _():
        for owner in range(owners):
            for chunk in range(chunks):
                table_ref[
                    owner * body : (owner + 1) * body, chunk * LANES : (chunk + 1) * LANES
                ] = held_ref[owner, chunk * body : (chunk + 1) * body, :]

    spot = lax.broadcasted_iota(jnp.int32, (TILE, table_ref.shape[0]), 1).astype(jnp.float32)
    chosen = []
    for reader in range(SELECT_READERS):
        tile = held_ref[step * SELECT_READERS + reader, chunks * body :, :].astype(jnp.float32)
        for block in range(blocks):
            wanted = tile[:, block : block + 1] * float(body)
            wanted = wanted + tile[:, blocks + block : blocks + block + 1]
            chosen.append(jnp.where(spot == wanted, 1.0, 0.0))
    chosen = jnp.concatenate(chosen, axis=0).astype(jnp.bfloat16)
    out_ref[...] = jnp.dot(chosen, table_ref[...], preferred_element_type=jnp.float32).astype(
        jnp.bfloat16
    )


def select_rows(held, blocks, body, width):
    owners = held.shape[0]
    step_rows = SELECT_READERS * blocks * TILE
    return pl.pallas_call(
        lambda *refs: select_kernel(blocks, *refs),
        grid=(owners // SELECT_READERS,),
        in_specs=[whole],
        out_specs=pl.BlockSpec((step_rows, width), lambda i: (i, 0)),
        out_shape=jax.ShapeDtypeStruct((owners * blocks * TILE, width), jnp.bfloat16),
        scratch_shapes=[pltpu.VMEM((owners * body, width), jnp.bfloat16)],
        name="select_rows",
    )(held)


def attend_kernel(half, query_ref, gate_ref, table_ref, out_ref):
    holders, _, both = table_ref.shape
    width = query_ref.shape[1]
    rows = out_ref.shape[0]
    for block in range(rows // BLK):
        place = half * rows // BLK + block
        mine = slice(place * BLK, (place + 1) * BLK)
        table = table_ref[:, place * TILE : (place + 1) * TILE, :].astype(jnp.float32)
        table = table.reshape(holders * TILE, both).astype(jnp.bfloat16)
        for head in range(width // HD):
            cols = slice(head * HD, (head + 1) * HD)
            late = slice(width + head * HD, width + (head + 1) * HD)
            scores = lax.dot_general(
                query_ref[mine, cols],
                table[:, cols],
                (((1,), (1,)), ((), ())),
                preferred_element_type=jnp.float32,
            ) * HD ** (-0.5)
            weights = jnp.exp(scores - jnp.max(scores, axis=-1, keepdims=True))
            total = jnp.sum(weights, axis=-1, keepdims=True)
            probabilities = (weights * (1.0 / total)).astype(jnp.bfloat16)
            attended = jnp.dot(probabilities, table[:, late], preferred_element_type=jnp.float32)
            out_ref[block * BLK : (block + 1) * BLK, cols] = (
                attended * gate_ref[mine, head : head + 1]
            ).astype(jnp.bfloat16)


def attend(queries, gates, table, half):
    rows, width = queries.shape
    return pl.pallas_call(
        lambda *refs: attend_kernel(half, *refs),
        in_specs=[whole, whole, whole],
        out_specs=whole,
        out_shape=jax.ShapeDtypeStruct((rows // 2, width), jnp.bfloat16),
        name="attend",
    )(queries, gates, table)


def finish_kernel(halves, weight_ref, base_ref, *refs):
    out_ref = refs[-1]
    pieces = refs[:-1]
    count = len(pieces) // halves
    step = pl.program_id(0)
    each = pl.num_programs(0) // halves
    rows = out_ref.shape[0]
    for half in range(halves):

        @pl.when(step // each == half)
        def _():
            total = base_ref[pl.ds(pl.multiple_of(step * rows, rows), rows), :]
            mine = pl.ds(pl.multiple_of((step - half * each) * rows, rows), rows)
            for k in range(count):
                total = total + jnp.dot(
                    pieces[half * count + k][mine, :],
                    weight_ref[k],
                    preferred_element_type=jnp.float32,
                )
            out_ref[...] = total.astype(out_ref.dtype)


def finish(base, sides, weights):
    rows, width = base.shape
    halves = len(sides)
    pieces = [piece for side in sides for piece in side]
    return pl.pallas_call(
        lambda *refs: finish_kernel(halves, *refs),
        grid=(rows // OUT_ROWS,),
        in_specs=[whole] * (2 + len(pieces)),
        out_specs=pl.BlockSpec((OUT_ROWS, width), lambda i: (i, 0)),
        out_shape=jax.ShapeDtypeStruct((rows, width), jnp.bfloat16),
        name="finish",
    )(weights, base, *pieces)


def per_device(
    tokens,
    norm_gain,
    pool_weight,
    pool_scale,
    query_weight,
    gate_weight,
    key_weight,
    value_weight,
    out_weight,
    passage_gain,
    passage_store,
    passage_ids,
):
    head_index = lax.axis_index("tp")
    tp_count = lax.axis_size("tp")
    tok_rows, width_local = tokens.shape
    full_width = width_local * tp_count
    local_heads = query_weight.shape[1] // HD
    st_count = lax.axis_size("st")
    passages = passage_store.shape[0]
    shares = PLEN // st_count
    spread = spread_store(
        passage_ids, passage_store, passage_gain, key_weight, value_weight, st_count
    )
    held = lax.all_to_all(spread, "st", split_axis=0, concat_axis=0, tiled=True)
    width_both = key_weight.shape[1] + value_weight.shape[1]
    packed = select_rows(held, tok_rows // BLK, shares * passages, width_both)
    returned = lax.all_to_all(
        packed.reshape(st_count, -1, width_both), "st", split_axis=0, concat_axis=0, tiled=True
    )

    wide_tokens = tokens.astype(jnp.float32)
    square_sums = lax.psum(jnp.sum(wide_tokens * wide_tokens, axis=1), "tp")
    inverse = lax.rsqrt(square_sums / full_width + epsilon)
    gain_local = lax.dynamic_slice_in_dim(norm_gain, head_index * width_local, width_local)
    normed = (wide_tokens * inverse[:, None] * gain_local[None, :]).astype(jnp.bfloat16)
    columns = lax.all_gather(normed, "tp", axis=1, tiled=True)

    sequences = tok_rows // SEQ_LEN
    window = jnp.left_shift(jnp.int32(2), head_index)
    grouped = normed.astype(jnp.float32).reshape(sequences, SEQ_LEN, width_local)
    total = grouped
    for level in range(GROUPS):
        shift = 2**level
        moved = jnp.pad(total, ((0, 0), (shift, 0), (0, 0)))[:, :SEQ_LEN]
        total = jnp.where(level <= head_index, total + moved, total)
    position = jnp.arange(SEQ_LEN, dtype=jnp.int32)
    divisor = jnp.minimum(position + 1, window).astype(jnp.float32)
    pooled = (
        (total / divisor[None, :, None] - grouped)
        .astype(jnp.bfloat16)
        .reshape(tok_rows, width_local)
    )
    base = (
        jnp.dot(pooled, pool_weight[0], preferred_element_type=jnp.float32) * pool_scale[None, :]
    )

    gate_columns = lax.dynamic_slice_in_dim(
        gate_weight, head_index * local_heads, local_heads, axis=1
    )
    query_sum = jnp.dot(columns, query_weight, preferred_element_type=jnp.float32)
    gate_sum = jnp.dot(columns, gate_columns, preferred_element_type=jnp.float32)
    queries = query_sum.astype(jnp.bfloat16)
    gating = jax.nn.sigmoid(gate_sum)

    rows_of = out_weight.reshape(tp_count, local_heads * HD, width_local)
    turned = (head_index + jnp.array([0, tp_count - 1, 1, 2], dtype=jnp.int32)) % tp_count
    weights = jnp.take(rows_of, turned, axis=0, mode="clip")
    queries, gating, base, weights = lax.optimization_barrier((queries, gating, base, weights))

    up = [(i, (i + 1) % tp_count) for i in range(tp_count)]
    down = [(i, (i - 1) % tp_count) for i in range(tp_count)]
    low = attend(queries, gating, returned, 0)
    low_before = lax.ppermute(low, "tp", up)
    low_after = lax.ppermute(low, "tp", down)
    high = attend(queries, gating, returned, 1)
    high_before = lax.ppermute(high, "tp", up)
    high_after = lax.ppermute(high, "tp", down)
    low_far = lax.ppermute(low_before, "tp", up)
    high_far = lax.ppermute(high_after, "tp", down)
    sides = ((low, low_before, low_after, low_far), (high, high_before, high_after, high_far))
    return finish(base, sides, weights)


def solution(mesh):
    in_specs = (
        P(("grp", "st"), "tp"),
        P(),
        P("tp", None, None),
        P("tp"),
        P(None, "tp"),
        P(),
        P(None, "tp"),
        P(None, "tp"),
        P(None, "tp"),
        P(),
        P(("grp", "st"), None, None),
        P(("grp", "st"), None),
    )
    out_specs = P(("grp", "st"), "tp")
    return jax.shard_map(
        per_device, mesh=mesh, in_specs=in_specs, out_specs=out_specs, check_vma=False
    )
```

time: 306 us -> 283 us (0.925)
  starting transfers between devices: 44.1 us -> 14.6 us
  blocking collectives: 102 us -> 114 us
  Pallas kernels: 37.6 us -> 33.9 us
    all_to_all x0 -> x1, blocking collectives: none -> 103 us  [per_device(): held = lax.all_to_all(spread, 'st', split_axis=0, concat_axis=0, tiled=True)]
    all_gather x1 -> x0, blocking collectives: 91.4 us -> none  [per_device(): all_ids = lax.all_gather(passage_ids.reshape(-1), 'st', axis=0)]
    all_to_all x1 -> x0, starting transfers between devices: 23.4 us -> none  [per_device(): held = lax.all_to_all(spread, 'st', split_axis=0, concat_axis=0, tiled=True)]
    all_to_all x1, starting transfers between devices: 12.1 us -> 6.06 us  [per_device(): lax.all_to_all(packed.reshape(st_count, -1, width_both), 'st', split_axis...]
    pallas_call x5, Pallas kernels: 37.6 us -> 33.9 us  [the longest x1 13.7 us: spread_store(): pl.pallas_call(spread_kernel, grid_spec=pltpu.PrefetchScalarGridSpec(num_...]
  transfers between devices with their start and end apart: 9 -> 8, of which waited for: 6 -> 6; matrix products, arithmetic and copies ran while one was open for 8% -> 8% of each run, Pallas kernels for 2% -> 1%
where the time goes in v3:
time: 283 us; the launch traced here: 277 us
  blocking collectives  114 us (40%)
  waiting for transfers between devices  74.7 us (26%)
  Pallas kernels  33.9 us (12%)
  starting transfers between devices  14.6 us (5%)
  between operations  13.5 us (5%)
  other arithmetic  10.9 us (4%)
  matrix products  8.48 us (3%)
  local copies, waits for them, and re-layouts  7.33 us (3%)
    all_to_all x1, blocking collectives, per_device(): held = lax.all_to_all(spread, 'st', split_axis=0, concat_axis=0, tiled=True)  103 us
    all_gather x1, waiting for transfers between devices, per_device(): columns = lax.all_gather(normed, 'tp', axis=1, tiled=True)  41.9 us
    all_to_all x1, waiting for transfers between devices, per_device(): lax.all_to_all(packed.reshape(st_count, -1, width_both), 'st', split_axis...  23 us
    pallas_call x1, Pallas kernels, spread_store(): pl.pallas_call(spread_kernel, grid_spec=pltpu.PrefetchScalarGridSpec(num_...  13.7 us
    psum x1, blocking collectives, per_device(): square_sums = lax.psum(jnp.sum(wide_tokens * wide_tokens, axis=1), 'tp')  10.9 us
    pallas_call x2, Pallas kernels, attend(): pl.pallas_call(lambda *refs: attend_kernel(half, *refs), in_specs=[whole,...  7.68 us
    pallas_call x1, Pallas kernels, select_rows(): pl.pallas_call(lambda *refs: select_kernel(blocks, *refs), grid=(owners /...  7.27 us
    all_to_all x1, starting transfers between devices, per_device(): lax.all_to_all(packed.reshape(st_count, -1, width_both), 'st', split_axis...  6.06 us
  transfers between devices with their start and end apart: 8, of which 6 were waited for; matrix products, arithmetic and copies ran while one was open for 8% of the time, Pallas kernels for 1%

profile of v3, /device:TPU:160, one launch (start us, length us, event | category | flops | bytes accessed | tf_op | source)
XLA Modules:
  0.0 277.3 jit_solution(15985689903892019495)
XLA Ops:
  6.6 1.4 copy.15.ids_ref
  8.0 13.7 %spread_store.1 = bf16[32,200,128]{2,1,0:T(8,128)(2,1)} custom-call(s32[8,4]{1,0:T(8,128)} %copy.15.ids_ref, bf16[24,64,2048]{2,1,0:T(8,128)(2,1)} %store_ref.1, f32[1,2048]{1,0:T(1,128)} %bitcast.18, bf16[2048,256]{1,0:T(8,128)(2,1)} %key_ref.1, bf16[2048,256]{1,0:T(8,128)(2,1)} %value_ref.1), custom_call_target="tpu_custom_call" | custom-call | tf_op jit(solution)/shard_map/spread_store/pallas_call | solution.py:80
  21.7 102.9 %all_to_all.10.refs_0_ = bf16[32,200,128]{2,1,0:T(8,128)(2,1)} all-to-all(bf16[32,200,128]{2,1,0:T(8,128)(2,1)} %spread_store.1), channel_id=1, replica_groups=mesh['grp'=2,'st'=32,'tp'=4] {'st'}, dimensions={0} | all-to-all | bytes 3276800 | tf_op jit(solution)/shard_map/all_to_all | solution.py:240
  124.5 7.3 %select_rows.1 = bf16[2048,512]{1,0:T(8,128)(2,1)} custom-call(bf16[32,200,128]{2,1,0:T(8,128)(2,1)} %all_to_all.10.refs_0_), custom_call_target="tpu_custom_call" | custom-call | tf_op jit(solution)/shard_map/select_rows/pallas_call | solution.py:130
  131.8 6.1 %all-to-all-start.1 = ((bf16[32,64,512]{2,1,0:T(8,128)(2,1)}), bf16[32,64,512]{2,1,0:T(8,128)(2,1)S(1)}, u32[]{:S(2)}, u32[]{:S(2)}) async-start(bf16[32,64,512]{2,1,0:T(8,128)(2,1)} %bitcast.16), calls=%async_computation.1 | async-start | bytes 4194304 | tf_op jit(solution)/shard_map/all_to_all | solution.py:243
  137.9 0.8 dynamic_slice.6
  138.7 1.5 fusion
  140.2 10.9 %psum.7 = f32[1024]{0:T(1024)S(1)} all-reduce(f32[1024]{0:T(1024)S(1)} %fusion), channel_id=1, replica_groups=mesh['grp'=2,'st'=32,'tp'=4] {'tp'}, use_global_device_ids=true, to_apply=%region_1.0 | all-reduce | flops 1024 | bytes 8192 | tf_op jit(solution)/shard_map/psum | solution.py:248
  151.1 2.5 fusion.2
  153.7 2.9 %convert.1 = f32[4,256,512]{2,1,0:T(8,128)} convert(bf16[4,256,512]{2,1,0:T(8,128)(2,1)} %bitcast.14) | non-fusion elementwise | flops 524288 | bytes 3145728 | tf_op jit(solution)/shard_map/reshape | solution.py:256
  156.6 1.7 gather_fusion
  158.3 2.7 add_select_fusion.3
  161.8 0.9 copy-done.2
  162.7 0.6 fusion.5
  163.7 2.1 convolution_multiply_fusion.refs_1_
  165.8 41.9 %all-gather.2.cloned.1.call-done = bf16[1024,2048]{1,0:T(8,128)(2,1)} async-done(((bf16[1024,512]{1,0:T(8,128)(2,1)}), bf16[1024,2048]{1,0:T(8,128)(2,1)}) %all-gather.2.cloned.1.call-update) | async-done | bytes 4194320 | tf_op jit(solution)/shard_map/all_gather | solution.py:252
  207.7 4.4 %fusion.8.refs_1_ = f32[1024,2]{1,0:T(8,128)} fusion(bf16[1024,2048]{1,0:T(8,128)(2,1)} %all-gather.2.cloned.1.call-done, bf16[2048,8]{0,1:T(8,128)(2,1)} %param.18, s32[]{:T(128)S(6)} %select_n.40), kind=kOutput, calls=%fused_computation.22 | convolution fusion | flops 8394752 | bytes 4210692 | tf_op jit(solution)/shard_map/dot_general | solution.py:277
  212.1 2.0 convolution_convert_fusion.refs_0_
  214.1 23.0 %all-to-all-done.1.refs_2_ = bf16[32,64,512]{2,1,0:T(8,128)(2,1)S(1)} async-done(((bf16[32,64,512]{2,1,0:T(8,128)(2,1)}), bf16[32,64,512]{2,1,0:T(8,128)(2,1)S(1)}, u32[]{:S(2)}, u32[]{:S(2)}) %all-to-all-start.1) | async-done | bytes 2097184 | tf_op jit(solution)/shard_map/all_to_all | solution.py:243
  237.1 1.3 copy-done.1
  238.5 3.8 %attend.2.refs_2_ = bf16[512,256]{1,0:T(8,128)(2,1)} custom-call(bf16[1024,256]{1,0:T(8,128)(2,1)} %convolution_convert_fusion.refs_0_, f32[1024,2]{1,0:T(8,128)} %fusion.8.refs_1_, bf16[32,64,512]{2,1,0:T(8,128)(2,1)} %copy-done.1), custom_call_target="tpu_custom_call" | custom-call | tf_op jit(solution)/shard_map/attend/pallas_call | solution.py:170
  242.3 1.6 collective-permute-start
  243.9 3.8 %attend.3.refs_6_ = bf16[512,256]{1,0:T(8,128)(2,1)} custom-call(bf16[1024,256]{1,0:T(8,128)(2,1)} %convolution_convert_fusion.refs_0_, f32[1024,2]{1,0:T(8,128)} %fusion.8.refs_1_, bf16[32,64,512]{2,1,0:T(8,128)(2,1)} %copy-done.1), custom_call_target="tpu_custom_call" | custom-call | tf_op jit(solution)/shard_map/attend/pallas_call | solution.py:170
  247.8 1.6 collective-permute-start.4
  249.4 1.9 collective-permute-start.1
  251.8 5.3 %collective-permute-done.4.refs_8_ = bf16[512,256]{1,0:T(8,128)(2,1)S(1)} collective-permute-done((bf16[512,256]{1,0:T(8,128)(2,1)}, bf16[512,256]{1,0:T(8,128)(2,1)S(1)}, u32[]{:S(2)}, u32[]{:S(2)}) %collective-permute-start.4) | collective-permute-done | bytes 262176 | tf_op jit(solution)/shard_map/ppermute | solution.py:293
  257.2 2.8 %collective-permute-start.5 = (bf16[512,256]{1,0:T(8,128)(2,1)S(1)}, bf16[512,256]{1,0:T(8,128)(2,1)S(1)}, u32[]{:S(2)}, u32[]{:S(2)}) collective-permute-start(bf16[512,256]{1,0:T(8,128)(2,1)S(1)} %collective-permute-done.4.refs_8_), channel_id=1, source_target_pairs={{0,3},{1,0},{2,1},{3,2},{4,7},{5,4},{6,5},{7,6},{8,11},{9,8},{10,9... | collective-permute-start | bytes 786440 | tf_op jit(solution)/shard_map/ppermute | solution.py:295
  260.0 1.6 collective-permute-done.1.refs_4_
  261.6 1.4 collective-permute-done.2.refs_5_
  263.0 1.4 collective-permute-done.5.refs_9_
  264.4 0.7 copy-done.10
  265.1 5.3 %finish.1 = bf16[1024,512]{1,0:T(8,128)(2,1)} custom-call(bf16[4,256,512]{2,1,0:T(8,128)(2,1)} %gather_fusion, f32[1024,512]{1,0:T(8,128)} %convolution_multiply_fusion.refs_1_, bf16[512,256]{1,0:T(8,128)(2,1)} %attend.2.refs_2_, bf16[512,256]{1,0:T(8,128)(2,1)} %copy-done.5, bf16[512,256]{1,0:T(8,128)(2,1)} %copy-done.7, bf16[512,256]{1,0:T(8,128)(2,1)} %copy-done.9, ...), custom_call_target="tpu_custom_call" | custom-call | tf_op jit(solution)/shard_map/finish/pallas_call | solution.py:205
  (39 shorter events, 1.9 us)
Async XLA Ops:
  6.5 150.1 %copy-start = (bf16[1024,512]{1,0:T(8,128)(2,1)S(1)}, bf16[1024,512]{1,0:T(8,128)(2,1)}, u32[]{:S(2)}) copy-start(bf16[1024,512]{1,0:T(8,128)(2,1)} %param.21) | copy-start | bytes 3145732
  131.8 105.3 %all-to-all-start.1 = ((bf16[32,64,512]{2,1,0:T(8,128)(2,1)}), bf16[32,64,512]{2,1,0:T(8,128)(2,1)S(1)}, u32[]{:S(2)}, u32[]{:S(2)}) async-start(bf16[32,64,512]{2,1,0:T(8,128)(2,1)} %bitcast.16), calls=%async_computation.1 | async-start | bytes 4194304 | tf_op jit(solution)/shard_map/all_to_all | solution.py:243
  137.9 69.8 %all-gather.2.cloned.1.call-start = ((), (), s32[]{:S(2)}) async-start(), calls=%async_computation.2 | async-start | bytes 5242880 | tf_op jit(solution)/shard_map/all_gather | solution.py:252
  153.6 2.9 %copy-start.14 = (s32[4]{0:T(128)S(1)}, s32[4]{0:T(128)}, u32[]{:S(2)}) copy-start(s32[4]{0:T(128)} %constant.44.clone) | copy-start | bytes 52
  161.4 1.2 copy-start.2
  162.7 1.0 copy-start.4
  162.7 1.0 copy-start.11
  207.7 4.4 %copy-start.12 = (bf16[1024,2048]{1,0:T(8,128)(2,1)S(1)}, bf16[1024,2048]{1,0:T(8,128)(2,1)}, u32[]{:S(2)}) copy-start(bf16[1024,2048]{1,0:T(8,128)(2,1)} %all-gather.2.cloned.1.call-done) | copy-start | bytes 12582916
  207.7 4.4 %copy-start.13 = (bf16[2048,256]{1,0:T(8,128)(2,1)S(1)}, bf16[2048,256]{1,0:T(8,128)(2,1)}, u32[]{:S(2)}) copy-start(bf16[2048,256]{1,0:T(8,128)(2,1)} %param.17) | copy-start | bytes 3145732
  237.1 1.3 copy-start.1
  242.3 7.1 %copy-start.3 = (bf16[512,256]{1,0:T(8,128)(2,1)S(1)}, bf16[512,256]{1,0:T(8,128)(2,1)}, u32[]{:S(2)}) copy-start(bf16[512,256]{1,0:T(8,128)(2,1)} %attend.2.refs_2_) | copy-start | bytes 786436
  242.3 9.1 %collective-permute-start = (bf16[512,256]{1,0:T(8,128)(2,1)}, bf16[512,256]{1,0:T(8,128)(2,1)S(1)}, u32[]{:S(2)}, u32[]{:S(2)}) collective-permute-start(bf16[512,256]{1,0:T(8,128)(2,1)} %attend.2.refs_2_), channel_id=1, source_target_pairs={{0,1},{1,2},{2,3},{3,0},{4,5},{5,6},{6,7},{7,4},{8,9},{9,10},{10,1... | collective-permute-start | bytes 786440 | tf_op jit(solution)/shard_map/ppermute | solution.py:289
  247.8 9.4 %collective-permute-start.4 = (bf16[512,256]{1,0:T(8,128)(2,1)}, bf16[512,256]{1,0:T(8,128)(2,1)S(1)}, u32[]{:S(2)}, u32[]{:S(2)}) collective-permute-start(bf16[512,256]{1,0:T(8,128)(2,1)} %attend.3.refs_6_), channel_id=1, source_target_pairs={{0,3},{1,0},{2,1},{3,2},{4,7},{5,4},{6,5},{7,6},{8,11},{9,8},{10,9... | collective-permute-start | bytes 786440 | tf_op jit(solution)/shard_map/ppermute | solution.py:293
  249.4 12.2 %collective-permute-start.1 = (bf16[512,256]{1,0:T(8,128)(2,1)S(1)}, bf16[512,256]{1,0:T(8,128)(2,1)S(1)}, u32[]{:S(2)}, u32[]{:S(2)}) collective-permute-start(bf16[512,256]{1,0:T(8,128)(2,1)S(1)} %copy-done.3), channel_id=1, source_target_pairs={{0,3},{1,0},{2,1},{3,2},{4,7},{5,4},{6,5},{7,6},{8,11},{9,8},{10,9... | collective-permute-start | bytes 786440 | tf_op jit(solution)/shard_map/ppermute | solution.py:290
  251.3 10.3 %collective-permute-start.3 = (bf16[512,256]{1,0:T(8,128)(2,1)}, bf16[512,256]{1,0:T(8,128)(2,1)S(1)}, u32[]{:S(2)}, u32[]{:S(2)}) collective-permute-start(bf16[512,256]{1,0:T(8,128)(2,1)} %attend.3.refs_6_), channel_id=1, source_target_pairs={{0,1},{1,2},{2,3},{3,0},{4,5},{5,6},{6,7},{7,4},{8,9},{9,10},{10,1... | collective-permute-start | bytes 786440 | tf_op jit(solution)/shard_map/ppermute | solution.py:292
  251.4 13.0 %copy-start.5 = (bf16[512,256]{1,0:T(8,128)(2,1)}, bf16[512,256]{1,0:T(8,128)(2,1)S(1)}, u32[]{:S(2)}) copy-start(bf16[512,256]{1,0:T(8,128)(2,1)S(1)} %collective-permute-done.refs_3_) | copy-start | bytes 786436
  251.4 11.6 %collective-permute-start.2 = (bf16[512,256]{1,0:T(8,128)(2,1)S(1)}, bf16[512,256]{1,0:T(8,128)(2,1)S(1)}, u32[]{:S(2)}, u32[]{:S(2)}) collective-permute-start(bf16[512,256]{1,0:T(8,128)(2,1)S(1)} %collective-permute-done.refs_3_), channel_id=1, source_target_pairs={{0,1},{1,2},{2,3},{3,0},{4,5},{5,6},{6,7},{7,4},{8,9},{9,10},{10,1... | collective-permute-start | bytes 786440 | tf_op jit(solution)/shard_map/ppermute | solution.py:294
  257.2 7.2 %copy-start.6 = (bf16[512,256]{1,0:T(8,128)(2,1)}, bf16[512,256]{1,0:T(8,128)(2,1)S(1)}, u32[]{:S(2)}) copy-start(bf16[512,256]{1,0:T(8,128)(2,1)S(1)} %collective-permute-done.4.refs_8_) | copy-start | bytes 786436
  257.2 7.2 %collective-permute-start.5 = (bf16[512,256]{1,0:T(8,128)(2,1)S(1)}, bf16[512,256]{1,0:T(8,128)(2,1)S(1)}, u32[]{:S(2)}, u32[]{:S(2)}) collective-permute-start(bf16[512,256]{1,0:T(8,128)(2,1)S(1)} %collective-permute-done.4.refs_8_), channel_id=1, source_target_pairs={{0,3},{1,0},{2,1},{3,2},{4,7},{5,4},{6,5},{7,6},{8,11},{9,8},{10,9... | collective-permute-start | bytes 786440 | tf_op jit(solution)/shard_map/ppermute | solution.py:295
  261.6 2.8 %copy-start.7 = (bf16[512,256]{1,0:T(8,128)(2,1)}, bf16[512,256]{1,0:T(8,128)(2,1)S(1)}, u32[]{:S(2)}) copy-start(bf16[512,256]{1,0:T(8,128)(2,1)S(1)} %collective-permute-done.1.refs_4_) | copy-start | bytes 786436
  261.6 2.8 %copy-start.8 = (bf16[512,256]{1,0:T(8,128)(2,1)}, bf16[512,256]{1,0:T(8,128)(2,1)S(1)}, u32[]{:S(2)}) copy-start(bf16[512,256]{1,0:T(8,128)(2,1)S(1)} %collective-permute-done.3.refs_7_) | copy-start | bytes 786436
  263.0 1.4 copy-start.9
  264.4 0.7 copy-start.10
Sparse Core Ops, SparseCore 0:
  153.8 53.8 all-gather.1

commit v4 on v3

--- a/solution.py
+++ b/solution.py
@@ -41,11 +41,11 @@
         lane = lax.broadcasted_iota(jnp.int32, (TILE, LANES), 1)
         share = lax.shift_right_logical(line, 2)
         part_of = line - share * NPB
-        blocks = ids_ref.shape[0]
+        blocks = ids_ref.shape[1]
         tile = jnp.zeros((TILE, LANES), jnp.int32)
         for block in range(blocks):
             for part in range(NPB):
-                name = ids_ref[block, part]
+                name = ids_ref[part, block]
                 owner = lax.div(name, jnp.int32(passages))
                 inside = name - owner * passages
                 here = part_of == part
@@ -138,14 +138,13 @@
     )(held)
 
 
-def attend_kernel(half, query_ref, gate_ref, table_ref, out_ref):
+def attend_kernel(query_ref, gate_ref, table_ref, out_ref):
     holders, _, both = table_ref.shape
     width = query_ref.shape[1]
     rows = out_ref.shape[0]
     for block in range(rows // BLK):
-        place = half * rows // BLK + block
-        mine = slice(place * BLK, (place + 1) * BLK)
-        table = table_ref[:, place * TILE : (place + 1) * TILE, :].astype(jnp.float32)
+        mine = slice(block * BLK, (block + 1) * BLK)
+        table = table_ref[:, block * TILE : (block + 1) * TILE, :].astype(jnp.float32)
         table = table.reshape(holders * TILE, both).astype(jnp.bfloat16)
         for head in range(width // HD):
             cols = slice(head * HD, (head + 1) * HD)
@@ -160,56 +159,92 @@
             total = jnp.sum(weights, axis=-1, keepdims=True)
             probabilities = (weights * (1.0 / total)).astype(jnp.bfloat16)
             attended = jnp.dot(probabilities, table[:, late], preferred_element_type=jnp.float32)
-            out_ref[block * BLK : (block + 1) * BLK, cols] = (
-                attended * gate_ref[mine, head : head + 1]
-            ).astype(jnp.bfloat16)
+            out_ref[mine, cols] = (attended * gate_ref[mine, head : head + 1]).astype(jnp.bfloat16)
 
 
 def attend(queries, gates, table, half):
     rows, width = queries.shape
-    return pl.pallas_call(
-        lambda *refs: attend_kernel(half, *refs),
-        in_specs=[whole, whole, whole],
-        out_specs=whole,
-        out_shape=jax.ShapeDtypeStruct((rows // 2, width), jnp.bfloat16),
+    rows = rows // 2
+    holders, slots, both = table.shape
+    return pl.pallas_call(
+        attend_kernel,
+        grid=(1,),
+        in_specs=[
+            pl.BlockSpec((rows, width), lambda i: (half, 0)),
+            pl.BlockSpec((rows, gates.shape[1]), lambda i: (half, 0)),
+            pl.BlockSpec((holders, slots // 2, both), lambda i: (0, half, 0)),
+        ],
+        out_specs=pl.BlockSpec((rows, width), lambda i: (0, 0)),
+        out_shape=jax.ShapeDtypeStruct((rows, width), jnp.bfloat16),
         name="attend",
     )(queries, gates, table)
 
 
-def finish_kernel(halves, weight_ref, base_ref, *refs):
+def add_products_kernel(weight_ref, base_ref, *refs):
     out_ref = refs[-1]
-    pieces = refs[:-1]
-    count = len(pieces) // halves
+    total = base_ref[...]
+    for k, piece_ref in enumerate(refs[:-1]):
+        total = total + jnp.dot(piece_ref[...], weight_ref[k], preferred_element_type=jnp.float32)
+    out_ref[...] = total
+
+
+def add_products(base, half, pieces, weights):
+    rows, narrow = pieces[0].shape
+    width = base.shape[1]
+    steps = rows // OUT_ROWS
+    return pl.pallas_call(
+        add_products_kernel,
+        grid=(steps,),
+        in_specs=[
+            pl.BlockSpec((len(pieces), narrow, width), lambda i: (0, 0, 0)),
+            pl.BlockSpec((OUT_ROWS, width), lambda i: (half * steps + i, 0)),
+        ]
+        + [pl.BlockSpec((OUT_ROWS, narrow), lambda i: (i, 0))] * len(pieces),
+        out_specs=pl.BlockSpec((OUT_ROWS, width), lambda i: (i, 0)),
+        out_shape=jax.ShapeDtypeStruct((rows, width), jnp.float32),
+        name="add_products",
+    )(weights, base, *pieces)
+
+
+def finish_kernel(weight_ref, low_base, low_piece, high_base, high_piece, out_ref):
     step = pl.program_id(0)
-    each = pl.num_programs(0) // halves
-    rows = out_ref.shape[0]
-    for half in range(halves):
-
-        @pl.when(step // each == half)
+    half = pl.num_programs(0) // 2
+    for place, base_ref, piece_ref in ((0, low_base, low_piece), (1, high_base, high_piece)):
+
+        @pl.when(step // half == place)
         def _():
-            total = base_ref[pl.ds(pl.multiple_of(step * rows, rows), rows), :]
-            mine = pl.ds(pl.multiple_of((step - half * each) * rows, rows), rows)
-            for k in range(count):
-                total = total + jnp.dot(
-                    pieces[half * count + k][mine, :],
-                    weight_ref[k],
-                    preferred_element_type=jnp.float32,
-                )
+            total = base_ref[...] + jnp.dot(
+                piece_ref[...], weight_ref[0], preferred_element_type=jnp.float32
+            )
             out_ref[...] = total.astype(out_ref.dtype)
 
 
-def finish(base, sides, weights):
-    rows, width = base.shape
-    halves = len(sides)
-    pieces = [piece for side in sides for piece in side]
-    return pl.pallas_call(
-        lambda *refs: finish_kernel(halves, *refs),
-        grid=(rows // OUT_ROWS,),
-        in_specs=[whole] * (2 + len(pieces)),
+def finish(weights, low_base, low_piece, high_base, high_piece):
+    rows, width = low_base.shape
+    narrow = low_piece.shape[1]
+    steps = rows // OUT_ROWS
+    last = weights.shape[0] - 1
+
+    def low(i):
+        return jnp.minimum(i, steps - 1), 0
+
+    def high(i):
+        return jnp.maximum(i - steps, 0), 0
+
+    return pl.pallas_call(
+        finish_kernel,
+        grid=(2 * steps,),
+        in_specs=[
+            pl.BlockSpec((1, narrow, width), lambda i: (last, 0, 0)),
+            pl.BlockSpec((OUT_ROWS, width), low),
+            pl.BlockSpec((OUT_ROWS, narrow), low),
+            pl.BlockSpec((OUT_ROWS, width), high),
+            pl.BlockSpec((OUT_ROWS, narrow), high),
+        ],
         out_specs=pl.BlockSpec((OUT_ROWS, width), lambda i: (i, 0)),
-        out_shape=jax.ShapeDtypeStruct((rows, width), jnp.bfloat16),
+        out_shape=jax.ShapeDtypeStruct((2 * rows, width), jnp.bfloat16),
         name="finish",
-    )(weights, base, *pieces)
+    )(weights, low_base, low_piece, high_base, high_piece)
 
 
 def per_device(
@@ -235,7 +270,7 @@
     passages = passage_store.shape[0]
     shares = PLEN // st_count
     spread = spread_store(
-        passage_ids, passage_store, passage_gain, key_weight, value_weight, st_count
+        passage_ids.T, passage_store, passage_gain, key_weight, value_weight, st_count
     )
     held = lax.all_to_all(spread, "st", split_axis=0, concat_axis=0, tiled=True)
     width_both = key_weight.shape[1] + value_weight.shape[1]
@@ -249,7 +284,16 @@
     inverse = lax.rsqrt(square_sums / full_width + epsilon)
     gain_local = lax.dynamic_slice_in_dim(norm_gain, head_index * width_local, width_local)
     normed = (wide_tokens * inverse[:, None] * gain_local[None, :]).astype(jnp.bfloat16)
-    columns = lax.all_gather(normed, "tp", axis=1, tiled=True)
+    up = [(i, (i + 1) % tp_count) for i in range(tp_count)]
+    down = [(i, (i - 1) % tp_count) for i in range(tp_count)]
+    half = tok_rows // 2
+    turned = (head_index + jnp.array([0, tp_count - 1, 1, 2], dtype=jnp.int32)) % tp_count
+    before = lax.ppermute(normed, "tp", up)
+    after = lax.ppermute(normed, "tp", down)
+    far_low = lax.ppermute(before[:half], "tp", up)
+    far_high = lax.ppermute(after[half:], "tp", down)
+    far = jnp.concatenate([far_low, far_high], axis=0)
+    columns = jnp.concatenate([normed, before, after, far], axis=1)
 
     sequences = tok_rows // SEQ_LEN
     window = jnp.left_shift(jnp.int32(2), head_index)
@@ -270,21 +314,25 @@
         jnp.dot(pooled, pool_weight[0], preferred_element_type=jnp.float32) * pool_scale[None, :]
     )
 
+    def turn(weight):
+        pieces = weight.reshape(tp_count, weight.shape[0] // tp_count, weight.shape[1])
+        return jnp.take(pieces, turned, axis=0, mode="clip")
+
     gate_columns = lax.dynamic_slice_in_dim(
         gate_weight, head_index * local_heads, local_heads, axis=1
     )
-    query_sum = jnp.dot(columns, query_weight, preferred_element_type=jnp.float32)
-    gate_sum = jnp.dot(columns, gate_columns, preferred_element_type=jnp.float32)
+    query_sum = jnp.dot(
+        columns, turn(query_weight).reshape(query_weight.shape), preferred_element_type=jnp.float32
+    )
+    gate_sum = jnp.dot(
+        columns, turn(gate_columns).reshape(gate_columns.shape), preferred_element_type=jnp.float32
+    )
     queries = query_sum.astype(jnp.bfloat16)
     gating = jax.nn.sigmoid(gate_sum)
 
-    rows_of = out_weight.reshape(tp_count, local_heads * HD, width_local)
-    turned = (head_index + jnp.array([0, tp_count - 1, 1, 2], dtype=jnp.int32)) % tp_count
-    weights = jnp.take(rows_of, turned, axis=0, mode="clip")
+    weights = turn(out_weight)
     queries, gating, base, weights = lax.optimization_barrier((queries, gating, base, weights))
 
-    up = [(i, (i + 1) % tp_count) for i in range(tp_count)]
-    down = [(i, (i - 1) % tp_count) for i in range(tp_count)]
     low = attend(queries, gating, returned, 0)
     low_before = lax.ppermute(low, "tp", up)
     low_after = lax.ppermute(low, "tp", down)
@@ -293,8 +341,9 @@
     high_after = lax.ppermute(high, "tp", down)
     low_far = lax.ppermute(low_before, "tp", up)
     high_far = lax.ppermute(high_after, "tp", down)
-    sides = ((low, low_before, low_after, low_far), (high, high_before, high_after, high_far))
-    return finish(base, sides, weights)
+    low_base = add_products(base, 0, (low, low_before, low_after), weights)
+    high_base = add_products(base, 1, (high, high_before, high_after), weights)
+    return finish(weights, low_base, low_far, high_base, high_far)
 
 
 def solution(mesh):
@@ -313,6 +362,4 @@
         P(("grp", "st"), None),
     )
     out_specs = P(("grp", "st"), "tp")
-    return jax.shard_map(
-        per_device, mesh=mesh, in_specs=in_specs, out_specs=out_specs, check_vma=False
-    )
+    return jax.shard_map(per_device, mesh=mesh, in_specs=in_specs, out_specs=out_specs, check_vma=False)

time: 283 us -> 271 us (0.958)
  waiting for transfers between devices: 74.7 us -> 52.1 us
  between operations: 13.5 us -> 0.11 us
  matrix products: 8.48 us -> 15.6 us
  local copies, waits for them, and re-layouts: 7.33 us -> 14.4 us
  Pallas kernels: 33.9 us -> 38.2 us
  starting transfers between devices: 14.6 us -> 18.6 us
    all_gather x1 -> x0, waiting for transfers between devices: 41.9 us -> none  [per_device(): columns = lax.all_gather(normed, 'tp', axis=1, tiled=True)]
    ppermute x0 -> x4, waiting for transfers between devices: none -> 16.3 us  [the longest x1 11.2 us: per_device(): after = lax.ppermute(normed, 'tp', down)]
    all_to_all x1, waiting for transfers between devices: 23 us -> 28.8 us  [per_device(): lax.all_to_all(packed.reshape(st_count, -1, width_both), 'st', split_axis...]
    dot_general x2, matrix products: 6.42 us -> 12.2 us  [the longest x1 6.14 us: per_device(): jnp.dot(columns, turn(gate_columns).reshape(gate_columns.shape), preferre...]
    pallas_call x3 -> x5, Pallas kernels: 13 us -> 17.2 us  [the longest x2 6.67 us: attend(): pl.pallas_call(attend_kernel, grid=(1,), in_specs=[pl.BlockSpec((rows, wi...]
    ppermute x0 -> x4, starting transfers between devices: none -> 4.05 us  [the longest x1 2.02 us: per_device(): before = lax.ppermute(normed, 'tp', up)]
    slice x0 -> x2, local copies, waits for them, and re-layouts: none -> 3.74 us  [the longest x1 1.87 us: per_device(): far_high = lax.ppermute(after[half:], 'tp', down)]
    gather x1 -> x3, local copies, waits for them, and re-layouts: 1.69 us -> 5.04 us  [turn(): return jnp.take(pieces, turned, axis=0, mode='clip')]
  transfers between devices with their start and end apart: 8 -> 11, of which waited for: 6 -> 6; matrix products, arithmetic and copies ran while one was open for 8% -> 15% of each run, Pallas kernels for 1% -> 4%
where the time goes in v4:
time: 271 us; the launch traced here: 266 us
  blocking collectives  114 us (42%)
  waiting for transfers between devices  52.1 us (19%)
  Pallas kernels  38.2 us (14%)
  starting transfers between devices  18.6 us (7%)
  matrix products  15.6 us (6%)
  local copies, waits for them, and re-layouts  14.4 us (5%)
  other arithmetic  13.2 us (5%)
    all_to_all x1, blocking collectives, per_device(): held = lax.all_to_all(spread, 'st', split_axis=0, concat_axis=0, tiled=True)  103 us
    all_to_all x1, waiting for transfers between devices, per_device(): lax.all_to_all(packed.reshape(st_count, -1, width_both), 'st', split_axis...  28.8 us
    pallas_call x1, Pallas kernels, spread_store(): pl.pallas_call(spread_kernel, grid_spec=pltpu.PrefetchScalarGridSpec(num_...  13.8 us
    ppermute x1, waiting for transfers between devices, per_device(): after = lax.ppermute(normed, 'tp', down)  11.2 us
    psum x1, blocking collectives, per_device(): square_sums = lax.psum(jnp.sum(wide_tokens * wide_tokens, axis=1), 'tp')  10.9 us
    pallas_call x1, Pallas kernels, select_rows(): pl.pallas_call(lambda *refs: select_kernel(blocks, *refs), grid=(owners /...  7.24 us
    pallas_call x2, Pallas kernels, attend(): pl.pallas_call(attend_kernel, grid=(1,), in_specs=[pl.BlockSpec((rows, wi...  6.67 us
    dot_general x1, matrix products, per_device(): jnp.dot(columns, turn(gate_columns).reshape(gate_columns.shape), preferre...  6.14 us
  transfers between devices with their start and end apart: 11, of which 6 were waited for; matrix products, arithmetic and copies ran while one was open for 15% of the time, Pallas kernels for 4%

profile of v4, /device:TPU:160, one launch (start us, length us, event | category | flops | bytes accessed | tf_op | source)
XLA Modules:
  0.0 266.0 jit_solution(13781144853704537640)
XLA Ops:
  0.0 13.8 %spread_store.1 = bf16[32,200,128]{2,1,0:T(8,128)(2,1)} custom-call(s32[4,8]{1,0:T(4,128)} %bitcast.25, bf16[24,64,2048]{2,1,0:T(8,128)(2,1)} %store_ref.1, f32[1,2048]{1,0:T(1,128)} %bitcast.24, bf16[2048,256]{1,0:T(8,128)(2,1)} %key_ref.1, bf16[2048,256]{1,0:T(8,128)(2,1)} %value_ref.1), custom_call_target="tpu_custom_call" | custom-call | tf_op jit(solution)/shard_map/spread_store/pallas_call | solution.py:80
  13.8 102.9 %all_to_all.10.refs_0_ = bf16[32,200,128]{2,1,0:T(8,128)(2,1)} all-to-all(bf16[32,200,128]{2,1,0:T(8,128)(2,1)} %spread_store.1), channel_id=1, replica_groups=mesh['grp'=2,'st'=32,'tp'=4] {'st'}, dimensions={0} | all-to-all | bytes 3276800 | tf_op jit(solution)/shard_map/all_to_all | solution.py:275
  116.6 7.2 %select_rows.1 = bf16[2048,512]{1,0:T(8,128)(2,1)} custom-call(bf16[32,200,128]{2,1,0:T(8,128)(2,1)} %all_to_all.10.refs_0_), custom_call_target="tpu_custom_call" | custom-call | tf_op jit(solution)/shard_map/select_rows/pallas_call | solution.py:130
  123.9 6.0 %all-to-all-start.1 = ((bf16[32,64,512]{2,1,0:T(8,128)(2,1)}), bf16[32,64,512]{2,1,0:T(8,128)(2,1)S(1)}, u32[]{:S(2)}, u32[]{:S(2)}) async-start(bf16[32,64,512]{2,1,0:T(8,128)(2,1)} %bitcast.20), calls=%async_computation.1 | async-start | bytes 4194304 | tf_op jit(solution)/shard_map/all_to_all | solution.py:278
  130.7 1.5 fusion
  132.2 10.9 %psum.7 = f32[1024]{0:T(1024)S(1)} all-reduce(f32[1024]{0:T(1024)S(1)} %fusion), channel_id=1, replica_groups=mesh['grp'=2,'st'=32,'tp'=4] {'tp'}, use_global_device_ids=true, to_apply=%region_1.0 | all-reduce | flops 1024 | bytes 8192 | tf_op jit(solution)/shard_map/psum | solution.py:283
  143.2 2.5 fusion.2
  145.7 2.0 collective-permute-start
  147.7 2.9 %convert.1 = f32[4,256,512]{2,1,0:T(8,128)} convert(bf16[4,256,512]{2,1,0:T(8,128)(2,1)} %bitcast.5) | non-fusion elementwise | flops 524288 | bytes 3145728 | tf_op jit(solution)/shard_map/reshape | solution.py:300
  150.6 1.6 gather_fusion
  152.3 2.7 %add_select_fusion.3 = f32[4,256,512]{2,1,0:T(8,128)S(1)} fusion(f32[4,256,512]{2,1,0:T(8,128)} %convert.1, pred[]{:T(512)S(6)} %ge.15), kind=kLoop, calls=%fused_computation.7 | loop fusion | flops 1048576 | bytes 4194305 | tf_op jit(solution)/shard_map/jit(_where)/select_n | solution.py:305
  155.7 2.9 %fusion.5 = bf16[4,256,512]{2,1,0:T(8,128)(2,1)} fusion(f32[4,256,512]{2,1,0:T(8,128)S(1)} %add_select_fusion.1, f32[256]{0:T(256)S(1)} %minimum_convert_fusion, pred[]{:T(512)S(6)} %ge.12, bf16[4,256,512]{2,1,0:T(8,128)(2,1)} %bitcast.5), kind=kLoop, calls=%fused_computation.19 | loop fusion | flops 3145728 | bytes 4195329 | tf_op jit(solution)/shard_map/convert_element_type | solution.py:310
  158.6 11.2 %collective-permute-done.1 = bf16[1024,512]{1,0:T(8,128)(2,1)} collective-permute-done((bf16[1024,512]{1,0:T(8,128)(2,1)}, bf16[1024,512]{1,0:T(8,128)(2,1)}, u32[]{:S(2)}, u32[]{:S(2)}) %collective-permute-start.1) | collective-permute-done | bytes 1048608 | tf_op jit(solution)/shard_map/ppermute | solution.py:292
  169.7 1.9 slice.31
  173.1 1.9 slice.30
  176.9 2.8 %gather_fusion.2 = bf16[4,256,512]{2,1,0:T(8,128)(2,1)} fusion(bf16[4,256,512]{2,1,0:T(8,128)(2,1)} %bitcast.22, s32[1024]{0:T(1024)S(1)} %pad_clamp_fusion), kind=kCustom, calls=%fused_computation.2 | custom fusion | bytes 2097168 | tf_op jit(solution)/shard_map/jit(_take)/gather | solution.py:319
  179.7 3.4 %convolution_multiply_fusion.base_ref = f32[1024,512]{1,0:T(8,128)} fusion(bf16[1024,512]{1,0:T(8,128)(2,1)} %bitcast.21, f32[512]{0:T(512)S(1)} %copy-done.10, bf16[1,512,512]{2,1,0:T(8,128)(2,1)} %param.15), kind=kOutput, calls=%fused_computation.20 | convolution fusion | flops 537395200 | bytes 3672064 | tf_op jit(solution)/shard_map/dot_general | solution.py:314
  183.6 4.6 %collective-permute-done.2 = bf16[512,512]{1,0:T(8,128)(2,1)} collective-permute-done((bf16[512,512]{1,0:T(8,128)(2,1)}, bf16[512,512]{1,0:T(8,128)(2,1)}, u32[]{:S(2)}, u32[]{:S(2)}) %collective-permute-start.2) | collective-permute-done | bytes 524320 | tf_op jit(solution)/shard_map/ppermute | solution.py:293
  188.2 6.1 %fusion.8.gate_ref = f32[1024,2]{1,0:T(8,128)} fusion(bf16[2048,2]{0,1:T(2,128)(2,1)S(1)} %bitcast.19, bf16[512,512]{1,0:T(8,128)(2,1)} %collective-permute-done.3, bf16[512,512]{1,0:T(8,128)(2,1)} %collective-permute-done.2, bf16[1024,512]{1,0:T(8,128)(2,1)} %collective-permute-done.1, bf16[1024,512]{1,0:T(8,128)(2,1)} %collective-permute-done, ...), kind=kOutput, calls=%fused_computation.25 | convolution fusion | flops 29366272 | bytes 4210688 | tf_op jit(solution)/shard_map/dot_general | solution.py:327
  194.3 6.0 %convolution_convert_fusion.query_ref = bf16[1024,256]{1,0:T(8,128)(2,1)} fusion(bf16[2048,256]{1,0:T(8,128)(2,1)S(1)} %bitcast.23, bf16[512,512]{1,0:T(8,128)(2,1)} %collective-permute-done.3, bf16[512,512]{1,0:T(8,128)(2,1)} %collective-permute-done.2, bf16[1024,512]{1,0:T(8,128)(2,1)} %collective-permute-done.1, ...), kind=kOutput, calls=%fused_computation.21 | convolution fusion | flops 1094975488 | bytes 5767168 | tf_op jit(solution)/shard_map/dot_general | solution.py:324
  200.4 28.8 %all-to-all-done.1.table_ref = bf16[32,64,512]{2,1,0:T(8,128)(2,1)S(1)} async-done(((bf16[32,64,512]{2,1,0:T(8,128)(2,1)}), bf16[32,64,512]{2,1,0:T(8,128)(2,1)S(1)}, u32[]{:S(2)}, u32[]{:S(2)}) %all-to-all-start.1) | async-done | bytes 2097184 | tf_op jit(solution)/shard_map/all_to_all | solution.py:278
  230.5 3.3 %attend.2.refs_0_ = bf16[512,256]{1,0:T(8,128)(2,1)} custom-call(bf16[1024,256]{1,0:T(8,128)(2,1)} %convolution_convert_fusion.query_ref, f32[1024,2]{1,0:T(8,128)} %fusion.8.gate_ref, bf16[32,64,512]{2,1,0:T(8,128)(2,1)} %copy-done.1), custom_call_target="tpu_custom_call" | custom-call | tf_op jit(solution)/shard_map/attend/pallas_call | solution.py:169
  233.8 1.6 collective-permute-start.4
  235.5 3.4 %attend.3.refs_0_ = bf16[512,256]{1,0:T(8,128)(2,1)} custom-call(bf16[1024,256]{1,0:T(8,128)(2,1)} %convolution_convert_fusion.query_ref, f32[1024,2]{1,0:T(8,128)} %fusion.8.gate_ref, bf16[32,64,512]{2,1,0:T(8,128)(2,1)} %copy-done.1), custom_call_target="tpu_custom_call" | custom-call | tf_op jit(solution)/shard_map/attend/pallas_call | solution.py:169
  238.8 1.6 collective-permute-start.8
  240.5 1.9 collective-permute-start.5
  242.9 5.3 %collective-permute-done.8.refs_2_ = bf16[512,256]{1,0:T(8,128)(2,1)S(1)} collective-permute-done((bf16[512,256]{1,0:T(8,128)(2,1)}, bf16[512,256]{1,0:T(8,128)(2,1)S(1)}, u32[]{:S(2)}, u32[]{:S(2)}) %collective-permute-start.8) | collective-permute-done | bytes 262176 | tf_op jit(solution)/shard_map/ppermute | solution.py:341
  248.2 2.8 %collective-permute-start.9 = (bf16[512,256]{1,0:T(8,128)(2,1)S(1)}, bf16[512,256]{1,0:T(8,128)(2,1)S(1)}, u32[]{:S(2)}, u32[]{:S(2)}) collective-permute-start(bf16[512,256]{1,0:T(8,128)(2,1)S(1)} %collective-permute-done.8.refs_2_), channel_id=1, source_target_pairs={{0,3},{1,0},{2,1},{3,2},{4,7},{5,4},{6,5},{7,6},{8,11},{9,8},{10,9... | collective-permute-start | bytes 786440 | tf_op jit(solution)/shard_map/ppermute | solution.py:343
  251.1 1.6 collective-permute-done.5.refs_2_
  253.4 3.1 %add_products.2.low_base = f32[512,512]{1,0:T(8,128)} custom-call(bf16[4,256,512]{2,1,0:T(8,128)(2,1)} %gather_fusion.2, f32[1024,512]{1,0:T(8,128)} %convolution_multiply_fusion.base_ref, bf16[512,256]{1,0:T(8,128)(2,1)} %attend.2.refs_0_, bf16[512,256]{1,0:T(8,128)(2,1)} %copy-done.4, bf16[512,256]{1,0:T(8,128)(2,1)} %copy-done.9), custom_call_target="tpu_custom_call" | custom-call | tf_op jit(solution)/shard_map/add_products/pallas_call | solution.py:195
  257.1 3.1 %add_products.3.high_base = f32[512,512]{1,0:T(8,128)} custom-call(bf16[4,256,512]{2,1,0:T(8,128)(2,1)} %gather_fusion.2, f32[1024,512]{1,0:T(8,128)} %convolution_multiply_fusion.base_ref, bf16[512,256]{1,0:T(8,128)(2,1)} %attend.3.refs_0_, bf16[512,256]{1,0:T(8,128)(2,1)} %copy-done.7, bf16[512,256]{1,0:T(8,128)(2,1)} %copy-done.5), custom_call_target="tpu_custom_call" | custom-call | tf_op jit(solution)/shard_map/add_products/pallas_call | solution.py:195
  261.6 4.4 %finish.1 = bf16[1024,512]{1,0:T(8,128)(2,1)} custom-call(bf16[4,256,512]{2,1,0:T(8,128)(2,1)} %gather_fusion.2, f32[512,512]{1,0:T(8,128)} %add_products.2.low_base, bf16[512,256]{1,0:T(8,128)(2,1)} %copy-done.6, f32[512,512]{1,0:T(8,128)} %add_products.3.high_base, bf16[512,256]{1,0:T(8,128)(2,1)} %copy-done.8), custom_call_target="tpu_custom_call" | custom-call | tf_op jit(solution)/shard_map/finish/pallas_call | solution.py:234
  (44 shorter events, 10.0 us)
Async XLA Ops:
  0.0 150.6 %copy-start = (bf16[2048,256]{1,0:T(8,128)(2,1)S(1)}, bf16[2048,256]{1,0:T(8,128)(2,1)}, u32[]{:S(2)}) copy-start(bf16[2048,256]{1,0:T(8,128)(2,1)} %param.17) | copy-start | bytes 3145732
  123.9 105.3 %all-to-all-start.1 = ((bf16[32,64,512]{2,1,0:T(8,128)(2,1)}), bf16[32,64,512]{2,1,0:T(8,128)(2,1)S(1)}, u32[]{:S(2)}, u32[]{:S(2)}) async-start(bf16[32,64,512]{2,1,0:T(8,128)(2,1)} %bitcast.20), calls=%async_computation.1 | async-start | bytes 4194304 | tf_op jit(solution)/shard_map/all_to_all | solution.py:278
  145.7 4.9 %copy-start.11 = (s32[4]{0:T(128)S(1)}, s32[4]{0:T(128)}, u32[]{:S(2)}) copy-start(s32[4]{0:T(128)} %constant.44.clone) | copy-start | bytes 52
  145.7 24.1 %collective-permute-start.1 = (bf16[1024,512]{1,0:T(8,128)(2,1)}, bf16[1024,512]{1,0:T(8,128)(2,1)}, u32[]{:S(2)}, u32[]{:S(2)}) collective-permute-start(bf16[1024,512]{1,0:T(8,128)(2,1)} %fusion.2), channel_id=1, source_target_pairs={{0,3},{1,0},{2,1},{3,2},{4,7},{5,4},{6,5},{7,6},{8,11},{9,8},{10,9... | collective-permute-start | bytes 3145736 | tf_op jit(solution)/shard_map/ppermute | solution.py:292
  145.7 27.5 %collective-permute-start = (bf16[1024,512]{1,0:T(8,128)(2,1)}, bf16[1024,512]{1,0:T(8,128)(2,1)}, u32[]{:S(2)}, u32[]{:S(2)}) collective-permute-start(bf16[1024,512]{1,0:T(8,128)(2,1)} %fusion.2), channel_id=1, source_target_pairs={{0,1},{1,2},{2,3},{3,0},{4,5},{5,6},{6,7},{7,4},{8,9},{9,10},{10,1... | collective-permute-start | bytes 3145736 | tf_op jit(solution)/shard_map/ppermute | solution.py:291
  171.6 8.1 %copy-start.10 = (f32[512]{0:T(512)S(1)}, f32[512]{0:T(512)}, u32[]{:S(2)}) copy-start(f32[512]{0:T(512)} %param.16) | copy-start | bytes 6148
  171.6 12.0 %collective-permute-start.3 = (bf16[512,512]{1,0:T(8,128)(2,1)}, bf16[512,512]{1,0:T(8,128)(2,1)}, u32[]{:S(2)}, u32[]{:S(2)}) collective-permute-start(bf16[512,512]{1,0:T(8,128)(2,1)} %slice.31), channel_id=1, source_target_pairs={{0,3},{1,0},{2,1},{3,2},{4,7},{5,4},{6,5},{7,6},{8,11},{9,8},{10,9... | collective-permute-start | bytes 1572872 | tf_op jit(solution)/shard_map/ppermute | solution.py:294
  175.0 13.2 %collective-permute-start.2 = (bf16[512,512]{1,0:T(8,128)(2,1)}, bf16[512,512]{1,0:T(8,128)(2,1)}, u32[]{:S(2)}, u32[]{:S(2)}) collective-permute-start(bf16[512,512]{1,0:T(8,128)(2,1)} %slice.30), channel_id=1, source_target_pairs={{0,1},{1,2},{2,3},{3,0},{4,5},{5,6},{6,7},{7,4},{8,9},{9,10},{10,1... | collective-permute-start | bytes 1572872 | tf_op jit(solution)/shard_map/ppermute | solution.py:293
  188.2 6.1 %copy-start.2 = (bf16[4,512,256]{2,1,0:T(8,128)(2,1)S(1)}, bf16[4,512,256]{2,1,0:T(8,128)(2,1)}, u32[]{:S(2)}) copy-start(bf16[4,512,256]{2,1,0:T(8,128)(2,1)} %gather_fusion) | copy-start | bytes 3145732
  229.2 1.3 copy-start.1
  233.8 6.6 %copy-start.3 = (bf16[512,256]{1,0:T(8,128)(2,1)S(1)}, bf16[512,256]{1,0:T(8,128)(2,1)}, u32[]{:S(2)}) copy-start(bf16[512,256]{1,0:T(8,128)(2,1)} %attend.2.refs_0_) | copy-start | bytes 786436
  233.8 8.6 %collective-permute-start.4 = (bf16[512,256]{1,0:T(8,128)(2,1)}, bf16[512,256]{1,0:T(8,128)(2,1)S(1)}, u32[]{:S(2)}, u32[]{:S(2)}) collective-permute-start(bf16[512,256]{1,0:T(8,128)(2,1)} %attend.2.refs_0_), channel_id=1, source_target_pairs={{0,1},{1,2},{2,3},{3,0},{4,5},{5,6},{6,7},{7,4},{8,9},{9,10},{10,1... | collective-permute-start | bytes 786440 | tf_op jit(solution)/shard_map/ppermute | solution.py:337
  238.8 9.4 %collective-permute-start.8 = (bf16[512,256]{1,0:T(8,128)(2,1)}, bf16[512,256]{1,0:T(8,128)(2,1)S(1)}, u32[]{:S(2)}, u32[]{:S(2)}) collective-permute-start(bf16[512,256]{1,0:T(8,128)(2,1)} %attend.3.refs_0_), channel_id=1, source_target_pairs={{0,3},{1,0},{2,1},{3,2},{4,7},{5,4},{6,5},{7,6},{8,11},{9,8},{10,9... | collective-permute-start | bytes 786440 | tf_op jit(solution)/shard_map/ppermute | solution.py:341
  240.5 12.2 %collective-permute-start.5 = (bf16[512,256]{1,0:T(8,128)(2,1)S(1)}, bf16[512,256]{1,0:T(8,128)(2,1)S(1)}, u32[]{:S(2)}, u32[]{:S(2)}) collective-permute-start(bf16[512,256]{1,0:T(8,128)(2,1)S(1)} %copy-done.3), channel_id=1, source_target_pairs={{0,3},{1,0},{2,1},{3,2},{4,7},{5,4},{6,5},{7,6},{8,11},{9,8},{10,9... | collective-permute-start | bytes 786440 | tf_op jit(solution)/shard_map/ppermute | solution.py:338
  242.4 14.0 %collective-permute-start.7 = (bf16[512,256]{1,0:T(8,128)(2,1)}, bf16[512,256]{1,0:T(8,128)(2,1)S(1)}, u32[]{:S(2)}, u32[]{:S(2)}) collective-permute-start(bf16[512,256]{1,0:T(8,128)(2,1)} %attend.3.refs_0_), channel_id=1, source_target_pairs={{0,1},{1,2},{2,3},{3,0},{4,5},{5,6},{6,7},{7,4},{8,9},{9,10},{10,1... | collective-permute-start | bytes 786440 | tf_op jit(solution)/shard_map/ppermute | solution.py:340
  242.5 10.2 %copy-start.4 = (bf16[512,256]{1,0:T(8,128)(2,1)}, bf16[512,256]{1,0:T(8,128)(2,1)S(1)}, u32[]{:S(2)}) copy-start(bf16[512,256]{1,0:T(8,128)(2,1)S(1)} %collective-permute-done.4.refs_1_) | copy-start | bytes 786436
  242.5 17.7 %collective-permute-start.6 = (bf16[512,256]{1,0:T(8,128)(2,1)S(1)}, bf16[512,256]{1,0:T(8,128)(2,1)S(1)}, u32[]{:S(2)}, u32[]{:S(2)}) collective-permute-start(bf16[512,256]{1,0:T(8,128)(2,1)S(1)} %collective-permute-done.4.refs_1_), channel_id=1, source_target_pairs={{0,1},{1,2},{2,3},{3,0},{4,5},{5,6},{6,7},{7,4},{8,9},{9,10},{10,1... | collective-permute-start | bytes 786440 | tf_op jit(solution)/shard_map/ppermute | solution.py:342
  248.2 8.2 %copy-start.5 = (bf16[512,256]{1,0:T(8,128)(2,1)}, bf16[512,256]{1,0:T(8,128)(2,1)S(1)}, u32[]{:S(2)}) copy-start(bf16[512,256]{1,0:T(8,128)(2,1)S(1)} %collective-permute-done.8.refs_2_) | copy-start | bytes 786436
  248.2 12.0 %collective-permute-start.9 = (bf16[512,256]{1,0:T(8,128)(2,1)S(1)}, bf16[512,256]{1,0:T(8,128)(2,1)S(1)}, u32[]{:S(2)}, u32[]{:S(2)}) collective-permute-start(bf16[512,256]{1,0:T(8,128)(2,1)S(1)} %collective-permute-done.8.refs_2_), channel_id=1, source_target_pairs={{0,3},{1,0},{2,1},{3,2},{4,7},{5,4},{6,5},{7,6},{8,11},{9,8},{10,9... | collective-permute-start | bytes 786440 | tf_op jit(solution)/shard_map/ppermute | solution.py:343
  252.7 0.7 copy-start.9
  256.4 0.7 copy-start.7
  260.2 0.7 copy-start.6
  260.9 0.7 copy-start.8

commit v5 on v4

--- a/solution.py
+++ b/solution.py
@@ -17,59 +17,52 @@
 TILE = 8
 SHARE_ROWS = 16
 SELECT_READERS = 8
-OUT_ROWS = 256
 whole = pl.BlockSpec(memory_space=pltpu.VMEM)
 
 
-def spread_kernel(ids_ref, store_ref, gain_ref, key_ref, value_ref, out_ref, order_ref):
+def spread_kernel(ids_ref, store_ref, gain_ref, key_ref, value_ref, out_ref, order_ref, both_ref):
     step = pl.program_id(0)
     passages, span, width = store_ref.shape
     rows = passages * span
-    holders = out_ref.shape[0]
+    holders, length, _ = out_ref.shape
     groups = holders // span
-    shares = pl.num_programs(0) // groups
-    body = shares * passages
+    half = key_ref.shape[1]
+    chunks = 2 * half // LANES
+    body = (length - TILE) // chunks
 
     @pl.when(step == 0)
     def _():
+        both_ref[:, :half] = key_ref[...]
+        both_ref[:, half:] = value_ref[...]
         spot = lax.broadcasted_iota(jnp.int32, (rows, rows), 0)
-        holder = lax.div(spot, jnp.int32(passages))
+        holder = jnp.floor((spot.astype(jnp.float32) + 0.5) * (1.0 / passages)).astype(jnp.int32)
         wanted = (spot - holder * passages) * span + holder
         other = lax.broadcasted_iota(jnp.int32, (rows, rows), 1)
         order_ref[...] = jnp.where(wanted == other, 1.0, 0.0).astype(jnp.bfloat16)
-        line = lax.broadcasted_iota(jnp.int32, (TILE, LANES), 0)
-        lane = lax.broadcasted_iota(jnp.int32, (TILE, LANES), 1)
-        share = lax.shift_right_logical(line, 2)
-        part_of = line - share * NPB
-        blocks = ids_ref.shape[1]
-        tile = jnp.zeros((TILE, LANES), jnp.int32)
-        for block in range(blocks):
-            for part in range(NPB):
-                name = ids_ref[part, block]
-                owner = lax.div(name, jnp.int32(passages))
-                inside = name - owner * passages
-                here = part_of == part
-                tile = jnp.where(here & (lane == block), owner, tile)
-                tile = jnp.where(here & (lane == blocks + block), inside + share * passages, tile)
+        ids = ids_ref[...]
+        ids = jnp.concatenate([ids] * (TILE // NPB), axis=0)
+        share = lax.broadcasted_iota(jnp.int32, ids.shape, 0) // NPB
+        owner = lax.div(ids, jnp.int32(passages))
+        inside = ids - owner * passages + share * passages
+        spare = jnp.zeros((TILE, LANES - 2 * ids.shape[1]), jnp.int32)
+        tile = jnp.concatenate([owner, inside, spare], axis=1)
         tile = tile.astype(jnp.float32).astype(jnp.bfloat16)
-        out_ref[:, out_ref.shape[1] - TILE :, :] = jnp.broadcast_to(tile, (holders, TILE, LANES))
+        out_ref[:, length - TILE :, :] = jnp.broadcast_to(tile, (holders, TILE, LANES))
 
     wide = store_ref[...].astype(jnp.float32).reshape(rows, width)
     inverse = lax.rsqrt(jnp.mean(wide * wide, axis=-1, keepdims=True) + epsilon)
     scaled = (wide * gain_ref[...]).astype(jnp.bfloat16)
     first = pl.multiple_of((step % groups) * span, span)
     offset = (step // groups) * passages
-    chunks = key_ref.shape[1] // LANES
-    for half, weight_ref in enumerate((key_ref, value_ref)):
-        product = jnp.dot(scaled, weight_ref[...], preferred_element_type=jnp.float32)
-        product = (product * inverse).astype(jnp.bfloat16)
-        turned = jnp.dot(order_ref[...], product, preferred_element_type=jnp.float32)
-        turned = turned.reshape(span, passages, chunks * LANES).astype(jnp.bfloat16)
-        for chunk in range(chunks):
-            start = pl.multiple_of((half * chunks + chunk) * body + offset, TILE)
-            out_ref[pl.ds(first, span), pl.ds(start, passages), :] = turned[
-                :, :, chunk * LANES : (chunk + 1) * LANES
-            ]
+    product = jnp.dot(scaled, both_ref[...], preferred_element_type=jnp.float32)
+    product = (product * inverse).astype(jnp.bfloat16)
+    turned = jnp.dot(order_ref[...], product, preferred_element_type=jnp.float32)
+    turned = turned.reshape(span, passages, chunks * LANES).astype(jnp.bfloat16)
+    for chunk in range(chunks):
+        start = pl.multiple_of(chunk * body + offset, TILE)
+        out_ref[pl.ds(first, span), pl.ds(start, passages), :] = turned[
+            :, :, chunk * LANES : (chunk + 1) * LANES
+        ]
 
 
 def spread_store(ids, store, gain, key_weight, value_weight, holders):
@@ -79,19 +72,20 @@
     per_holder = passages * length // holders * (2 * head_width // LANES) + TILE
     return pl.pallas_call(
         spread_kernel,
-        grid_spec=pltpu.PrefetchScalarGridSpec(
-            num_scalar_prefetch=1,
-            grid=(length // SHARE_ROWS,),
-            in_specs=[
-                pl.BlockSpec((passages, SHARE_ROWS, width), lambda i, s: (0, i, 0)),
-                pl.BlockSpec((1, width), lambda i, s: (0, 0)),
-                pl.BlockSpec((width, head_width), lambda i, s: (0, 0)),
-                pl.BlockSpec((width, head_width), lambda i, s: (0, 0)),
-            ],
-            out_specs=pl.BlockSpec((holders, per_holder, LANES), lambda i, s: (0, 0, 0)),
-            scratch_shapes=[pltpu.VMEM((rows, rows), jnp.bfloat16)],
-        ),
+        grid=(length // SHARE_ROWS,),
+        in_specs=[
+            pl.BlockSpec(ids.shape, lambda i: (0, 0)),
+            pl.BlockSpec((passages, SHARE_ROWS, width), lambda i: (0, i, 0)),
+            pl.BlockSpec((1, width), lambda i: (0, 0)),
+            pl.BlockSpec((width, head_width), lambda i: (0, 0)),
+            pl.BlockSpec((width, head_width), lambda i: (0, 0)),
+        ],
+        out_specs=pl.BlockSpec((holders, per_holder, LANES), lambda i: (0, 0, 0)),
         out_shape=jax.ShapeDtypeStruct((holders, per_holder, LANES), jnp.bfloat16),
+        scratch_shapes=[
+            pltpu.VMEM((rows, rows), jnp.bfloat16),
+            pltpu.VMEM((width, 2 * head_width), jnp.bfloat16),
+        ],
         name="spread_store",
     )(ids, store, gain.reshape(1, width), key_weight, value_weight)
 
@@ -178,73 +172,6 @@
         out_shape=jax.ShapeDtypeStruct((rows, width), jnp.bfloat16),
         name="attend",
     )(queries, gates, table)
-
-
-def add_products_kernel(weight_ref, base_ref, *refs):
-    out_ref = refs[-1]
-    total = base_ref[...]
-    for k, piece_ref in enumerate(refs[:-1]):
-        total = total + jnp.dot(piece_ref[...], weight_ref[k], preferred_element_type=jnp.float32)
-    out_ref[...] = total
-
-
-def add_products(base, half, pieces, weights):
-    rows, narrow = pieces[0].shape
-    width = base.shape[1]
-    steps = rows // OUT_ROWS
-    return pl.pallas_call(
-        add_products_kernel,
-        grid=(steps,),
-        in_specs=[
-            pl.BlockSpec((len(pieces), narrow, width), lambda i: (0, 0, 0)),
-            pl.BlockSpec((OUT_ROWS, width), lambda i: (half * steps + i, 0)),
-        ]
-        + [pl.BlockSpec((OUT_ROWS, narrow), lambda i: (i, 0))] * len(pieces),
-        out_specs=pl.BlockSpec((OUT_ROWS, width), lambda i: (i, 0)),
-        out_shape=jax.ShapeDtypeStruct((rows, width), jnp.float32),
-        name="add_products",
-    )(weights, base, *pieces)
-
-
-def finish_kernel(weight_ref, low_base, low_piece, high_base, high_piece, out_ref):
-    step = pl.program_id(0)
-    half = pl.num_programs(0) // 2
-    for place, base_ref, piece_ref in ((0, low_base, low_piece), (1, high_base, high_piece)):
-
-        @pl.when(step // half == place)
-        def _():
-            total = base_ref[...] + jnp.dot(
-                piece_ref[...], weight_ref[0], preferred_element_type=jnp.float32
-            )
-            out_ref[...] = total.astype(out_ref.dtype)
-
-
-def finish(weights, low_base, low_piece, high_base, high_piece):
-    rows, width = low_base.shape
-    narrow = low_piece.shape[1]
-    steps = rows // OUT_ROWS
-    last = weights.shape[0] - 1
-
-    def low(i):
-        return jnp.minimum(i, steps - 1), 0
-
-    def high(i):
-        return jnp.maximum(i - steps, 0), 0
-
-    return pl.pallas_call(
-        finish_kernel,
-        grid=(2 * steps,),
-        in_specs=[
-            pl.BlockSpec((1, narrow, width), lambda i: (last, 0, 0)),
-            pl.BlockSpec((OUT_ROWS, width), low),
-            pl.BlockSpec((OUT_ROWS, narrow), low),
-            pl.BlockSpec((OUT_ROWS, width), high),
-            pl.BlockSpec((OUT_ROWS, narrow), high),
-        ],
-        out_specs=pl.BlockSpec((OUT_ROWS, width), lambda i: (i, 0)),
-        out_shape=jax.ShapeDtypeStruct((2 * rows, width), jnp.bfloat16),
-        name="finish",
-    )(weights, low_base, low_piece, high_base, high_piece)
 
 
 def per_device(
@@ -341,9 +268,17 @@
     high_after = lax.ppermute(high, "tp", down)
     low_far = lax.ppermute(low_before, "tp", up)
     high_far = lax.ppermute(high_after, "tp", down)
-    low_base = add_products(base, 0, (low, low_before, low_after), weights)
-    high_base = add_products(base, 1, (high, high_before, high_after), weights)
-    return finish(weights, low_base, low_far, high_base, high_far)
+    near = weights[:3].reshape(-1, width_local)
+    low_near = jnp.concatenate([low, low_before, low_after], axis=1)
+    low_base = base[:half] + jnp.dot(low_near, near, preferred_element_type=jnp.float32)
+    high_near = jnp.concatenate([high, high_before, high_after], axis=1)
+    high_base = base[half:] + jnp.dot(high_near, near, preferred_element_type=jnp.float32)
+    low_base, high_base = lax.optimization_barrier((low_base, high_base))
+    far = jnp.concatenate([low_far, high_far], axis=0)
+    base = jnp.concatenate([low_base, high_base], axis=0)
+    return (base + jnp.dot(far, weights[3], preferred_element_type=jnp.float32)).astype(
+        jnp.bfloat16
+    )
 
 
 def solution(mesh):

time: 271 us -> 261 us (0.963)
  the two profiles are of different devices: /device:TPU:160 before, /device:TPU:40 now
where the time goes in v5:
time: 261 us; the launch traced here: 260 us
  blocking collectives  117 us (45%)
  waiting for transfers between devices  55.7 us (21%)
  Pallas kernels  23.1 us (9%)
  starting transfers between devices  19.9 us (8%)
  matrix products  19.4 us (7%)
  other arithmetic  13.1 us (5%)
  local copies, waits for them, and re-layouts  11.8 us (5%)
    all_to_all x1, blocking collectives, per_device(): held = lax.all_to_all(spread, 'st', split_axis=0, concat_axis=0, tiled=True)  106 us
    all_to_all x1, waiting for transfers between devices, per_device(): lax.all_to_all(packed.reshape(st_count, -1, width_both), 'st', split_axis...  32.2 us
    ppermute x1, waiting for transfers between devices, per_device(): before = lax.ppermute(normed, 'tp', up)  11.9 us
    psum x1, blocking collectives, per_device(): square_sums = lax.psum(jnp.sum(wide_tokens * wide_tokens, axis=1), 'tp')  10.9 us
    pallas_call x1, Pallas kernels, spread_store(): pl.pallas_call(spread_kernel, grid=(length // SHARE_ROWS,), in_specs=[pl....  9.17 us
    pallas_call x1, Pallas kernels, select_rows(): pl.pallas_call(lambda *refs: select_kernel(blocks, *refs), grid=(owners /...  7.24 us
    pallas_call x2, Pallas kernels, attend(): pl.pallas_call(attend_kernel, grid=(1,), in_specs=[pl.BlockSpec((rows, wi...  6.67 us
    dot_general x1, matrix products, per_device(): jnp.dot(columns, turn(gate_columns).reshape(gate_columns.shape), preferre...  6.12 us
  transfers between devices with their start and end apart: 11, of which 5 were waited for; matrix products, arithmetic and copies ran while one was open for 16% of the time, Pallas kernels for 1%

profile of v5, /device:TPU:40, one launch (start us, length us, event | category | flops | bytes accessed | tf_op | source)
XLA Modules:
  0.0 259.9 jit_solution(11874026263908329470)
XLA Ops:
  0.0 9.2 %spread_store.1 = bf16[32,200,128]{2,1,0:T(8,128)(2,1)} custom-call(s32[4,8]{1,0:T(4,128)} %bitcast.33, bf16[24,64,2048]{2,1,0:T(8,128)(2,1)} %store_ref.1, f32[1,2048]{1,0:T(1,128)} %bitcast.32, bf16[2048,256]{1,0:T(8,128)(2,1)} %key_ref.1, bf16[2048,256]{1,0:T(8,128)(2,1)} %value_ref.1), custom_call_target="tpu_custom_call" | custom-call | tf_op jit(solution)/shard_map/spread_store/pallas_call | solution.py:73
  9.2 105.8 %all_to_all.10.refs_0_ = bf16[32,200,128]{2,1,0:T(8,128)(2,1)} all-to-all(bf16[32,200,128]{2,1,0:T(8,128)(2,1)} %spread_store.1), channel_id=1, replica_groups=mesh['grp'=2,'st'=32,'tp'=4] {'st'}, dimensions={0} | all-to-all | bytes 3276800 | tf_op jit(solution)/shard_map/all_to_all | solution.py:202
  114.9 7.2 %select_rows.1 = bf16[2048,512]{1,0:T(8,128)(2,1)} custom-call(bf16[32,200,128]{2,1,0:T(8,128)(2,1)} %all_to_all.10.refs_0_), custom_call_target="tpu_custom_call" | custom-call | tf_op jit(solution)/shard_map/select_rows/pallas_call | solution.py:124
  122.2 4.9 %all-to-all-start.1 = ((bf16[32,64,512]{2,1,0:T(8,128)(2,1)}), bf16[32,64,512]{2,1,0:T(8,128)(2,1)S(1)}, u32[]{:S(2)}, u32[]{:S(2)}) async-start(bf16[32,64,512]{2,1,0:T(8,128)(2,1)} %bitcast.26), calls=%async_computation.1 | async-start | bytes 4194304 | tf_op jit(solution)/shard_map/all_to_all | solution.py:205
  127.9 1.5 fusion
  129.4 10.9 %psum.7 = f32[1024]{0:T(1024)S(1)} all-reduce(f32[1024]{0:T(1024)S(1)} %fusion), channel_id=1, replica_groups=mesh['grp'=2,'st'=32,'tp'=4] {'tp'}, use_global_device_ids=true, to_apply=%region_1.0 | all-reduce | flops 1024 | bytes 8192 | tf_op jit(solution)/shard_map/psum | solution.py:210
  140.3 2.5 fusion.2
  142.8 3.2 %collective-permute-start.1 = (bf16[1024,512]{1,0:T(8,128)(2,1)}, bf16[1024,512]{1,0:T(8,128)(2,1)}, u32[]{:S(2)}, u32[]{:S(2)}) collective-permute-start(bf16[1024,512]{1,0:T(8,128)(2,1)} %fusion.2), channel_id=1, source_target_pairs={{0,3},{1,0},{2,1},{3,2},{4,7},{5,4},{6,5},{7,6},{8,11},{9,8},{10,9... | collective-permute-start | bytes 3145736 | tf_op jit(solution)/shard_map/ppermute | solution.py:219
  146.1 2.9 %convert.1 = f32[4,256,512]{2,1,0:T(8,128)} convert(bf16[4,256,512]{2,1,0:T(8,128)(2,1)} %bitcast.5) | non-fusion elementwise | flops 524288 | bytes 3145728 | tf_op jit(solution)/shard_map/reshape | solution.py:227
  148.9 2.7 %add_select_fusion.3 = f32[4,256,512]{2,1,0:T(8,128)S(1)} fusion(f32[4,256,512]{2,1,0:T(8,128)} %convert.1, pred[]{:T(512)S(6)} %ge.15), kind=kLoop, calls=%fused_computation.7 | loop fusion | flops 1048576 | bytes 4194305 | tf_op jit(solution)/shard_map/jit(_where)/select_n | solution.py:232
  152.4 2.8 %fusion.6 = bf16[4,256,512]{2,1,0:T(8,128)(2,1)} fusion(f32[4,256,512]{2,1,0:T(8,128)S(1)} %add_select_fusion.1, f32[256]{0:T(256)S(1)} %minimum_convert_fusion, pred[]{:T(512)S(6)} %ge.12, bf16[4,256,512]{2,1,0:T(8,128)(2,1)} %bitcast.5), kind=kLoop, calls=%fused_computation.21 | loop fusion | flops 3145728 | bytes 4195329 | tf_op jit(solution)/shard_map/convert_element_type | solution.py:237
  155.2 11.9 %collective-permute-done = bf16[1024,512]{1,0:T(8,128)(2,1)} collective-permute-done((bf16[1024,512]{1,0:T(8,128)(2,1)}, bf16[1024,512]{1,0:T(8,128)(2,1)}, u32[]{:S(2)}, u32[]{:S(2)}) %collective-permute-start) | collective-permute-done | bytes 1048608 | tf_op jit(solution)/shard_map/ppermute | solution.py:218
  167.2 1.9 slice.46
  169.1 1.9 slice.47
  170.9 3.2 %collective-permute-start.3 = (bf16[512,512]{1,0:T(8,128)(2,1)}, bf16[512,512]{1,0:T(8,128)(2,1)}, u32[]{:S(2)}, u32[]{:S(2)}) collective-permute-start(bf16[512,512]{1,0:T(8,128)(2,1)} %slice.47), channel_id=1, source_target_pairs={{0,3},{1,0},{2,1},{3,2},{4,7},{5,4},{6,5},{7,6},{8,11},{9,8},{10,9... | collective-permute-start | bytes 1572872 | tf_op jit(solution)/shard_map/ppermute | solution.py:221
  175.5 1.7 gather_fusion
  177.2 2.8 %gather_fusion.2 = bf16[4,256,512]{2,1,0:T(8,128)(2,1)} fusion(bf16[4,256,512]{2,1,0:T(8,128)(2,1)} %bitcast.28, s32[1024]{0:T(1024)S(1)} %pad_clamp_fusion), kind=kCustom, calls=%fused_computation.2 | custom fusion | bytes 2097168 | tf_op jit(solution)/shard_map/jit(_take)/gather | solution.py:246
  180.0 3.4 %convolution_multiply_fusion = f32[1024,512]{1,0:T(8,128)} fusion(bf16[1024,512]{1,0:T(8,128)(2,1)} %bitcast.27, f32[512]{0:T(512)S(1)} %copy-done.7, bf16[1,512,512]{2,1,0:T(8,128)(2,1)} %param.15), kind=kOutput, calls=%fused_computation.22 | convolution fusion | flops 537395200 | bytes 3672064 | tf_op jit(solution)/shard_map/dot_general | solution.py:241
  183.4 6.1 %fusion.9.gate_ref = f32[1024,2]{1,0:T(8,128)} fusion(bf16[2048,2]{0,1:T(2,128)(2,1)S(1)} %bitcast.25, bf16[512,512]{1,0:T(8,128)(2,1)} %collective-permute-done.3, bf16[512,512]{1,0:T(8,128)(2,1)} %collective-permute-done.2, bf16[1024,512]{1,0:T(8,128)(2,1)} %collective-permute-done.1, bf16[1024,512]{1,0:T(8,128)(2,1)} %collective-permute-done, ...), kind=kOutput, calls=%fused_computation.29 | convolution fusion | flops 29366272 | bytes 4210688 | tf_op jit(solution)/shard_map/dot_general | solution.py:254
  189.5 6.0 %convolution_convert_fusion.query_ref = bf16[1024,256]{1,0:T(8,128)(2,1)} fusion(bf16[2048,256]{1,0:T(8,128)(2,1)S(1)} %bitcast.29, bf16[512,512]{1,0:T(8,128)(2,1)} %collective-permute-done.3, bf16[512,512]{1,0:T(8,128)(2,1)} %collective-permute-done.2, bf16[1024,512]{1,0:T(8,128)(2,1)} %collective-permute-done.1, ...), kind=kOutput, calls=%fused_computation.25 | convolution fusion | flops 1094975488 | bytes 5767168 | tf_op jit(solution)/shard_map/dot_general | solution.py:251
  195.6 32.2 %all-to-all-done.1.table_ref = bf16[32,64,512]{2,1,0:T(8,128)(2,1)S(1)} async-done(((bf16[32,64,512]{2,1,0:T(8,128)(2,1)}), bf16[32,64,512]{2,1,0:T(8,128)(2,1)S(1)}, u32[]{:S(2)}, u32[]{:S(2)}) %all-to-all-start.1) | async-done | bytes 2097184 | tf_op jit(solution)/shard_map/all_to_all | solution.py:205
  227.8 1.3 copy-done.1
  229.1 3.3 %attend.3 = bf16[512,256]{1,0:T(8,128)(2,1)} custom-call(bf16[1024,256]{1,0:T(8,128)(2,1)} %convolution_convert_fusion.query_ref, f32[1024,2]{1,0:T(8,128)} %fusion.9.gate_ref, bf16[32,64,512]{2,1,0:T(8,128)(2,1)} %copy-done.1), custom_call_target="tpu_custom_call" | custom-call | tf_op jit(solution)/shard_map/attend/pallas_call | solution.py:163
  232.4 3.1 %collective-permute-start.7 = (bf16[512,256]{1,0:T(8,128)(2,1)}, bf16[512,256]{1,0:T(8,128)(2,1)}, u32[]{:S(2)}, u32[]{:S(2)}) collective-permute-start(bf16[512,256]{1,0:T(8,128)(2,1)} %attend.3), channel_id=1, source_target_pairs={{0,3},{1,0},{2,1},{3,2},{4,7},{5,4},{6,5},{7,6},{8,11},{9,8},{10,9... | collective-permute-start | bytes 786440 | tf_op jit(solution)/shard_map/ppermute | solution.py:268
  235.6 3.3 %attend.2 = bf16[512,256]{1,0:T(8,128)(2,1)} custom-call(bf16[1024,256]{1,0:T(8,128)(2,1)} %convolution_convert_fusion.query_ref, f32[1024,2]{1,0:T(8,128)} %fusion.9.gate_ref, bf16[32,64,512]{2,1,0:T(8,128)(2,1)} %copy-done.1), custom_call_target="tpu_custom_call" | custom-call | tf_op jit(solution)/shard_map/attend/pallas_call | solution.py:163
  239.5 2.9 %collective-permute-start.5 = (bf16[512,256]{1,0:T(8,128)(2,1)}, bf16[512,256]{1,0:T(8,128)(2,1)S(1)}, u32[]{:S(2)}, u32[]{:S(2)}) collective-permute-start(bf16[512,256]{1,0:T(8,128)(2,1)} %attend.2), channel_id=1, source_target_pairs={{0,3},{1,0},{2,1},{3,2},{4,7},{5,4},{6,5},{7,6},{8,11},{9,8},{10,9... | collective-permute-start | bytes 786440 | tf_op jit(solution)/shard_map/ppermute | solution.py:265
  242.4 2.0 collective-permute-start.9
  244.4 5.1 %collective-permute-done.4 = bf16[512,256]{1,0:T(8,128)(2,1)S(1)} collective-permute-done((bf16[512,256]{1,0:T(8,128)(2,1)}, bf16[512,256]{1,0:T(8,128)(2,1)S(1)}, u32[]{:S(2)}, u32[]{:S(2)}) %collective-permute-start.4) | collective-permute-done | bytes 262176 | tf_op jit(solution)/shard_map/ppermute | solution.py:264
  249.5 5.6 %collective-permute-done.6 = bf16[512,256]{1,0:T(8,128)(2,1)S(1)} collective-permute-done((bf16[512,256]{1,0:T(8,128)(2,1)S(1)}, bf16[512,256]{1,0:T(8,128)(2,1)S(1)}, u32[]{:S(2)}, u32[]{:S(2)}) %collective-permute-start.6) | collective-permute-done | bytes 262176 | tf_op jit(solution)/shard_map/ppermute | solution.py:267
  255.1 1.9 convolution_add_fusion
  257.6 0.8 collective-permute-done.8
  258.5 1.4 fusion.5
  (39 shorter events, 4.0 us)
Async XLA Ops:
  0.0 175.5 %copy-start = (bf16[2048,256]{1,0:T(8,128)(2,1)S(1)}, bf16[2048,256]{1,0:T(8,128)(2,1)}, u32[]{:S(2)}) copy-start(bf16[2048,256]{1,0:T(8,128)(2,1)} %param.17) | copy-start | bytes 3145732
  122.2 105.6 %all-to-all-start.1 = ((bf16[32,64,512]{2,1,0:T(8,128)(2,1)}), bf16[32,64,512]{2,1,0:T(8,128)(2,1)S(1)}, u32[]{:S(2)}, u32[]{:S(2)}) async-start(bf16[32,64,512]{2,1,0:T(8,128)(2,1)} %bitcast.26), calls=%async_computation.1 | async-start | bytes 4194304 | tf_op jit(solution)/shard_map/all_to_all | solution.py:205
  142.8 6.1 %copy-start.8 = (s32[4]{0:T(128)S(1)}, s32[4]{0:T(128)}, u32[]{:S(2)}) copy-start(s32[4]{0:T(128)} %constant.44.clone) | copy-start | bytes 52
  142.8 24.4 %collective-permute-start = (bf16[1024,512]{1,0:T(8,128)(2,1)}, bf16[1024,512]{1,0:T(8,128)(2,1)}, u32[]{:S(2)}, u32[]{:S(2)}) collective-permute-start(bf16[1024,512]{1,0:T(8,128)(2,1)} %fusion.2), channel_id=1, source_target_pairs={{0,1},{1,2},{2,3},{3,0},{4,5},{5,6},{6,7},{7,4},{8,9},{9,10},{10,1... | collective-permute-start | bytes 3145736 | tf_op jit(solution)/shard_map/ppermute | solution.py:218
  142.8 26.2 %collective-permute-start.1 = (bf16[1024,512]{1,0:T(8,128)(2,1)}, bf16[1024,512]{1,0:T(8,128)(2,1)}, u32[]{:S(2)}, u32[]{:S(2)}) collective-permute-start(bf16[1024,512]{1,0:T(8,128)(2,1)} %fusion.2), channel_id=1, source_target_pairs={{0,3},{1,0},{2,1},{3,2},{4,7},{5,4},{6,5},{7,6},{8,11},{9,8},{10,9... | collective-permute-start | bytes 3145736 | tf_op jit(solution)/shard_map/ppermute | solution.py:219
  169.0 14.4 %collective-permute-start.2 = (bf16[512,512]{1,0:T(8,128)(2,1)}, bf16[512,512]{1,0:T(8,128)(2,1)}, u32[]{:S(2)}, u32[]{:S(2)}) collective-permute-start(bf16[512,512]{1,0:T(8,128)(2,1)} %slice.46), channel_id=1, source_target_pairs={{0,1},{1,2},{2,3},{3,0},{4,5},{5,6},{6,7},{7,4},{8,9},{9,10},{10,1... | collective-permute-start | bytes 1572872 | tf_op jit(solution)/shard_map/ppermute | solution.py:220
  170.9 12.5 %collective-permute-start.3 = (bf16[512,512]{1,0:T(8,128)(2,1)}, bf16[512,512]{1,0:T(8,128)(2,1)}, u32[]{:S(2)}, u32[]{:S(2)}) collective-permute-start(bf16[512,512]{1,0:T(8,128)(2,1)} %slice.47), channel_id=1, source_target_pairs={{0,3},{1,0},{2,1},{3,2},{4,7},{5,4},{6,5},{7,6},{8,11},{9,8},{10,9... | collective-permute-start | bytes 1572872 | tf_op jit(solution)/shard_map/ppermute | solution.py:221
  175.5 4.5 %copy-start.7 = (f32[512]{0:T(512)S(1)}, f32[512]{0:T(512)}, u32[]{:S(2)}) copy-start(f32[512]{0:T(512)} %param.16) | copy-start | bytes 6148
  183.4 6.1 %copy-start.4 = (bf16[4,512,256]{2,1,0:T(8,128)(2,1)S(1)}, bf16[4,512,256]{2,1,0:T(8,128)(2,1)}, u32[]{:S(2)}) copy-start(bf16[4,512,256]{2,1,0:T(8,128)(2,1)} %gather_fusion) | copy-start | bytes 3145732
  227.8 1.3 copy-start.1
  232.4 6.5 %copy-start.6 = (bf16[512,256]{1,0:T(8,128)(2,1)S(1)}, bf16[512,256]{1,0:T(8,128)(2,1)}, u32[]{:S(2)}) copy-start(bf16[512,256]{1,0:T(8,128)(2,1)} %attend.3) | copy-start | bytes 786436
  232.4 7.0 %copy-start.2 = (bf16[4,256,512]{2,1,0:T(8,128)(2,1)S(1)}, bf16[4,256,512]{2,1,0:T(8,128)(2,1)}, u32[]{:S(2)}) copy-start(bf16[4,256,512]{2,1,0:T(8,128)(2,1)} %gather_fusion.2) | copy-start | bytes 3145732
  232.4 9.9 %collective-permute-start.7 = (bf16[512,256]{1,0:T(8,128)(2,1)}, bf16[512,256]{1,0:T(8,128)(2,1)}, u32[]{:S(2)}, u32[]{:S(2)}) collective-permute-start(bf16[512,256]{1,0:T(8,128)(2,1)} %attend.3), channel_id=1, source_target_pairs={{0,3},{1,0},{2,1},{3,2},{4,7},{5,4},{6,5},{7,6},{8,11},{9,8},{10,9... | collective-permute-start | bytes 786440 | tf_op jit(solution)/shard_map/ppermute | solution.py:268
  238.9 10.6 %collective-permute-start.4 = (bf16[512,256]{1,0:T(8,128)(2,1)}, bf16[512,256]{1,0:T(8,128)(2,1)S(1)}, u32[]{:S(2)}, u32[]{:S(2)}) collective-permute-start(bf16[512,256]{1,0:T(8,128)(2,1)} %attend.2), channel_id=1, source_target_pairs={{0,1},{1,2},{2,3},{3,0},{4,5},{5,6},{6,7},{7,4},{8,9},{9,10},{10,1... | collective-permute-start | bytes 786440 | tf_op jit(solution)/shard_map/ppermute | solution.py:264
  238.9 16.2 %collective-permute-start.6 = (bf16[512,256]{1,0:T(8,128)(2,1)S(1)}, bf16[512,256]{1,0:T(8,128)(2,1)S(1)}, u32[]{:S(2)}, u32[]{:S(2)}) collective-permute-start(bf16[512,256]{1,0:T(8,128)(2,1)S(1)} %copy-done.6), channel_id=1, source_target_pairs={{0,1},{1,2},{2,3},{3,0},{4,5},{5,6},{6,7},{7,4},{8,9},{9,10},{10,1... | collective-permute-start | bytes 786440 | tf_op jit(solution)/shard_map/ppermute | solution.py:267
  239.5 17.6 %copy-start.3 = (f32[1024,512]{1,0:T(8,128)S(1)}, f32[1024,512]{1,0:T(8,128)}, u32[]{:S(2)}) copy-start(f32[1024,512]{1,0:T(8,128)} %convolution_multiply_fusion) | copy-start | bytes 6291460
  239.5 17.6 %copy-start.5 = (bf16[512,256]{1,0:T(8,128)(2,1)S(1)}, bf16[512,256]{1,0:T(8,128)(2,1)}, u32[]{:S(2)}) copy-start(bf16[512,256]{1,0:T(8,128)(2,1)} %attend.2) | copy-start | bytes 786436
  239.5 17.5 %collective-permute-start.5 = (bf16[512,256]{1,0:T(8,128)(2,1)}, bf16[512,256]{1,0:T(8,128)(2,1)S(1)}, u32[]{:S(2)}, u32[]{:S(2)}) collective-permute-start(bf16[512,256]{1,0:T(8,128)(2,1)} %attend.2), channel_id=1, source_target_pairs={{0,3},{1,0},{2,1},{3,2},{4,7},{5,4},{6,5},{7,6},{8,11},{9,8},{10,9... | collective-permute-start | bytes 786440 | tf_op jit(solution)/shard_map/ppermute | solution.py:265
  242.4 15.3 %collective-permute-start.9 = (bf16[512,256]{1,0:T(8,128)(2,1)}, bf16[512,256]{1,0:T(8,128)(2,1)S(1)}, u32[]{:S(2)}, u32[]{:S(2)}) collective-permute-start(bf16[512,256]{1,0:T(8,128)(2,1)} %collective-permute-done.7), channel_id=1, source_target_pairs={{0,3},{1,0},{2,1},{3,2},{4,7},{5,4},{6,5},{7,6},{8,11},{9,8},{10,9... | collective-permute-start | bytes 786440 | tf_op jit(solution)/shard_map/ppermute | solution.py:270
  249.5 9.0 %collective-permute-start.8 = (bf16[512,256]{1,0:T(8,128)(2,1)S(1)}, bf16[512,256]{1,0:T(8,128)(2,1)S(1)}, u32[]{:S(2)}, u32[]{:S(2)}) collective-permute-start(bf16[512,256]{1,0:T(8,128)(2,1)S(1)} %collective-permute-done.4), channel_id=1, source_target_pairs={{0,1},{1,2},{2,3},{3,0},{4,5},{5,6},{6,7},{7,4},{8,9},{9,10},{10,1... | collective-permute-start | bytes 786440 | tf_op jit(solution)/shard_map/ppermute | solution.py:269

commit v6 on v5

--- a/solution.py
+++ b/solution.py
@@ -41,9 +41,8 @@
         order_ref[...] = jnp.where(wanted == other, 1.0, 0.0).astype(jnp.bfloat16)
         ids = ids_ref[...]
         ids = jnp.concatenate([ids] * (TILE // NPB), axis=0)
-        share = lax.broadcasted_iota(jnp.int32, ids.shape, 0) // NPB
         owner = lax.div(ids, jnp.int32(passages))
-        inside = ids - owner * passages + share * passages
+        inside = ids - owner * passages
         spare = jnp.zeros((TILE, LANES - 2 * ids.shape[1]), jnp.int32)
         tile = jnp.concatenate([owner, inside, spare], axis=1)
         tile = tile.astype(jnp.float32).astype(jnp.bfloat16)
@@ -90,70 +89,89 @@
     )(ids, store, gain.reshape(1, width), key_weight, value_weight)
 
 
-def select_kernel(blocks, held_ref, out_ref, table_ref):
+def select_kernel(blocks, shares, held_ref, out_ref, table_ref):
     step = pl.program_id(0)
-    owners = held_ref.shape[0]
-    chunks = table_ref.shape[1] // LANES
-    body = table_ref.shape[0] // owners
+    owners, length, _ = held_ref.shape
+    passages = table_ref.shape[0] // owners
+    width = table_ref.shape[1]
+    chunks = width // shares // LANES
 
     @pl.when(step == 0)
     def _():
         for owner in range(owners):
-            for chunk in range(chunks):
-                table_ref[
-                    owner * body : (owner + 1) * body, chunk * LANES : (chunk + 1) * LANES
-                ] = held_ref[owner, chunk * body : (chunk + 1) * body, :]
+            rows = slice(owner * passages, (owner + 1) * passages)
+            for share in range(shares):
+                for chunk in range(chunks):
+                    source = (chunk * shares + share) * passages
+                    lane = (share * chunks + chunk) * LANES
+                    table_ref[rows, lane : lane + LANES] = held_ref[
+                        owner, source : source + passages, :
+                    ]
 
     spot = lax.broadcasted_iota(jnp.int32, (TILE, table_ref.shape[0]), 1).astype(jnp.float32)
+    early = lax.broadcasted_iota(jnp.int32, (TILE, 1), 0) < NPB
     chosen = []
     for reader in range(SELECT_READERS):
-        tile = held_ref[step * SELECT_READERS + reader, chunks * body :, :].astype(jnp.float32)
-        for block in range(blocks):
-            wanted = tile[:, block : block + 1] * float(body)
-            wanted = wanted + tile[:, blocks + block : blocks + block + 1]
-            chosen.append(jnp.where(spot == wanted, 1.0, 0.0))
+        tile = held_ref[step * SELECT_READERS + reader, length - TILE :, :].astype(jnp.float32)
+        wanted = tile[:, :blocks] * float(passages) + tile[:, blocks : 2 * blocks]
+        for pair in range(0, blocks, 2):
+            mine = jnp.where(early, wanted[:, pair : pair + 1], wanted[:, pair + 1 : pair + 2])
+            chosen.append(jnp.where(spot == mine, 1.0, 0.0))
     chosen = jnp.concatenate(chosen, axis=0).astype(jnp.bfloat16)
     out_ref[...] = jnp.dot(chosen, table_ref[...], preferred_element_type=jnp.float32).astype(
         jnp.bfloat16
     )
 
 
-def select_rows(held, blocks, body, width):
+def select_rows(held, blocks, passages, shares, width):
     owners = held.shape[0]
-    step_rows = SELECT_READERS * blocks * TILE
+    step_rows = SELECT_READERS * blocks * NPB
     return pl.pallas_call(
-        lambda *refs: select_kernel(blocks, *refs),
+        lambda *refs: select_kernel(blocks, shares, *refs),
         grid=(owners // SELECT_READERS,),
         in_specs=[whole],
-        out_specs=pl.BlockSpec((step_rows, width), lambda i: (i, 0)),
-        out_shape=jax.ShapeDtypeStruct((owners * blocks * TILE, width), jnp.bfloat16),
-        scratch_shapes=[pltpu.VMEM((owners * body, width), jnp.bfloat16)],
+        out_specs=pl.BlockSpec((step_rows, shares * width), lambda i: (i, 0)),
+        out_shape=jax.ShapeDtypeStruct((owners * blocks * NPB, shares * width), jnp.bfloat16),
+        scratch_shapes=[pltpu.VMEM((owners * passages, shares * width), jnp.bfloat16)],
         name="select_rows",
     )(held)
 
 
 def attend_kernel(query_ref, gate_ref, table_ref, out_ref):
-    holders, _, both = table_ref.shape
+    holders, slots, _ = table_ref.shape
     width = query_ref.shape[1]
-    rows = out_ref.shape[0]
-    for block in range(rows // BLK):
-        mine = slice(block * BLK, (block + 1) * BLK)
-        table = table_ref[:, block * TILE : (block + 1) * TILE, :].astype(jnp.float32)
-        table = table.reshape(holders * TILE, both).astype(jnp.bfloat16)
-        for head in range(width // HD):
-            cols = slice(head * HD, (head + 1) * HD)
-            late = slice(width + head * HD, width + (head + 1) * HD)
-            scores = lax.dot_general(
-                query_ref[mine, cols],
-                table[:, cols],
-                (((1,), (1,)), ((), ())),
-                preferred_element_type=jnp.float32,
-            ) * HD ** (-0.5)
-            weights = jnp.exp(scores - jnp.max(scores, axis=-1, keepdims=True))
-            total = jnp.sum(weights, axis=-1, keepdims=True)
-            probabilities = (weights * (1.0 / total)).astype(jnp.bfloat16)
-            attended = jnp.dot(probabilities, table[:, late], preferred_element_type=jnp.float32)
-            out_ref[mine, cols] = (attended * gate_ref[mine, head : head + 1]).astype(jnp.bfloat16)
+    both = 2 * width
+    early = lax.broadcasted_iota(jnp.int32, (holders, TILE, both), 1) < NPB
+    for pair in range(slots // TILE):
+        here = slice(pair * TILE, (pair + 1) * TILE)
+        first = table_ref[:, here, :both].astype(jnp.float32)
+        second = table_ref[:, here, both:].astype(jnp.float32)
+        tables = (
+            jnp.where(early, first, pltpu.roll(second, NPB, 1)),
+            jnp.where(early, pltpu.roll(first, NPB, 1), second),
+        )
+        for place, table in enumerate(tables):
+            table = table.reshape(holders * TILE, both).astype(jnp.bfloat16)
+            block = 2 * pair + place
+            mine = slice(block * BLK, (block + 1) * BLK)
+            for head in range(width // HD):
+                cols = slice(head * HD, (head + 1) * HD)
+                late = slice(width + head * HD, width + (head + 1) * HD)
+                scores = lax.dot_general(
+                    query_ref[mine, cols],
+                    table[:, cols],
+                    (((1,), (1,)), ((), ())),
+                    preferred_element_type=jnp.float32,
+                ) * HD ** (-0.5)
+                weights = jnp.exp(scores - jnp.max(scores, axis=-1, keepdims=True))
+                total = jnp.sum(weights, axis=-1, keepdims=True)
+                probabilities = (weights * (1.0 / total)).astype(jnp.bfloat16)
+                attended = jnp.dot(
+                    probabilities, table[:, late], preferred_element_type=jnp.float32
+                )
+                out_ref[mine, cols] = (attended * gate_ref[mine, head : head + 1]).astype(
+                    jnp.bfloat16
+                )
 
 
 def attend(queries, gates, table, half):
@@ -201,9 +219,13 @@
     )
     held = lax.all_to_all(spread, "st", split_axis=0, concat_axis=0, tiled=True)
     width_both = key_weight.shape[1] + value_weight.shape[1]
-    packed = select_rows(held, tok_rows // BLK, shares * passages, width_both)
+    packed = select_rows(held, tok_rows // BLK, passages, shares, width_both)
     returned = lax.all_to_all(
-        packed.reshape(st_count, -1, width_both), "st", split_axis=0, concat_axis=0, tiled=True
+        packed.reshape(st_count, -1, shares * width_both),
+        "st",
+        split_axis=0,
+        concat_axis=0,
+        tiled=True,
     )
 
     wide_tokens = tokens.astype(jnp.float32)
@@ -213,13 +235,12 @@
     normed = (wide_tokens * inverse[:, None] * gain_local[None, :]).astype(jnp.bfloat16)
     up = [(i, (i + 1) % tp_count) for i in range(tp_count)]
     down = [(i, (i - 1) % tp_count) for i in range(tp_count)]
+    across = [(i, (i + 2) % tp_count) for i in range(tp_count)]
     half = tok_rows // 2
     turned = (head_index + jnp.array([0, tp_count - 1, 1, 2], dtype=jnp.int32)) % tp_count
     before = lax.ppermute(normed, "tp", up)
     after = lax.ppermute(normed, "tp", down)
-    far_low = lax.ppermute(before[:half], "tp", up)
-    far_high = lax.ppermute(after[half:], "tp", down)
-    far = jnp.concatenate([far_low, far_high], axis=0)
+    far = lax.ppermute(normed, "tp", across)
     columns = jnp.concatenate([normed, before, after, far], axis=1)
 
     sequences = tok_rows // SEQ_LEN
@@ -266,8 +287,8 @@
     high = attend(queries, gating, returned, 1)
     high_before = lax.ppermute(high, "tp", up)
     high_after = lax.ppermute(high, "tp", down)
-    low_far = lax.ppermute(low_before, "tp", up)
-    high_far = lax.ppermute(high_after, "tp", down)
+    low_far = lax.ppermute(low, "tp", across)
+    high_far = lax.ppermute(high, "tp", across)
     near = weights[:3].reshape(-1, width_local)
     low_near = jnp.concatenate([low, low_before, low_after], axis=1)
     low_base = base[:half] + jnp.dot(low_near, near, preferred_element_type=jnp.float32)

time: 261 us -> 263 us (level)
  the two profiles are of different devices: /device:TPU:40 before, /device:TPU:46 now
where the time goes in v6:
time: 263 us; the launch traced here: 262 us
  blocking collectives  113 us (43%)
  waiting for transfers between devices  71.8 us (27%)
  Pallas kernels  21.7 us (8%)
  starting transfers between devices  17.5 us (7%)
  matrix products  15.4 us (6%)
  other arithmetic  12.2 us (5%)
  local copies, waits for them, and re-layouts  10 us (4%)
    all_to_all x1, blocking collectives, per_device(): held = lax.all_to_all(spread, 'st', split_axis=0, concat_axis=0, tiled=True)  106 us
    all_to_all x1, waiting for transfers between devices, per_device(): lax.all_to_all(packed.reshape(st_count, -1, shares * width_both), 'st', s...  29.8 us
    ppermute x1, waiting for transfers between devices, per_device(): before = lax.ppermute(normed, 'tp', up)  25.5 us
    ppermute x1, waiting for transfers between devices, per_device(): low_after = lax.ppermute(low, 'tp', down)  11.1 us
    pallas_call x1, Pallas kernels, spread_store(): pl.pallas_call(spread_kernel, grid=(length // SHARE_ROWS,), in_specs=[pl....  9.13 us
    psum x1, blocking collectives, per_device(): square_sums = lax.psum(jnp.sum(wide_tokens * wide_tokens, axis=1), 'tp')  7.52 us
    pallas_call x2, Pallas kernels, attend(): pl.pallas_call(attend_kernel, grid=(1,), in_specs=[pl.BlockSpec((rows, wi...  6.87 us
    pallas_call x1, Pallas kernels, select_rows(): pl.pallas_call(lambda *refs: select_kernel(blocks, shares, *refs), grid=(...  5.67 us
  transfers between devices with their start and end apart: 10, of which 5 were waited for; matrix products, arithmetic and copies ran while one was open for 13% of the time, Pallas kernels for 1%

profile of v6, /device:TPU:46, one launch (start us, length us, event | category | flops | bytes accessed | tf_op | source)
XLA Modules:
  0.0 261.9 jit_solution(10342368874126020744)
XLA Ops:
  0.0 9.1 %spread_store.1 = bf16[32,200,128]{2,1,0:T(8,128)(2,1)} custom-call(s32[4,8]{1,0:T(4,128)} %bitcast.33, bf16[24,64,2048]{2,1,0:T(8,128)(2,1)} %store_ref.1, f32[1,2048]{1,0:T(1,128)} %bitcast.32, bf16[2048,256]{1,0:T(8,128)(2,1)} %key_ref.1, bf16[2048,256]{1,0:T(8,128)(2,1)} %value_ref.1), custom_call_target="tpu_custom_call" | custom-call | tf_op jit(solution)/shard_map/spread_store/pallas_call | solution.py:72
  9.1 105.7 %all_to_all.10.refs_0_ = bf16[32,200,128]{2,1,0:T(8,128)(2,1)} all-to-all(bf16[32,200,128]{2,1,0:T(8,128)(2,1)} %spread_store.1), channel_id=1, replica_groups=mesh['grp'=2,'st'=32,'tp'=4] {'st'}, dimensions={0} | all-to-all | bytes 3276800 | tf_op jit(solution)/shard_map/all_to_all | solution.py:220
  114.9 5.7 %select_rows.1 = bf16[1024,1024]{1,0:T(8,128)(2,1)} custom-call(bf16[32,200,128]{2,1,0:T(8,128)(2,1)} %all_to_all.10.refs_0_), custom_call_target="tpu_custom_call" | custom-call | tf_op jit(solution)/shard_map/select_rows/pallas_call | solution.py:129
  120.6 4.9 %all-to-all-start.1 = ((bf16[32,32,1024]{2,1,0:T(8,128)(2,1)}), bf16[32,32,1024]{2,1,0:T(8,128)(2,1)S(1)}, u32[]{:S(2)}, u32[]{:S(2)}) async-start(bf16[32,32,1024]{2,1,0:T(8,128)(2,1)} %bitcast.26), calls=%async_computation.1 | async-start | bytes 4194304 | tf_op jit(solution)/shard_map/all_to_all | solution.py:223
  126.3 1.5 fusion
  127.8 7.5 %psum.7 = f32[1024]{0:T(1024)S(1)} all-reduce(f32[1024]{0:T(1024)S(1)} %fusion), channel_id=1, replica_groups=mesh['grp'=2,'st'=32,'tp'=4] {'tp'}, use_global_device_ids=true, to_apply=%region_1.0 | all-reduce | flops 1024 | bytes 8192 | tf_op jit(solution)/shard_map/psum | solution.py:232
  135.3 2.5 fusion.2
  137.8 3.5 %collective-permute-start = (bf16[1024,512]{1,0:T(8,128)(2,1)}, bf16[1024,512]{1,0:T(8,128)(2,1)}, u32[]{:S(2)}, u32[]{:S(2)}) collective-permute-start(bf16[1024,512]{1,0:T(8,128)(2,1)} %fusion.2), channel_id=1, source_target_pairs={{0,1},{1,2},{2,3},{3,0},{4,5},{5,6},{6,7},{7,4},{8,9},{9,10},{10,1... | collective-permute-start | bytes 3145736 | tf_op jit(solution)/shard_map/ppermute | solution.py:241
  141.3 1.5 collective-permute-start.2
  144.2 1.7 gather_fusion
  145.8 2.8 %convert.1 = f32[4,256,512]{2,1,0:T(8,128)} convert(bf16[4,256,512]{2,1,0:T(8,128)(2,1)} %bitcast.5) | non-fusion elementwise | flops 524288 | bytes 3145728 | tf_op jit(solution)/shard_map/reshape | solution.py:248
  148.7 2.8 %gather_fusion.2 = bf16[4,256,512]{2,1,0:T(8,128)(2,1)} fusion(bf16[4,256,512]{2,1,0:T(8,128)(2,1)} %bitcast.28, s32[1024]{0:T(1024)S(1)} %pad_clamp_fusion), kind=kCustom, calls=%fused_computation.2 | custom fusion | bytes 2097168 | tf_op jit(solution)/shard_map/jit(_take)/gather | solution.py:267
  151.5 2.7 %add_select_fusion.3 = f32[4,256,512]{2,1,0:T(8,128)S(1)} fusion(f32[4,256,512]{2,1,0:T(8,128)} %convert.1, pred[]{:T(512)S(6)} %ge.15), kind=kLoop, calls=%fused_computation.7 | loop fusion | flops 1048576 | bytes 4194305 | tf_op jit(solution)/shard_map/jit(_where)/select_n | solution.py:253
  154.9 1.9 fusion.6
  156.8 2.0 convolution_multiply_fusion
  158.9 25.5 %collective-permute-done = bf16[1024,512]{1,0:T(8,128)(2,1)} collective-permute-done((bf16[1024,512]{1,0:T(8,128)(2,1)}, bf16[1024,512]{1,0:T(8,128)(2,1)}, u32[]{:S(2)}, u32[]{:S(2)}) %collective-permute-start) | collective-permute-done | bytes 1048608 | tf_op jit(solution)/shard_map/ppermute | solution.py:241
  184.4 3.4 %collective-permute-done.1 = bf16[1024,512]{1,0:T(8,128)(2,1)} collective-permute-done((bf16[1024,512]{1,0:T(8,128)(2,1)}, bf16[1024,512]{1,0:T(8,128)(2,1)}, u32[]{:S(2)}, u32[]{:S(2)}) %collective-permute-start.1) | collective-permute-done | bytes 1048608 | tf_op jit(solution)/shard_map/ppermute | solution.py:242
  187.8 4.3 %fusion.9.gate_ref = f32[1024,2]{1,0:T(8,128)} fusion(bf16[2048,2]{0,1:T(2,128)(2,1)S(1)} %bitcast.25, bf16[1024,512]{1,0:T(8,128)(2,1)} %collective-permute-done.2, bf16[1024,512]{1,0:T(8,128)(2,1)} %collective-permute-done.1, bf16[1024,512]{1,0:T(8,128)(2,1)} %collective-permute-done, bf16[1024,512]{1,0:T(8,128)(2,1)} %fusion.2), kind=kOutput, calls=%fused_computation.29 | convolution fusion | flops 25171968 | bytes 4210688 | tf_op jit(solution)/shard_map/dot_general | solution.py:275
  192.1 4.3 %convolution_convert_fusion.query_ref = bf16[1024,256]{1,0:T(8,128)(2,1)} fusion(bf16[2048,256]{1,0:T(8,128)(2,1)S(1)} %bitcast.29, bf16[1024,512]{1,0:T(8,128)(2,1)} %collective-permute-done.2, bf16[1024,512]{1,0:T(8,128)(2,1)} %collective-permute-done.1, bf16[1024,512]{1,0:T(8,128)(2,1)} %collective-permute-done, bf16[1024,512]{1,0:T(8,128)(2,1)} %fusion.2), kind=kOutput, calls=%fused_computation.25 | convolution fusion | flops 1090781184 | bytes 5767168 | tf_op jit(solution)/shard_map/dot_general | solution.py:272
  196.4 29.8 %all-to-all-done.1.table_ref = bf16[32,32,1024]{2,1,0:T(8,128)(2,1)S(1)} async-done(((bf16[32,32,1024]{2,1,0:T(8,128)(2,1)}), bf16[32,32,1024]{2,1,0:T(8,128)(2,1)S(1)}, u32[]{:S(2)}, u32[]{:S(2)}) %all-to-all-start.1) | async-done | bytes 2097184 | tf_op jit(solution)/shard_map/all_to_all | solution.py:223
  226.1 1.3 copy-done.1
  227.5 3.4 %attend.3 = bf16[512,256]{1,0:T(8,128)(2,1)} custom-call(bf16[1024,256]{1,0:T(8,128)(2,1)} %convolution_convert_fusion.query_ref, f32[1024,2]{1,0:T(8,128)} %fusion.9.gate_ref, bf16[32,32,1024]{2,1,0:T(8,128)(2,1)} %copy-done.1), custom_call_target="tpu_custom_call" | custom-call | tf_op jit(solution)/shard_map/attend/pallas_call | solution.py:181
  230.9 2.0 collective-permute-start.6
  232.9 2.1 slice.29
  234.9 3.5 %attend.2 = bf16[512,256]{1,0:T(8,128)(2,1)} custom-call(bf16[1024,256]{1,0:T(8,128)(2,1)} %convolution_convert_fusion.query_ref, f32[1024,2]{1,0:T(8,128)} %fusion.9.gate_ref, bf16[32,32,1024]{2,1,0:T(8,128)(2,1)} %copy-done.1), custom_call_target="tpu_custom_call" | custom-call | tf_op jit(solution)/shard_map/attend/pallas_call | solution.py:181
  238.4 1.3 collective-permute-start.3
  240.5 1.1 collective-permute-start.8
  241.6 2.4 collective-permute-start.7
  244.0 1.9 convolution_add_fusion
  245.9 1.9 collective-permute-done.3
  247.8 11.1 %collective-permute-done.4 = bf16[512,256]{1,0:T(8,128)(2,1)S(1)} collective-permute-done((bf16[512,256]{1,0:T(8,128)(2,1)}, bf16[512,256]{1,0:T(8,128)(2,1)S(1)}, u32[]{:S(2)}, u32[]{:S(2)}) %collective-permute-start.4) | collective-permute-done | bytes 262176 | tf_op jit(solution)/shard_map/ppermute | solution.py:286
  259.5 2.4 fusion.5
  (37 shorter events, 4.3 us)
Async XLA Ops:
  0.0 144.1 %copy-start = (bf16[2048,256]{1,0:T(8,128)(2,1)S(1)}, bf16[2048,256]{1,0:T(8,128)(2,1)}, u32[]{:S(2)}) copy-start(bf16[2048,256]{1,0:T(8,128)(2,1)} %param.17) | copy-start | bytes 3145732
  120.6 105.6 %all-to-all-start.1 = ((bf16[32,32,1024]{2,1,0:T(8,128)(2,1)}), bf16[32,32,1024]{2,1,0:T(8,128)(2,1)S(1)}, u32[]{:S(2)}, u32[]{:S(2)}) async-start(bf16[32,32,1024]{2,1,0:T(8,128)(2,1)} %bitcast.26), calls=%async_computation.1 | async-start | bytes 4194304 | tf_op jit(solution)/shard_map/all_to_all | solution.py:223
  125.5 17.3 %copy-start.9 = (s32[4]{0:T(128)S(1)}, s32[4]{0:T(128)}, u32[]{:S(2)}) copy-start(s32[4]{0:T(128)} %constant.44.clone) | copy-start | bytes 52
  137.8 46.6 %collective-permute-start = (bf16[1024,512]{1,0:T(8,128)(2,1)}, bf16[1024,512]{1,0:T(8,128)(2,1)}, u32[]{:S(2)}, u32[]{:S(2)}) collective-permute-start(bf16[1024,512]{1,0:T(8,128)(2,1)} %fusion.2), channel_id=1, source_target_pairs={{0,1},{1,2},{2,3},{3,0},{4,5},{5,6},{6,7},{7,4},{8,9},{9,10},{10,1... | collective-permute-start | bytes 3145736 | tf_op jit(solution)/shard_map/ppermute | solution.py:241
  141.3 46.5 %collective-permute-start.1 = (bf16[1024,512]{1,0:T(8,128)(2,1)}, bf16[1024,512]{1,0:T(8,128)(2,1)}, u32[]{:S(2)}, u32[]{:S(2)}) collective-permute-start(bf16[1024,512]{1,0:T(8,128)(2,1)} %fusion.2), channel_id=1, source_target_pairs={{0,3},{1,0},{2,1},{3,2},{4,7},{5,4},{6,5},{7,6},{8,11},{9,8},{10,9... | collective-permute-start | bytes 3145736 | tf_op jit(solution)/shard_map/ppermute | solution.py:242
  141.3 46.5 %collective-permute-start.2 = (bf16[1024,512]{1,0:T(8,128)(2,1)}, bf16[1024,512]{1,0:T(8,128)(2,1)}, u32[]{:S(2)}, u32[]{:S(2)}) collective-permute-start(bf16[1024,512]{1,0:T(8,128)(2,1)} %fusion.2), channel_id=1, source_target_pairs={{0,2},{1,3},{2,0},{3,1},{4,6},{5,7},{6,4},{7,5},{8,10},{9,11},{10,... | collective-permute-start | bytes 3145736 | tf_op jit(solution)/shard_map/ppermute | solution.py:243
  154.9 1.9 copy-start.5
  154.9 1.9 copy-start.8
  187.8 4.3 %copy-start.3 = (bf16[4,512,256]{2,1,0:T(8,128)(2,1)S(1)}, bf16[4,512,256]{2,1,0:T(8,128)(2,1)}, u32[]{:S(2)}) copy-start(bf16[4,512,256]{2,1,0:T(8,128)(2,1)} %gather_fusion) | copy-start | bytes 3145732
  226.1 1.3 copy-start.1
  230.8 9.6 %copy-start.6 = (bf16[512,256]{1,0:T(8,128)(2,1)S(1)}, bf16[512,256]{1,0:T(8,128)(2,1)}, u32[]{:S(2)}) copy-start(bf16[512,256]{1,0:T(8,128)(2,1)} %attend.3) | copy-start | bytes 786436
  230.8 10.8 %collective-permute-start.5 = (bf16[512,256]{1,0:T(8,128)(2,1)}, bf16[512,256]{1,0:T(8,128)(2,1)}, u32[]{:S(2)}, u32[]{:S(2)}) collective-permute-start(bf16[512,256]{1,0:T(8,128)(2,1)} %attend.3), channel_id=1, source_target_pairs={{0,1},{1,2},{2,3},{3,0},{4,5},{5,6},{6,7},{7,4},{8,9},{9,10},{10,1... | collective-permute-start | bytes 786440 | tf_op jit(solution)/shard_map/ppermute | solution.py:288
  230.9 13.1 %collective-permute-start.6 = (bf16[512,256]{1,0:T(8,128)(2,1)}, bf16[512,256]{1,0:T(8,128)(2,1)}, u32[]{:S(2)}, u32[]{:S(2)}) collective-permute-start(bf16[512,256]{1,0:T(8,128)(2,1)} %attend.3), channel_id=1, source_target_pairs={{0,3},{1,0},{2,1},{3,2},{4,7},{5,4},{6,5},{7,6},{8,11},{9,8},{10,9... | collective-permute-start | bytes 786440 | tf_op jit(solution)/shard_map/ppermute | solution.py:289
  234.9 9.1 %copy-start.2 = (f32[1024,512]{1,0:T(8,128)S(1)}, f32[1024,512]{1,0:T(8,128)}, u32[]{:S(2)}) copy-start(f32[1024,512]{1,0:T(8,128)} %convolution_multiply_fusion) | copy-start | bytes 6291460
  238.4 20.5 %copy-start.4 = (bf16[3,256,512]{2,1,0:T(8,128)(2,1)S(1)}, bf16[3,256,512]{2,1,0:T(8,128)(2,1)}, u32[]{:S(2)}) copy-start(bf16[3,256,512]{2,1,0:T(8,128)(2,1)} %slice.29) | copy-start | bytes 2359300
  238.4 20.5 %copy-start.7 = (bf16[512,256]{1,0:T(8,128)(2,1)S(1)}, bf16[512,256]{1,0:T(8,128)(2,1)}, u32[]{:S(2)}) copy-start(bf16[512,256]{1,0:T(8,128)(2,1)} %attend.2) | copy-start | bytes 786436
  238.4 9.4 %collective-permute-start.3 = (bf16[512,256]{1,0:T(8,128)(2,1)}, bf16[512,256]{1,0:T(8,128)(2,1)S(1)}, u32[]{:S(2)}, u32[]{:S(2)}) collective-permute-start(bf16[512,256]{1,0:T(8,128)(2,1)} %attend.2), channel_id=1, source_target_pairs={{0,1},{1,2},{2,3},{3,0},{4,5},{5,6},{6,7},{7,4},{8,9},{9,10},{10,1... | collective-permute-start | bytes 786440 | tf_op jit(solution)/shard_map/ppermute | solution.py:285
  239.7 19.2 %collective-permute-start.4 = (bf16[512,256]{1,0:T(8,128)(2,1)}, bf16[512,256]{1,0:T(8,128)(2,1)S(1)}, u32[]{:S(2)}, u32[]{:S(2)}) collective-permute-start(bf16[512,256]{1,0:T(8,128)(2,1)} %attend.2), channel_id=1, source_target_pairs={{0,3},{1,0},{2,1},{3,2},{4,7},{5,4},{6,5},{7,6},{8,11},{9,8},{10,9... | collective-permute-start | bytes 786440 | tf_op jit(solution)/shard_map/ppermute | solution.py:286
  240.5 19.0 %collective-permute-start.8 = (bf16[512,256]{1,0:T(8,128)(2,1)S(1)}, bf16[512,256]{1,0:T(8,128)(2,1)S(1)}, u32[]{:S(2)}, u32[]{:S(2)}) collective-permute-start(bf16[512,256]{1,0:T(8,128)(2,1)S(1)} %copy-done.6), channel_id=1, source_target_pairs={{0,2},{1,3},{2,0},{3,1},{4,6},{5,7},{6,4},{7,5},{8,10},{9,11},{10,... | collective-permute-start | bytes 786440 | tf_op jit(solution)/shard_map/ppermute | solution.py:291
  241.6 17.9 %collective-permute-start.7 = (bf16[512,256]{1,0:T(8,128)(2,1)}, bf16[512,256]{1,0:T(8,128)(2,1)S(1)}, u32[]{:S(2)}, u32[]{:S(2)}) collective-permute-start(bf16[512,256]{1,0:T(8,128)(2,1)} %attend.2), channel_id=1, source_target_pairs={{0,2},{1,3},{2,0},{3,1},{4,6},{5,7},{6,4},{7,5},{8,10},{9,11},{10,... | collective-permute-start | bytes 786440 | tf_op jit(solution)/shard_map/ppermute | solution.py:290

commit v7 on v6

--- a/solution.py
+++ b/solution.py
@@ -16,21 +16,20 @@
 LANES = 128
 TILE = 8
 SHARE_ROWS = 16
-SELECT_READERS = 8
+SELECT_READERS = 16
 whole = pl.BlockSpec(memory_space=pltpu.VMEM)
 
 
 def spread_kernel(ids_ref, store_ref, gain_ref, key_ref, value_ref, out_ref, order_ref, both_ref):
-    step = pl.program_id(0)
+    group, share = pl.program_id(0), pl.program_id(1)
     passages, span, width = store_ref.shape
     rows = passages * span
-    holders, length, _ = out_ref.shape
-    groups = holders // span
+    length = out_ref.shape[1]
     half = key_ref.shape[1]
     chunks = 2 * half // LANES
     body = (length - TILE) // chunks
 
-    @pl.when(step == 0)
+    @pl.when((group == 0) & (share == 0))
     def _():
         both_ref[:, :half] = key_ref[...]
         both_ref[:, half:] = value_ref[...]
@@ -39,6 +38,9 @@
         wanted = (spot - holder * passages) * span + holder
         other = lax.broadcasted_iota(jnp.int32, (rows, rows), 1)
         order_ref[...] = jnp.where(wanted == other, 1.0, 0.0).astype(jnp.bfloat16)
+
+    @pl.when(share == 0)
+    def _():
         ids = ids_ref[...]
         ids = jnp.concatenate([ids] * (TILE // NPB), axis=0)
         owner = lax.div(ids, jnp.int32(passages))
@@ -46,20 +48,18 @@
         spare = jnp.zeros((TILE, LANES - 2 * ids.shape[1]), jnp.int32)
         tile = jnp.concatenate([owner, inside, spare], axis=1)
         tile = tile.astype(jnp.float32).astype(jnp.bfloat16)
-        out_ref[:, length - TILE :, :] = jnp.broadcast_to(tile, (holders, TILE, LANES))
+        out_ref[:, length - TILE :, :] = jnp.broadcast_to(tile, (span, TILE, LANES))
 
     wide = store_ref[...].astype(jnp.float32).reshape(rows, width)
     inverse = lax.rsqrt(jnp.mean(wide * wide, axis=-1, keepdims=True) + epsilon)
     scaled = (wide * gain_ref[...]).astype(jnp.bfloat16)
-    first = pl.multiple_of((step % groups) * span, span)
-    offset = (step // groups) * passages
     product = jnp.dot(scaled, both_ref[...], preferred_element_type=jnp.float32)
     product = (product * inverse).astype(jnp.bfloat16)
     turned = jnp.dot(order_ref[...], product, preferred_element_type=jnp.float32)
     turned = turned.reshape(span, passages, chunks * LANES).astype(jnp.bfloat16)
     for chunk in range(chunks):
-        start = pl.multiple_of(chunk * body + offset, TILE)
-        out_ref[pl.ds(first, span), pl.ds(start, passages), :] = turned[
+        start = pl.multiple_of(chunk * body + share * passages, TILE)
+        out_ref[:, pl.ds(start, passages), :] = turned[
             :, :, chunk * LANES : (chunk + 1) * LANES
         ]
 
@@ -69,17 +69,18 @@
     head_width = key_weight.shape[1]
     rows = passages * SHARE_ROWS
     per_holder = passages * length // holders * (2 * head_width // LANES) + TILE
+    groups = holders // SHARE_ROWS
     return pl.pallas_call(
         spread_kernel,
-        grid=(length // SHARE_ROWS,),
+        grid=(groups, length // holders),
         in_specs=[
-            pl.BlockSpec(ids.shape, lambda i: (0, 0)),
-            pl.BlockSpec((passages, SHARE_ROWS, width), lambda i: (0, i, 0)),
-            pl.BlockSpec((1, width), lambda i: (0, 0)),
-            pl.BlockSpec((width, head_width), lambda i: (0, 0)),
-            pl.BlockSpec((width, head_width), lambda i: (0, 0)),
+            pl.BlockSpec(ids.shape, lambda g, i: (0, 0)),
+            pl.BlockSpec((passages, SHARE_ROWS, width), lambda g, i: (0, i * groups + g, 0)),
+            pl.BlockSpec((1, width), lambda g, i: (0, 0)),
+            pl.BlockSpec((width, head_width), lambda g, i: (0, 0)),
+            pl.BlockSpec((width, head_width), lambda g, i: (0, 0)),
         ],
-        out_specs=pl.BlockSpec((holders, per_holder, LANES), lambda i: (0, 0, 0)),
+        out_specs=pl.BlockSpec((SHARE_ROWS, per_holder, LANES), lambda g, i: (g, 0, 0)),
         out_shape=jax.ShapeDtypeStruct((holders, per_holder, LANES), jnp.bfloat16),
         scratch_shapes=[
             pltpu.VMEM((rows, rows), jnp.bfloat16),
@@ -137,10 +138,11 @@
     )(held)
 
 
-def attend_kernel(query_ref, gate_ref, table_ref, out_ref):
+def attend_kernel(query_ref, gate_ref, table_ref, out_ref, keys_ref, scores_ref):
     holders, slots, _ = table_ref.shape
-    width = query_ref.shape[1]
+    rows, width = query_ref.shape
     both = 2 * width
+    heads = width // HD
     early = lax.broadcasted_iota(jnp.int32, (holders, TILE, both), 1) < NPB
     for pair in range(slots // TILE):
         here = slice(pair * TILE, (pair + 1) * TILE)
@@ -151,27 +153,30 @@
             jnp.where(early, pltpu.roll(first, NPB, 1), second),
         )
         for place, table in enumerate(tables):
-            table = table.reshape(holders * TILE, both).astype(jnp.bfloat16)
-            block = 2 * pair + place
+            keys_ref[2 * pair + place] = table.reshape(holders * TILE, both).astype(jnp.bfloat16)
+    for head in range(heads):
+        cols = slice(head * HD, (head + 1) * HD)
+        for block in range(rows // BLK):
             mine = slice(block * BLK, (block + 1) * BLK)
-            for head in range(width // HD):
-                cols = slice(head * HD, (head + 1) * HD)
-                late = slice(width + head * HD, width + (head + 1) * HD)
-                scores = lax.dot_general(
-                    query_ref[mine, cols],
-                    table[:, cols],
-                    (((1,), (1,)), ((), ())),
-                    preferred_element_type=jnp.float32,
-                ) * HD ** (-0.5)
-                weights = jnp.exp(scores - jnp.max(scores, axis=-1, keepdims=True))
-                total = jnp.sum(weights, axis=-1, keepdims=True)
-                probabilities = (weights * (1.0 / total)).astype(jnp.bfloat16)
-                attended = jnp.dot(
-                    probabilities, table[:, late], preferred_element_type=jnp.float32
-                )
-                out_ref[mine, cols] = (attended * gate_ref[mine, head : head + 1]).astype(
-                    jnp.bfloat16
-                )
+            scores_ref[head, mine, :] = lax.dot_general(
+                query_ref[mine, cols],
+                keys_ref[block, :, cols],
+                (((1,), (1,)), ((), ())),
+                preferred_element_type=jnp.float32,
+            ) * HD ** (-0.5)
+    for head in range(heads):
+        cols = slice(head * HD, (head + 1) * HD)
+        late = slice(width + head * HD, width + (head + 1) * HD)
+        scores = scores_ref[head]
+        weights = jnp.exp(scores - jnp.max(scores, axis=-1, keepdims=True))
+        total = jnp.sum(weights, axis=-1, keepdims=True)
+        probabilities = (weights * (1.0 / total)).astype(jnp.bfloat16)
+        for block in range(rows // BLK):
+            mine = slice(block * BLK, (block + 1) * BLK)
+            attended = jnp.dot(
+                probabilities[mine, :], keys_ref[block, :, late], preferred_element_type=jnp.float32
+            )
+            out_ref[mine, cols] = (attended * gate_ref[mine, head : head + 1]).astype(jnp.bfloat16)
 
 
 def attend(queries, gates, table, half):
@@ -188,6 +193,10 @@
         ],
         out_specs=pl.BlockSpec((rows, width), lambda i: (0, 0)),
         out_shape=jax.ShapeDtypeStruct((rows, width), jnp.bfloat16),
+        scratch_shapes=[
+            pltpu.VMEM((rows // BLK, holders * TILE, both // 2), jnp.bfloat16),
+            pltpu.VMEM((width // HD, rows, holders * TILE), jnp.float32),
+        ],
         name="attend",
     )(queries, gates, table)
 
@@ -287,8 +296,8 @@
     high = attend(queries, gating, returned, 1)
     high_before = lax.ppermute(high, "tp", up)
     high_after = lax.ppermute(high, "tp", down)
-    low_far = lax.ppermute(low, "tp", across)
-    high_far = lax.ppermute(high, "tp", across)
+    low_far = lax.ppermute(low_before, "tp", up)
+    high_far = lax.ppermute(high_after, "tp", down)
     near = weights[:3].reshape(-1, width_local)
     low_near = jnp.concatenate([low, low_before, low_after], axis=1)
     low_base = base[:half] + jnp.dot(low_near, near, preferred_element_type=jnp.float32)

time: 263 us -> 258 us (0.981)
  the two profiles are of different devices: /device:TPU:46 before, /device:TPU:40 now
where the time goes in v7:
time: 258 us; the launch traced here: 257 us
  blocking collectives  117 us (45%)
  waiting for transfers between devices  68.5 us (27%)
  Pallas kernels  20.7 us (8%)
  starting transfers between devices  16.8 us (7%)
  matrix products  14.4 us (6%)
  other arithmetic  12.2 us (5%)
  local copies, waits for them, and re-layouts  8.01 us (3%)
    all_to_all x1, blocking collectives, per_device(): held = lax.all_to_all(spread, 'st', split_axis=0, concat_axis=0, tiled=True)  106 us
    all_to_all x1, waiting for transfers between devices, per_device(): lax.all_to_all(packed.reshape(st_count, -1, shares * width_both), 'st', s...  29.5 us
    ppermute x1, waiting for transfers between devices, per_device(): before = lax.ppermute(normed, 'tp', up)  27.5 us
    psum x1, blocking collectives, per_device(): square_sums = lax.psum(jnp.sum(wide_tokens * wide_tokens, axis=1), 'tp')  10.9 us
    pallas_call x1, Pallas kernels, spread_store(): pl.pallas_call(spread_kernel, grid=(groups, length // holders), in_specs=...  9.14 us
    pallas_call x2, Pallas kernels, attend(): pl.pallas_call(attend_kernel, grid=(1,), in_specs=[pl.BlockSpec((rows, wi...  6.3 us
    ppermute x1, waiting for transfers between devices, per_device(): high_before = lax.ppermute(high, 'tp', up)  5.61 us
    pallas_call x1, Pallas kernels, select_rows(): pl.pallas_call(lambda *refs: select_kernel(blocks, shares, *refs), grid=(...  5.22 us
  transfers between devices with their start and end apart: 10, of which 5 were waited for; matrix products, arithmetic and copies ran while one was open for 12% of the time, Pallas kernels for 1%

profile of v7, /device:TPU:40, one launch (start us, length us, event | category | flops | bytes accessed | tf_op | source)
XLA Modules:
  0.0 257.4 jit_solution(8166033389030887664)
XLA Ops:
  0.0 9.1 %spread_store.1 = bf16[32,200,128]{2,1,0:T(8,128)(2,1)} custom-call(s32[4,8]{1,0:T(4,128)} %bitcast.33, bf16[24,64,2048]{2,1,0:T(8,128)(2,1)} %store_ref.1, f32[1,2048]{1,0:T(1,128)} %bitcast.32, bf16[2048,256]{1,0:T(8,128)(2,1)} %key_ref.1, bf16[2048,256]{1,0:T(8,128)(2,1)} %value_ref.1), custom_call_target="tpu_custom_call" | custom-call | tf_op jit(solution)/shard_map/spread_store/pallas_call | solution.py:73
  9.1 105.7 %all_to_all.10.refs_0_ = bf16[32,200,128]{2,1,0:T(8,128)(2,1)} all-to-all(bf16[32,200,128]{2,1,0:T(8,128)(2,1)} %spread_store.1), channel_id=1, replica_groups=mesh['grp'=2,'st'=32,'tp'=4] {'st'}, dimensions={0} | all-to-all | bytes 3276800 | tf_op jit(solution)/shard_map/all_to_all | solution.py:229
  114.9 5.2 %select_rows.1 = bf16[1024,1024]{1,0:T(8,128)(2,1)} custom-call(bf16[32,200,128]{2,1,0:T(8,128)(2,1)} %all_to_all.10.refs_0_), custom_call_target="tpu_custom_call" | custom-call | tf_op jit(solution)/shard_map/select_rows/pallas_call | solution.py:130
  120.1 4.9 %all-to-all-start.1 = ((bf16[32,32,1024]{2,1,0:T(8,128)(2,1)}), bf16[32,32,1024]{2,1,0:T(8,128)(2,1)S(1)}, u32[]{:S(2)}, u32[]{:S(2)}) async-start(bf16[32,32,1024]{2,1,0:T(8,128)(2,1)} %bitcast.26), calls=%async_computation.1 | async-start | bytes 4194304 | tf_op jit(solution)/shard_map/all_to_all | solution.py:232
  125.0 0.8 dynamic_slice.6
  125.8 1.5 fusion
  127.3 10.9 %psum.7 = f32[1024]{0:T(1024)S(1)} all-reduce(f32[1024]{0:T(1024)S(1)} %fusion), channel_id=1, replica_groups=mesh['grp'=2,'st'=32,'tp'=4] {'tp'}, use_global_device_ids=true, to_apply=%region_1.0 | all-reduce | flops 1024 | bytes 8192 | tf_op jit(solution)/shard_map/psum | solution.py:241
  138.3 2.5 fusion.2
  140.8 3.2 %collective-permute-start.1 = (bf16[1024,512]{1,0:T(8,128)(2,1)}, bf16[1024,512]{1,0:T(8,128)(2,1)}, u32[]{:S(2)}, u32[]{:S(2)}) collective-permute-start(bf16[1024,512]{1,0:T(8,128)(2,1)} %fusion.2), channel_id=1, source_target_pairs={{0,3},{1,0},{2,1},{3,2},{4,7},{5,4},{6,5},{7,6},{8,11},{9,8},{10,9... | collective-permute-start | bytes 3145736 | tf_op jit(solution)/shard_map/ppermute | solution.py:251
  144.0 0.8 constant_dynamic-slice_fusion
  144.8 0.6 gather_fusion.1
  145.4 1.7 gather_fusion
  147.1 2.8 %convert.1 = f32[4,256,512]{2,1,0:T(8,128)} convert(bf16[4,256,512]{2,1,0:T(8,128)(2,1)} %bitcast.5) | non-fusion elementwise | flops 524288 | bytes 3145728 | tf_op jit(solution)/shard_map/reshape | solution.py:257
  149.9 2.8 %gather_fusion.2 = bf16[4,256,512]{2,1,0:T(8,128)(2,1)} fusion(bf16[4,256,512]{2,1,0:T(8,128)(2,1)} %bitcast.28, s32[1024]{0:T(1024)S(1)} %pad_clamp_fusion), kind=kCustom, calls=%fused_computation.2 | custom fusion | bytes 2097168 | tf_op jit(solution)/shard_map/jit(_take)/gather | solution.py:276
  152.7 2.7 %add_select_fusion.3 = f32[4,256,512]{2,1,0:T(8,128)S(1)} fusion(f32[4,256,512]{2,1,0:T(8,128)} %convert.1, pred[]{:T(512)S(6)} %ge.15), kind=kLoop, calls=%fused_computation.7 | loop fusion | flops 1048576 | bytes 4194305 | tf_op jit(solution)/shard_map/jit(_where)/select_n | solution.py:262
  156.2 1.9 fusion.6
  158.1 2.0 convolution_multiply_fusion
  160.1 27.5 %collective-permute-done = bf16[1024,512]{1,0:T(8,128)(2,1)} collective-permute-done((bf16[1024,512]{1,0:T(8,128)(2,1)}, bf16[1024,512]{1,0:T(8,128)(2,1)}, u32[]{:S(2)}, u32[]{:S(2)}) %collective-permute-start) | collective-permute-done | bytes 1048608 | tf_op jit(solution)/shard_map/ppermute | solution.py:250
  187.6 4.3 %fusion.9.gate_ref = f32[1024,2]{1,0:T(8,128)} fusion(bf16[2048,2]{0,1:T(2,128)(2,1)S(1)} %bitcast.25, bf16[1024,512]{1,0:T(8,128)(2,1)} %collective-permute-done.2, bf16[1024,512]{1,0:T(8,128)(2,1)} %collective-permute-done.1, bf16[1024,512]{1,0:T(8,128)(2,1)} %collective-permute-done, bf16[1024,512]{1,0:T(8,128)(2,1)} %fusion.2), kind=kOutput, calls=%fused_computation.29 | convolution fusion | flops 25171968 | bytes 4210688 | tf_op jit(solution)/shard_map/dot_general | solution.py:284
  191.9 4.3 %convolution_convert_fusion.query_ref = bf16[1024,256]{1,0:T(8,128)(2,1)} fusion(bf16[2048,256]{1,0:T(8,128)(2,1)S(1)} %bitcast.29, bf16[1024,512]{1,0:T(8,128)(2,1)} %collective-permute-done.2, bf16[1024,512]{1,0:T(8,128)(2,1)} %collective-permute-done.1, bf16[1024,512]{1,0:T(8,128)(2,1)} %collective-permute-done, bf16[1024,512]{1,0:T(8,128)(2,1)} %fusion.2), kind=kOutput, calls=%fused_computation.25 | convolution fusion | flops 1090781184 | bytes 5767168 | tf_op jit(solution)/shard_map/dot_general | solution.py:281
  196.1 29.5 %all-to-all-done.1.table_ref = bf16[32,32,1024]{2,1,0:T(8,128)(2,1)S(1)} async-done(((bf16[32,32,1024]{2,1,0:T(8,128)(2,1)}), bf16[32,32,1024]{2,1,0:T(8,128)(2,1)S(1)}, u32[]{:S(2)}, u32[]{:S(2)}) %all-to-all-start.1) | async-done | bytes 2097184 | tf_op jit(solution)/shard_map/all_to_all | solution.py:232
  225.7 1.3 copy-done.1
  227.0 3.2 %attend.3 = bf16[512,256]{1,0:T(8,128)(2,1)} custom-call(bf16[1024,256]{1,0:T(8,128)(2,1)} %convolution_convert_fusion.query_ref, f32[1024,2]{1,0:T(8,128)} %fusion.9.gate_ref, bf16[32,32,1024]{2,1,0:T(8,128)(2,1)} %copy-done.1), custom_call_target="tpu_custom_call" | custom-call | tf_op jit(solution)/shard_map/attend/pallas_call | solution.py:186
  230.2 3.2 %collective-permute-start.6 = (bf16[512,256]{1,0:T(8,128)(2,1)}, bf16[512,256]{1,0:T(8,128)(2,1)}, u32[]{:S(2)}, u32[]{:S(2)}) collective-permute-start(bf16[512,256]{1,0:T(8,128)(2,1)} %attend.3), channel_id=1, source_target_pairs={{0,3},{1,0},{2,1},{3,2},{4,7},{5,4},{6,5},{7,6},{8,11},{9,8},{10,9... | collective-permute-start | bytes 786440 | tf_op jit(solution)/shard_map/ppermute | solution.py:298
  233.3 3.1 %attend.2 = bf16[512,256]{1,0:T(8,128)(2,1)} custom-call(bf16[1024,256]{1,0:T(8,128)(2,1)} %convolution_convert_fusion.query_ref, f32[1024,2]{1,0:T(8,128)} %fusion.9.gate_ref, bf16[32,32,1024]{2,1,0:T(8,128)(2,1)} %copy-done.1), custom_call_target="tpu_custom_call" | custom-call | tf_op jit(solution)/shard_map/attend/pallas_call | solution.py:186
  237.1 2.9 %collective-permute-start.4 = (bf16[512,256]{1,0:T(8,128)(2,1)}, bf16[512,256]{1,0:T(8,128)(2,1)S(1)}, u32[]{:S(2)}, u32[]{:S(2)}) collective-permute-start(bf16[512,256]{1,0:T(8,128)(2,1)} %attend.2), channel_id=1, source_target_pairs={{0,3},{1,0},{2,1},{3,2},{4,7},{5,4},{6,5},{7,6},{8,11},{9,8},{10,9... | collective-permute-start | bytes 786440 | tf_op jit(solution)/shard_map/ppermute | solution.py:295
  239.9 2.1 collective-permute-start.8
  242.0 5.0 %collective-permute-done.3 = bf16[512,256]{1,0:T(8,128)(2,1)S(1)} collective-permute-done((bf16[512,256]{1,0:T(8,128)(2,1)}, bf16[512,256]{1,0:T(8,128)(2,1)S(1)}, u32[]{:S(2)}, u32[]{:S(2)}) %collective-permute-start.3) | collective-permute-done | bytes 262176 | tf_op jit(solution)/shard_map/ppermute | solution.py:294
  247.1 5.6 %collective-permute-done.5 = bf16[512,256]{1,0:T(8,128)(2,1)S(1)} collective-permute-done((bf16[512,256]{1,0:T(8,128)(2,1)S(1)}, bf16[512,256]{1,0:T(8,128)(2,1)S(1)}, u32[]{:S(2)}, u32[]{:S(2)}) %collective-permute-start.5) | collective-permute-done | bytes 262176 | tf_op jit(solution)/shard_map/ppermute | solution.py:297
  252.7 1.9 convolution_add_fusion
  255.2 0.8 collective-permute-done.7
  256.0 1.4 fusion.5
  (37 shorter events, 1.9 us)
Async XLA Ops:
  0.0 145.4 %copy-start = (bf16[2048,256]{1,0:T(8,128)(2,1)S(1)}, bf16[2048,256]{1,0:T(8,128)(2,1)}, u32[]{:S(2)}) copy-start(bf16[2048,256]{1,0:T(8,128)(2,1)} %param.17) | copy-start | bytes 3145732
  120.1 105.6 %all-to-all-start.1 = ((bf16[32,32,1024]{2,1,0:T(8,128)(2,1)}), bf16[32,32,1024]{2,1,0:T(8,128)(2,1)S(1)}, u32[]{:S(2)}, u32[]{:S(2)}) async-start(bf16[32,32,1024]{2,1,0:T(8,128)(2,1)} %bitcast.26), calls=%async_computation.1 | async-start | bytes 4194304 | tf_op jit(solution)/shard_map/all_to_all | solution.py:232
  125.0 19.0 %copy-start.9 = (s32[4]{0:T(128)S(1)}, s32[4]{0:T(128)}, u32[]{:S(2)}) copy-start(s32[4]{0:T(128)} %constant.44.clone) | copy-start | bytes 52
  140.8 46.8 %collective-permute-start = (bf16[1024,512]{1,0:T(8,128)(2,1)}, bf16[1024,512]{1,0:T(8,128)(2,1)}, u32[]{:S(2)}, u32[]{:S(2)}) collective-permute-start(bf16[1024,512]{1,0:T(8,128)(2,1)} %fusion.2), channel_id=1, source_target_pairs={{0,1},{1,2},{2,3},{3,0},{4,5},{5,6},{6,7},{7,4},{8,9},{9,10},{10,1... | collective-permute-start | bytes 3145736 | tf_op jit(solution)/shard_map/ppermute | solution.py:250
  140.8 46.8 %collective-permute-start.1 = (bf16[1024,512]{1,0:T(8,128)(2,1)}, bf16[1024,512]{1,0:T(8,128)(2,1)}, u32[]{:S(2)}, u32[]{:S(2)}) collective-permute-start(bf16[1024,512]{1,0:T(8,128)(2,1)} %fusion.2), channel_id=1, source_target_pairs={{0,3},{1,0},{2,1},{3,2},{4,7},{5,4},{6,5},{7,6},{8,11},{9,8},{10,9... | collective-permute-start | bytes 3145736 | tf_op jit(solution)/shard_map/ppermute | solution.py:251
  144.0 43.6 %collective-permute-start.2 = (bf16[1024,512]{1,0:T(8,128)(2,1)}, bf16[1024,512]{1,0:T(8,128)(2,1)}, u32[]{:S(2)}, u32[]{:S(2)}) collective-permute-start(bf16[1024,512]{1,0:T(8,128)(2,1)} %fusion.2), channel_id=1, source_target_pairs={{0,2},{1,3},{2,0},{3,1},{4,6},{5,7},{6,4},{7,5},{8,10},{9,11},{10,... | collective-permute-start | bytes 3145736 | tf_op jit(solution)/shard_map/ppermute | solution.py:252
  156.2 1.9 copy-start.5
  156.2 1.9 copy-start.8
  187.6 4.3 %copy-start.4 = (bf16[4,512,256]{2,1,0:T(8,128)(2,1)S(1)}, bf16[4,512,256]{2,1,0:T(8,128)(2,1)}, u32[]{:S(2)}) copy-start(bf16[4,512,256]{2,1,0:T(8,128)(2,1)} %gather_fusion) | copy-start | bytes 3145732
  225.7 1.3 copy-start.1
  230.2 6.3 %copy-start.7 = (bf16[512,256]{1,0:T(8,128)(2,1)S(1)}, bf16[512,256]{1,0:T(8,128)(2,1)}, u32[]{:S(2)}) copy-start(bf16[512,256]{1,0:T(8,128)(2,1)} %attend.3) | copy-start | bytes 786436
  230.2 6.8 %copy-start.2 = (bf16[4,256,512]{2,1,0:T(8,128)(2,1)S(1)}, bf16[4,256,512]{2,1,0:T(8,128)(2,1)}, u32[]{:S(2)}) copy-start(bf16[4,256,512]{2,1,0:T(8,128)(2,1)} %gather_fusion.2) | copy-start | bytes 3145732
  230.2 9.8 %collective-permute-start.6 = (bf16[512,256]{1,0:T(8,128)(2,1)}, bf16[512,256]{1,0:T(8,128)(2,1)}, u32[]{:S(2)}, u32[]{:S(2)}) collective-permute-start(bf16[512,256]{1,0:T(8,128)(2,1)} %attend.3), channel_id=1, source_target_pairs={{0,3},{1,0},{2,1},{3,2},{4,7},{5,4},{6,5},{7,6},{8,11},{9,8},{10,9... | collective-permute-start | bytes 786440 | tf_op jit(solution)/shard_map/ppermute | solution.py:298
  236.5 10.6 %collective-permute-start.3 = (bf16[512,256]{1,0:T(8,128)(2,1)}, bf16[512,256]{1,0:T(8,128)(2,1)S(1)}, u32[]{:S(2)}, u32[]{:S(2)}) collective-permute-start(bf16[512,256]{1,0:T(8,128)(2,1)} %attend.2), channel_id=1, source_target_pairs={{0,1},{1,2},{2,3},{3,0},{4,5},{5,6},{6,7},{7,4},{8,9},{9,10},{10,1... | collective-permute-start | bytes 786440 | tf_op jit(solution)/shard_map/ppermute | solution.py:294
  236.5 16.2 %collective-permute-start.5 = (bf16[512,256]{1,0:T(8,128)(2,1)S(1)}, bf16[512,256]{1,0:T(8,128)(2,1)S(1)}, u32[]{:S(2)}, u32[]{:S(2)}) collective-permute-start(bf16[512,256]{1,0:T(8,128)(2,1)S(1)} %copy-done.7), channel_id=1, source_target_pairs={{0,1},{1,2},{2,3},{3,0},{4,5},{5,6},{6,7},{7,4},{8,9},{9,10},{10,1... | collective-permute-start | bytes 786440 | tf_op jit(solution)/shard_map/ppermute | solution.py:297
  237.0 17.6 %copy-start.3 = (f32[1024,512]{1,0:T(8,128)S(1)}, f32[1024,512]{1,0:T(8,128)}, u32[]{:S(2)}) copy-start(f32[1024,512]{1,0:T(8,128)} %convolution_multiply_fusion) | copy-start | bytes 6291460
  237.0 17.6 %copy-start.6 = (bf16[512,256]{1,0:T(8,128)(2,1)S(1)}, bf16[512,256]{1,0:T(8,128)(2,1)}, u32[]{:S(2)}) copy-start(bf16[512,256]{1,0:T(8,128)(2,1)} %attend.2) | copy-start | bytes 786436
  237.1 17.5 %collective-permute-start.4 = (bf16[512,256]{1,0:T(8,128)(2,1)}, bf16[512,256]{1,0:T(8,128)(2,1)S(1)}, u32[]{:S(2)}, u32[]{:S(2)}) collective-permute-start(bf16[512,256]{1,0:T(8,128)(2,1)} %attend.2), channel_id=1, source_target_pairs={{0,3},{1,0},{2,1},{3,2},{4,7},{5,4},{6,5},{7,6},{8,11},{9,8},{10,9... | collective-permute-start | bytes 786440 | tf_op jit(solution)/shard_map/ppermute | solution.py:295
  239.9 15.3 %collective-permute-start.8 = (bf16[512,256]{1,0:T(8,128)(2,1)}, bf16[512,256]{1,0:T(8,128)(2,1)S(1)}, u32[]{:S(2)}, u32[]{:S(2)}) collective-permute-start(bf16[512,256]{1,0:T(8,128)(2,1)} %collective-permute-done.6), channel_id=1, source_target_pairs={{0,3},{1,0},{2,1},{3,2},{4,7},{5,4},{6,5},{7,6},{8,11},{9,8},{10,9... | collective-permute-start | bytes 786440 | tf_op jit(solution)/shard_map/ppermute | solution.py:300
  247.1 8.9 %collective-permute-start.7 = (bf16[512,256]{1,0:T(8,128)(2,1)S(1)}, bf16[512,256]{1,0:T(8,128)(2,1)S(1)}, u32[]{:S(2)}, u32[]{:S(2)}) collective-permute-start(bf16[512,256]{1,0:T(8,128)(2,1)S(1)} %collective-permute-done.3), channel_id=1, source_target_pairs={{0,1},{1,2},{2,3},{3,0},{4,5},{5,6},{6,7},{7,4},{8,9},{9,10},{10,1... | collective-permute-start | bytes 786440 | tf_op jit(solution)/shard_map/ppermute | solution.py:299

commit v8 on v7

--- a/solution.py
+++ b/solution.py
@@ -288,7 +288,10 @@
     gating = jax.nn.sigmoid(gate_sum)
 
     weights = turn(out_weight)
-    queries, gating, base, weights = lax.optimization_barrier((queries, gating, base, weights))
+    near = weights[:3].reshape(-1, width_local)
+    queries, gating, base, near, distant = lax.optimization_barrier(
+        (queries, gating, base, near, weights[3])
+    )
 
     low = attend(queries, gating, returned, 0)
     low_before = lax.ppermute(low, "tp", up)
@@ -298,7 +301,6 @@
     high_after = lax.ppermute(high, "tp", down)
     low_far = lax.ppermute(low_before, "tp", up)
     high_far = lax.ppermute(high_after, "tp", down)
-    near = weights[:3].reshape(-1, width_local)
     low_near = jnp.concatenate([low, low_before, low_after], axis=1)
     low_base = base[:half] + jnp.dot(low_near, near, preferred_element_type=jnp.float32)
     high_near = jnp.concatenate([high, high_before, high_after], axis=1)
@@ -306,9 +308,7 @@
     low_base, high_base = lax.optimization_barrier((low_base, high_base))
     far = jnp.concatenate([low_far, high_far], axis=0)
     base = jnp.concatenate([low_base, high_base], axis=0)
-    return (base + jnp.dot(far, weights[3], preferred_element_type=jnp.float32)).astype(
-        jnp.bfloat16
-    )
+    return (base + jnp.dot(far, distant, preferred_element_type=jnp.float32)).astype(jnp.bfloat16)
 
 
 def solution(mesh):

time: 258 us -> 258 us (level)
  waiting for transfers between devices: 68.5 us -> 62.8 us
  local copies, waits for them, and re-layouts: 8.01 us -> 11 us
  other arithmetic: 12.2 us -> 14.9 us
    ppermute x1, waiting for transfers between devices: 27.5 us -> 21.7 us  [per_device(): before = lax.ppermute(normed, 'tp', up)]
  transfers between devices with their start and end apart: 10 -> 10, of which waited for: 5 -> 5; matrix products, arithmetic and copies ran while one was open for 12% -> 15% of each run, Pallas kernels for 1% -> 1%
where the time goes in v8:
time: 258 us; the launch traced here: 257 us
  blocking collectives  117 us (45%)
  waiting for transfers between devices  62.8 us (24%)
  Pallas kernels  20.7 us (8%)
  starting transfers between devices  16.9 us (7%)
  other arithmetic  14.9 us (6%)
  matrix products  14.4 us (6%)
  local copies, waits for them, and re-layouts  11 us (4%)
    all_to_all x1, blocking collectives, per_device(): held = lax.all_to_all(spread, 'st', split_axis=0, concat_axis=0, tiled=True)  106 us
    all_to_all x1, waiting for transfers between devices, per_device(): lax.all_to_all(packed.reshape(st_count, -1, shares * width_both), 'st', s...  29.6 us
    ppermute x1, waiting for transfers between devices, per_device(): before = lax.ppermute(normed, 'tp', up)  21.7 us
    psum x1, blocking collectives, per_device(): square_sums = lax.psum(jnp.sum(wide_tokens * wide_tokens, axis=1), 'tp')  10.9 us
    pallas_call x1, Pallas kernels, spread_store(): pl.pallas_call(spread_kernel, grid=(groups, length // holders), in_specs=...  9.16 us
    pallas_call x2, Pallas kernels, attend(): pl.pallas_call(attend_kernel, grid=(1,), in_specs=[pl.BlockSpec((rows, wi...  6.33 us
    ppermute x1, waiting for transfers between devices, per_device(): high_before = lax.ppermute(high, 'tp', up)  5.61 us
    pallas_call x1, Pallas kernels, select_rows(): pl.pallas_call(lambda *refs: select_kernel(blocks, shares, *refs), grid=(...  5.21 us
  transfers between devices with their start and end apart: 10, of which 5 were waited for; matrix products, arithmetic and copies ran while one was open for 15% of the time, Pallas kernels for 1%

profile of v8, /device:TPU:40, one launch (start us, length us, event | category | flops | bytes accessed | tf_op | source)
XLA Modules:
  0.0 257.5 jit_solution(12708261780824191244)
XLA Ops:
  0.0 9.2 %spread_store.1 = bf16[32,200,128]{2,1,0:T(8,128)(2,1)} custom-call(s32[4,8]{1,0:T(4,128)} %bitcast.33, bf16[24,64,2048]{2,1,0:T(8,128)(2,1)} %store_ref.1, f32[1,2048]{1,0:T(1,128)} %bitcast.32, bf16[2048,256]{1,0:T(8,128)(2,1)} %key_ref.1, bf16[2048,256]{1,0:T(8,128)(2,1)} %value_ref.1), custom_call_target="tpu_custom_call" | custom-call | tf_op jit(solution)/shard_map/spread_store/pallas_call | solution.py:73
  9.2 105.7 %all_to_all.10.refs_0_ = bf16[32,200,128]{2,1,0:T(8,128)(2,1)} all-to-all(bf16[32,200,128]{2,1,0:T(8,128)(2,1)} %spread_store.1), channel_id=1, replica_groups=mesh['grp'=2,'st'=32,'tp'=4] {'st'}, dimensions={0} | all-to-all | bytes 3276800 | tf_op jit(solution)/shard_map/all_to_all | solution.py:229
  114.9 5.2 %select_rows.1 = bf16[1024,1024]{1,0:T(8,128)(2,1)} custom-call(bf16[32,200,128]{2,1,0:T(8,128)(2,1)} %all_to_all.10.refs_0_), custom_call_target="tpu_custom_call" | custom-call | tf_op jit(solution)/shard_map/select_rows/pallas_call | solution.py:130
  120.1 4.9 %all-to-all-start.1 = ((bf16[32,32,1024]{2,1,0:T(8,128)(2,1)}), bf16[32,32,1024]{2,1,0:T(8,128)(2,1)S(1)}, u32[]{:S(2)}, u32[]{:S(2)}) async-start(bf16[32,32,1024]{2,1,0:T(8,128)(2,1)} %bitcast.26), calls=%async_computation.1 | async-start | bytes 4194304 | tf_op jit(solution)/shard_map/all_to_all | solution.py:232
  125.8 1.5 fusion
  127.3 10.9 %psum.7 = f32[1024]{0:T(1024)S(1)} all-reduce(f32[1024]{0:T(1024)S(1)} %fusion), channel_id=1, replica_groups=mesh['grp'=2,'st'=32,'tp'=4] {'tp'}, use_global_device_ids=true, to_apply=%region_1.0 | all-reduce | flops 1024 | bytes 8192 | tf_op jit(solution)/shard_map/psum | solution.py:241
  138.3 2.5 fusion.2
  140.8 3.2 %collective-permute-start.1 = (bf16[1024,512]{1,0:T(8,128)(2,1)}, bf16[1024,512]{1,0:T(8,128)(2,1)}, u32[]{:S(2)}, u32[]{:S(2)}) collective-permute-start(bf16[1024,512]{1,0:T(8,128)(2,1)} %fusion.2), channel_id=1, source_target_pairs={{0,3},{1,0},{2,1},{3,2},{4,7},{5,4},{6,5},{7,6},{8,11},{9,8},{10,9... | collective-permute-start | bytes 3145736 | tf_op jit(solution)/shard_map/ppermute | solution.py:251
  144.0 2.9 %convert.1 = f32[4,256,512]{2,1,0:T(8,128)} convert(bf16[4,256,512]{2,1,0:T(8,128)(2,1)} %bitcast.5) | non-fusion elementwise | flops 524288 | bytes 3145728 | tf_op jit(solution)/shard_map/reshape | solution.py:257
  147.7 2.7 %add_select_fusion.3 = f32[4,256,512]{2,1,0:T(8,128)S(1)} fusion(f32[4,256,512]{2,1,0:T(8,128)} %convert.1, pred[]{:T(512)S(6)} %ge.15), kind=kLoop, calls=%fused_computation.7 | loop fusion | flops 1048576 | bytes 4194305 | tf_op jit(solution)/shard_map/jit(_where)/select_n | solution.py:262
  150.8 1.6 add_select_fusion.1
  153.0 1.7 gather_fusion
  154.7 2.8 %gather_fusion.2 = bf16[4,256,512]{2,1,0:T(8,128)(2,1)} fusion(bf16[4,256,512]{2,1,0:T(8,128)(2,1)} %bitcast.28, s32[1024]{0:T(1024)S(1)} %pad_clamp_fusion), kind=kCustom, calls=%fused_computation.2 | custom fusion | bytes 2097168 | tf_op jit(solution)/shard_map/jit(_take)/gather | solution.py:276
  157.5 2.1 slice.38
  159.6 1.0 slice_bitcast_fusion
  160.6 3.3 %fusion.6 = bf16[4,256,512]{2,1,0:T(8,128)(2,1)S(1)} fusion(f32[4,256,512]{2,1,0:T(8,128)} %add_select_fusion.1, f32[256]{0:T(256)S(1)} %minimum_convert_fusion, pred[]{:T(512)S(6)} %ge.12, bf16[4,256,512]{2,1,0:T(8,128)(2,1)} %bitcast.5), kind=kLoop, calls=%fused_computation.21 | loop fusion | flops 3145728 | bytes 4195329 | tf_op jit(solution)/shard_map/convert_element_type | solution.py:267
  163.8 2.0 convolution_multiply_fusion
  165.9 21.7 %collective-permute-done = bf16[1024,512]{1,0:T(8,128)(2,1)} collective-permute-done((bf16[1024,512]{1,0:T(8,128)(2,1)}, bf16[1024,512]{1,0:T(8,128)(2,1)}, u32[]{:S(2)}, u32[]{:S(2)}) %collective-permute-start) | collective-permute-done | bytes 1048608 | tf_op jit(solution)/shard_map/ppermute | solution.py:250
  187.6 4.3 %fusion.9.gate_ref = f32[1024,2]{1,0:T(8,128)} fusion(bf16[2048,2]{0,1:T(2,128)(2,1)S(1)} %bitcast.25, bf16[1024,512]{1,0:T(8,128)(2,1)} %collective-permute-done.2, bf16[1024,512]{1,0:T(8,128)(2,1)} %collective-permute-done.1, bf16[1024,512]{1,0:T(8,128)(2,1)} %collective-permute-done, bf16[1024,512]{1,0:T(8,128)(2,1)} %fusion.2), kind=kOutput, calls=%fused_computation.29 | convolution fusion | flops 25171968 | bytes 4210688 | tf_op jit(solution)/shard_map/dot_general | solution.py:284
  191.9 4.2 %convolution_convert_fusion.query_ref = bf16[1024,256]{1,0:T(8,128)(2,1)} fusion(bf16[2048,256]{1,0:T(8,128)(2,1)S(1)} %bitcast.29, bf16[1024,512]{1,0:T(8,128)(2,1)} %collective-permute-done.2, bf16[1024,512]{1,0:T(8,128)(2,1)} %collective-permute-done.1, bf16[1024,512]{1,0:T(8,128)(2,1)} %collective-permute-done, bf16[1024,512]{1,0:T(8,128)(2,1)} %fusion.2), kind=kOutput, calls=%fused_computation.25 | convolution fusion | flops 1090781184 | bytes 5767168 | tf_op jit(solution)/shard_map/dot_general | solution.py:281
  196.1 29.6 %all-to-all-done.1.table_ref = bf16[32,32,1024]{2,1,0:T(8,128)(2,1)S(1)} async-done(((bf16[32,32,1024]{2,1,0:T(8,128)(2,1)}), bf16[32,32,1024]{2,1,0:T(8,128)(2,1)S(1)}, u32[]{:S(2)}, u32[]{:S(2)}) %all-to-all-start.1) | async-done | bytes 2097184 | tf_op jit(solution)/shard_map/all_to_all | solution.py:232
  225.7 1.3 copy-done.1
  227.0 3.2 %attend.3 = bf16[512,256]{1,0:T(8,128)(2,1)} custom-call(bf16[1024,256]{1,0:T(8,128)(2,1)} %convolution_convert_fusion.query_ref, f32[1024,2]{1,0:T(8,128)} %fusion.9.gate_ref, bf16[32,32,1024]{2,1,0:T(8,128)(2,1)} %copy-done.1), custom_call_target="tpu_custom_call" | custom-call | tf_op jit(solution)/shard_map/attend/pallas_call | solution.py:186
  230.2 3.2 %collective-permute-start.6 = (bf16[512,256]{1,0:T(8,128)(2,1)}, bf16[512,256]{1,0:T(8,128)(2,1)}, u32[]{:S(2)}, u32[]{:S(2)}) collective-permute-start(bf16[512,256]{1,0:T(8,128)(2,1)} %attend.3), channel_id=1, source_target_pairs={{0,3},{1,0},{2,1},{3,2},{4,7},{5,4},{6,5},{7,6},{8,11},{9,8},{10,9... | collective-permute-start | bytes 786440 | tf_op jit(solution)/shard_map/ppermute | solution.py:301
  233.4 3.2 %attend.2 = bf16[512,256]{1,0:T(8,128)(2,1)} custom-call(bf16[1024,256]{1,0:T(8,128)(2,1)} %convolution_convert_fusion.query_ref, f32[1024,2]{1,0:T(8,128)} %fusion.9.gate_ref, bf16[32,32,1024]{2,1,0:T(8,128)(2,1)} %copy-done.1), custom_call_target="tpu_custom_call" | custom-call | tf_op jit(solution)/shard_map/attend/pallas_call | solution.py:186
  237.2 2.7 %collective-permute-start.4 = (bf16[512,256]{1,0:T(8,128)(2,1)}, bf16[512,256]{1,0:T(8,128)(2,1)S(1)}, u32[]{:S(2)}, u32[]{:S(2)}) collective-permute-start(bf16[512,256]{1,0:T(8,128)(2,1)} %attend.2), channel_id=1, source_target_pairs={{0,3},{1,0},{2,1},{3,2},{4,7},{5,4},{6,5},{7,6},{8,11},{9,8},{10,9... | collective-permute-start | bytes 786440 | tf_op jit(solution)/shard_map/ppermute | solution.py:298
  239.9 2.2 collective-permute-start.8
  242.1 5.1 %collective-permute-done.3 = bf16[512,256]{1,0:T(8,128)(2,1)S(1)} collective-permute-done((bf16[512,256]{1,0:T(8,128)(2,1)}, bf16[512,256]{1,0:T(8,128)(2,1)S(1)}, u32[]{:S(2)}, u32[]{:S(2)}) %collective-permute-start.3) | collective-permute-done | bytes 262176 | tf_op jit(solution)/shard_map/ppermute | solution.py:297
  247.1 5.6 %collective-permute-done.5 = bf16[512,256]{1,0:T(8,128)(2,1)S(1)} collective-permute-done((bf16[512,256]{1,0:T(8,128)(2,1)}, bf16[512,256]{1,0:T(8,128)(2,1)S(1)}, u32[]{:S(2)}, u32[]{:S(2)}) %collective-permute-start.5) | collective-permute-done | bytes 262176 | tf_op jit(solution)/shard_map/ppermute | solution.py:300
  252.8 1.9 convolution_add_fusion
  255.2 0.8 collective-permute-done.7
  256.1 1.4 fusion.5
  (36 shorter events, 3.8 us)
Async XLA Ops:
  0.0 153.0 %copy-start = (bf16[2048,256]{1,0:T(8,128)(2,1)S(1)}, bf16[2048,256]{1,0:T(8,128)(2,1)}, u32[]{:S(2)}) copy-start(bf16[2048,256]{1,0:T(8,128)(2,1)} %param.17) | copy-start | bytes 3145732
  120.1 105.6 %all-to-all-start.1 = ((bf16[32,32,1024]{2,1,0:T(8,128)(2,1)}), bf16[32,32,1024]{2,1,0:T(8,128)(2,1)S(1)}, u32[]{:S(2)}, u32[]{:S(2)}) async-start(bf16[32,32,1024]{2,1,0:T(8,128)(2,1)} %bitcast.26), calls=%async_computation.1 | async-start | bytes 4194304 | tf_op jit(solution)/shard_map/all_to_all | solution.py:232
  140.8 6.1 %copy-start.8 = (s32[4]{0:T(128)S(1)}, s32[4]{0:T(128)}, u32[]{:S(2)}) copy-start(s32[4]{0:T(128)} %constant.44.clone) | copy-start | bytes 52
  140.8 46.8 %collective-permute-start = (bf16[1024,512]{1,0:T(8,128)(2,1)}, bf16[1024,512]{1,0:T(8,128)(2,1)}, u32[]{:S(2)}, u32[]{:S(2)}) collective-permute-start(bf16[1024,512]{1,0:T(8,128)(2,1)} %fusion.2), channel_id=1, source_target_pairs={{0,1},{1,2},{2,3},{3,0},{4,5},{5,6},{6,7},{7,4},{8,9},{9,10},{10,1... | collective-permute-start | bytes 3145736 | tf_op jit(solution)/shard_map/ppermute | solution.py:250
  140.8 46.8 %collective-permute-start.1 = (bf16[1024,512]{1,0:T(8,128)(2,1)}, bf16[1024,512]{1,0:T(8,128)(2,1)}, u32[]{:S(2)}, u32[]{:S(2)}) collective-permute-start(bf16[1024,512]{1,0:T(8,128)(2,1)} %fusion.2), channel_id=1, source_target_pairs={{0,3},{1,0},{2,1},{3,2},{4,7},{5,4},{6,5},{7,6},{8,11},{9,8},{10,9... | collective-permute-start | bytes 3145736 | tf_op jit(solution)/shard_map/ppermute | solution.py:251
  144.0 43.6 %collective-permute-start.2 = (bf16[1024,512]{1,0:T(8,128)(2,1)}, bf16[1024,512]{1,0:T(8,128)(2,1)}, u32[]{:S(2)}, u32[]{:S(2)}) collective-permute-start(bf16[1024,512]{1,0:T(8,128)(2,1)} %fusion.2), channel_id=1, source_target_pairs={{0,2},{1,3},{2,0},{3,1},{4,6},{5,7},{6,4},{7,5},{8,10},{9,11},{10,... | collective-permute-start | bytes 3145736 | tf_op jit(solution)/shard_map/ppermute | solution.py:252
  160.5 3.3 %copy-start.5 = (bf16[1,512,512]{2,1,0:T(8,128)(2,1)S(1)}, bf16[1,512,512]{2,1,0:T(8,128)(2,1)}, u32[]{:S(2)}) copy-start(bf16[1,512,512]{2,1,0:T(8,128)(2,1)} %param.15) | copy-start | bytes 1572868
  160.5 3.3 %copy-start.7 = (f32[512]{0:T(512)S(1)}, f32[512]{0:T(512)}, u32[]{:S(2)}) copy-start(f32[512]{0:T(512)} %param.16) | copy-start | bytes 6148
  187.6 4.3 %copy-start.3 = (bf16[4,512,256]{2,1,0:T(8,128)(2,1)S(1)}, bf16[4,512,256]{2,1,0:T(8,128)(2,1)}, u32[]{:S(2)}) copy-start(bf16[4,512,256]{2,1,0:T(8,128)(2,1)} %gather_fusion) | copy-start | bytes 3145732
  225.7 1.3 copy-start.1
  230.2 22.6 %copy-start.2 = (f32[1024,512]{1,0:T(8,128)S(1)}, f32[1024,512]{1,0:T(8,128)}, u32[]{:S(2)}) copy-start(f32[1024,512]{1,0:T(8,128)} %convolution_multiply_fusion) | copy-start | bytes 6291460
  230.2 9.7 %collective-permute-start.6 = (bf16[512,256]{1,0:T(8,128)(2,1)}, bf16[512,256]{1,0:T(8,128)(2,1)}, u32[]{:S(2)}, u32[]{:S(2)}) collective-permute-start(bf16[512,256]{1,0:T(8,128)(2,1)} %attend.3), channel_id=1, source_target_pairs={{0,3},{1,0},{2,1},{3,2},{4,7},{5,4},{6,5},{7,6},{8,11},{9,8},{10,9... | collective-permute-start | bytes 786440 | tf_op jit(solution)/shard_map/ppermute | solution.py:301
  236.5 18.1 %copy-start.4 = (bf16[3,256,512]{2,1,0:T(8,128)(2,1)S(1)}, bf16[3,256,512]{2,1,0:T(8,128)(2,1)}, u32[]{:S(2)}) copy-start(bf16[3,256,512]{2,1,0:T(8,128)(2,1)} %slice.38) | copy-start | bytes 2359300
  236.5 18.1 %copy-start.6 = (bf16[512,256]{1,0:T(8,128)(2,1)S(1)}, bf16[512,256]{1,0:T(8,128)(2,1)}, u32[]{:S(2)}) copy-start(bf16[512,256]{1,0:T(8,128)(2,1)} %attend.2) | copy-start | bytes 786436
  236.5 10.6 %collective-permute-start.3 = (bf16[512,256]{1,0:T(8,128)(2,1)}, bf16[512,256]{1,0:T(8,128)(2,1)S(1)}, u32[]{:S(2)}, u32[]{:S(2)}) collective-permute-start(bf16[512,256]{1,0:T(8,128)(2,1)} %attend.2), channel_id=1, source_target_pairs={{0,1},{1,2},{2,3},{3,0},{4,5},{5,6},{6,7},{7,4},{8,9},{9,10},{10,1... | collective-permute-start | bytes 786440 | tf_op jit(solution)/shard_map/ppermute | solution.py:297
  236.5 16.2 %collective-permute-start.5 = (bf16[512,256]{1,0:T(8,128)(2,1)}, bf16[512,256]{1,0:T(8,128)(2,1)S(1)}, u32[]{:S(2)}, u32[]{:S(2)}) collective-permute-start(bf16[512,256]{1,0:T(8,128)(2,1)} %attend.3), channel_id=1, source_target_pairs={{0,1},{1,2},{2,3},{3,0},{4,5},{5,6},{6,7},{7,4},{8,9},{9,10},{10,1... | collective-permute-start | bytes 786440 | tf_op jit(solution)/shard_map/ppermute | solution.py:300
  237.2 17.4 %collective-permute-start.4 = (bf16[512,256]{1,0:T(8,128)(2,1)}, bf16[512,256]{1,0:T(8,128)(2,1)S(1)}, u32[]{:S(2)}, u32[]{:S(2)}) collective-permute-start(bf16[512,256]{1,0:T(8,128)(2,1)} %attend.2), channel_id=1, source_target_pairs={{0,3},{1,0},{2,1},{3,2},{4,7},{5,4},{6,5},{7,6},{8,11},{9,8},{10,9... | collective-permute-start | bytes 786440 | tf_op jit(solution)/shard_map/ppermute | solution.py:298
  239.9 15.3 %collective-permute-start.8 = (bf16[512,256]{1,0:T(8,128)(2,1)}, bf16[512,256]{1,0:T(8,128)(2,1)S(1)}, u32[]{:S(2)}, u32[]{:S(2)}) collective-permute-start(bf16[512,256]{1,0:T(8,128)(2,1)} %collective-permute-done.6), channel_id=1, source_target_pairs={{0,3},{1,0},{2,1},{3,2},{4,7},{5,4},{6,5},{7,6},{8,11},{9,8},{10,9... | collective-permute-start | bytes 786440 | tf_op jit(solution)/shard_map/ppermute | solution.py:303
  247.1 9.0 %collective-permute-start.7 = (bf16[512,256]{1,0:T(8,128)(2,1)S(1)}, bf16[512,256]{1,0:T(8,128)(2,1)S(1)}, u32[]{:S(2)}, u32[]{:S(2)}) collective-permute-start(bf16[512,256]{1,0:T(8,128)(2,1)S(1)} %collective-permute-done.3), channel_id=1, source_target_pairs={{0,1},{1,2},{2,3},{3,0},{4,5},{5,6},{6,7},{7,4},{8,9},{9,10},{10,1... | collective-permute-start | bytes 786440 | tf_op jit(solution)/shard_map/ppermute | solution.py:302

commit v9 on v8

--- a/solution.py
+++ b/solution.py
@@ -20,7 +20,7 @@
 whole = pl.BlockSpec(memory_space=pltpu.VMEM)
 
 
-def spread_kernel(ids_ref, store_ref, gain_ref, key_ref, value_ref, out_ref, order_ref, both_ref):
+def spread_kernel(ids_ref, store_ref, gain_ref, key_ref, value_ref, out_ref, turn_ref, both_ref):
     group, share = pl.program_id(0), pl.program_id(1)
     passages, span, width = store_ref.shape
     rows = passages * span
@@ -33,11 +33,6 @@
     def _():
         both_ref[:, :half] = key_ref[...]
         both_ref[:, half:] = value_ref[...]
-        spot = lax.broadcasted_iota(jnp.int32, (rows, rows), 0)
-        holder = jnp.floor((spot.astype(jnp.float32) + 0.5) * (1.0 / passages)).astype(jnp.int32)
-        wanted = (spot - holder * passages) * span + holder
-        other = lax.broadcasted_iota(jnp.int32, (rows, rows), 1)
-        order_ref[...] = jnp.where(wanted == other, 1.0, 0.0).astype(jnp.bfloat16)
 
     @pl.when(share == 0)
     def _():
@@ -54,14 +49,14 @@
     inverse = lax.rsqrt(jnp.mean(wide * wide, axis=-1, keepdims=True) + epsilon)
     scaled = (wide * gain_ref[...]).astype(jnp.bfloat16)
     product = jnp.dot(scaled, both_ref[...], preferred_element_type=jnp.float32)
-    product = (product * inverse).astype(jnp.bfloat16)
-    turned = jnp.dot(order_ref[...], product, preferred_element_type=jnp.float32)
-    turned = turned.reshape(span, passages, chunks * LANES).astype(jnp.bfloat16)
+    product = product * inverse
+    for chunk in range(chunks):
+        turn_ref[chunk] = product[:, chunk * LANES : (chunk + 1) * LANES]
     for chunk in range(chunks):
         start = pl.multiple_of(chunk * body + share * passages, TILE)
-        out_ref[:, pl.ds(start, passages), :] = turned[
-            :, :, chunk * LANES : (chunk + 1) * LANES
-        ]
+        for holder in range(span):
+            turned = turn_ref[chunk, pl.ds(holder, passages, stride=span), :]
+            out_ref[holder, pl.ds(start, passages), :] = turned.astype(jnp.bfloat16)
 
 
 def spread_store(ids, store, gain, key_weight, value_weight, holders):
@@ -83,7 +78,7 @@
         out_specs=pl.BlockSpec((SHARE_ROWS, per_holder, LANES), lambda g, i: (g, 0, 0)),
         out_shape=jax.ShapeDtypeStruct((holders, per_holder, LANES), jnp.bfloat16),
         scratch_shapes=[
-            pltpu.VMEM((rows, rows), jnp.bfloat16),
+            pltpu.VMEM((2 * head_width // LANES, rows, LANES), jnp.float32),
             pltpu.VMEM((width, 2 * head_width), jnp.bfloat16),
         ],
         name="spread_store",
@@ -183,13 +178,14 @@
     rows, width = queries.shape
     rows = rows // 2
     holders, slots, both = table.shape
+    span = rows // BLK * NPB
     return pl.pallas_call(
         attend_kernel,
         grid=(1,),
         in_specs=[
             pl.BlockSpec((rows, width), lambda i: (half, 0)),
             pl.BlockSpec((rows, gates.shape[1]), lambda i: (half, 0)),
-            pl.BlockSpec((holders, slots // 2, both), lambda i: (0, half, 0)),
+            pl.BlockSpec((holders, span, both), lambda i: (0, slots // span - 1, 0)),
         ],
         out_specs=pl.BlockSpec((rows, width), lambda i: (0, 0)),
         out_shape=jax.ShapeDtypeStruct((rows, width), jnp.bfloat16),
@@ -293,7 +289,7 @@
         (queries, gating, base, near, weights[3])
     )
 
-    low = attend(queries, gating, returned, 0)
+    low = attend(queries, gating, returned[:, : returned.shape[1] // 2], 0)
     low_before = lax.ppermute(low, "tp", up)
     low_after = lax.ppermute(low, "tp", down)
     high = attend(queries, gating, returned, 1)

time: 258 us -> 260 us (level)
    ppermute x1, waiting for transfers between devices: 21.7 us -> 2.88 us  [per_device(): before = lax.ppermute(normed, 'tp', up)]
    ppermute x1, waiting for transfers between devices: 0.01 us -> 16.3 us  [per_device(): after = lax.ppermute(normed, 'tp', down)]
    ppermute x1, waiting for transfers between devices: 0.01 us -> 3.17 us  [per_device(): far = lax.ppermute(normed, 'tp', across)]
  transfers between devices with their start and end apart: 10 -> 10, of which waited for: 5 -> 7; matrix products, arithmetic and copies ran while one was open for 15% -> 16% of each run, Pallas kernels for 1% -> 1%
where the time goes in v9:
time: 260 us
  blocking collectives  117 us (45%)
  waiting for transfers between devices  61.4 us (24%)
  Pallas kernels  20.4 us (8%)
  starting transfers between devices  17.4 us (7%)
  matrix products  15.3 us (6%)
  other arithmetic  14.8 us (6%)
  local copies, waits for them, and re-layouts  13.3 us (5%)
    all_to_all x1, blocking collectives, per_device(): held = lax.all_to_all(spread, 'st', split_axis=0, concat_axis=0, tiled=True)  106 us
    all_to_all x1, waiting for transfers between devices, per_device(): lax.all_to_all(packed.reshape(st_count, -1, shares * width_both), 'st', s...  29.3 us
    ppermute x1, waiting for transfers between devices, per_device(): after = lax.ppermute(normed, 'tp', down)  16.3 us
    psum x1, blocking collectives, per_device(): square_sums = lax.psum(jnp.sum(wide_tokens * wide_tokens, axis=1), 'tp')  10.9 us
    pallas_call x1, Pallas kernels, spread_store(): pl.pallas_call(spread_kernel, grid=(groups, length // holders), in_specs=...  8.9 us
    pallas_call x2, Pallas kernels, attend(): pl.pallas_call(attend_kernel, grid=(1,), in_specs=[pl.BlockSpec((rows, wi...  6.34 us
    pallas_call x1, Pallas kernels, select_rows(): pl.pallas_call(lambda *refs: select_kernel(blocks, shares, *refs), grid=(...  5.21 us
  transfers between devices with their start and end apart: 10, of which 7 were waited for; matrix products, arithmetic and copies ran while one was open for 16% of the time, Pallas kernels for 1%

profile of v9, /device:TPU:40, one launch (start us, length us, event | category | flops | bytes accessed | tf_op | source)
XLA Modules:
  0.0 259.5 jit_solution(17747514420502428795)
XLA Ops:
  0.0 8.9 %spread_store.1 = bf16[32,200,128]{2,1,0:T(8,128)(2,1)} custom-call(s32[4,8]{1,0:T(4,128)} %bitcast.33, bf16[24,64,2048]{2,1,0:T(8,128)(2,1)} %store_ref.1, f32[1,2048]{1,0:T(1,128)} %bitcast.32, bf16[2048,256]{1,0:T(8,128)(2,1)} %key_ref.1, bf16[2048,256]{1,0:T(8,128)(2,1)} %value_ref.1), custom_call_target="tpu_custom_call" | custom-call | tf_op jit(solution)/shard_map/spread_store/pallas_call | solution.py:68
  8.9 105.7 %all_to_all.10.refs_0_ = bf16[32,200,128]{2,1,0:T(8,128)(2,1)} all-to-all(bf16[32,200,128]{2,1,0:T(8,128)(2,1)} %spread_store.1), channel_id=1, replica_groups=mesh['grp'=2,'st'=32,'tp'=4] {'st'}, dimensions={0} | all-to-all | bytes 3276800 | tf_op jit(solution)/shard_map/all_to_all | solution.py:225
  114.6 5.2 %select_rows.1 = bf16[1024,1024]{1,0:T(8,128)(2,1)} custom-call(bf16[32,200,128]{2,1,0:T(8,128)(2,1)} %all_to_all.10.refs_0_), custom_call_target="tpu_custom_call" | custom-call | tf_op jit(solution)/shard_map/select_rows/pallas_call | solution.py:125
  119.8 4.9 %all-to-all-start.1 = ((bf16[32,32,1024]{2,1,0:T(8,128)(2,1)}), bf16[32,32,1024]{2,1,0:T(8,128)(2,1)S(1)}, u32[]{:S(2)}, u32[]{:S(2)}) async-start(bf16[32,32,1024]{2,1,0:T(8,128)(2,1)} %bitcast.26), calls=%async_computation.1 | async-start | bytes 4194304 | tf_op jit(solution)/shard_map/all_to_all | solution.py:228
  125.5 1.5 fusion
  127.0 10.9 %psum.7 = f32[1024]{0:T(1024)S(1)} all-reduce(f32[1024]{0:T(1024)S(1)} %fusion), channel_id=1, replica_groups=mesh['grp'=2,'st'=32,'tp'=4] {'tp'}, use_global_device_ids=true, to_apply=%region_1.0 | all-reduce | flops 1024 | bytes 8192 | tf_op jit(solution)/shard_map/psum | solution.py:237
  138.0 2.5 fusion.2
  143.4 2.9 %convert.1 = f32[4,256,512]{2,1,0:T(8,128)} convert(bf16[4,256,512]{2,1,0:T(8,128)(2,1)} %bitcast.5) | non-fusion elementwise | flops 524288 | bytes 3145728 | tf_op jit(solution)/shard_map/reshape | solution.py:253
  147.1 2.7 %add_select_fusion.3 = f32[4,256,512]{2,1,0:T(8,128)S(1)} fusion(f32[4,256,512]{2,1,0:T(8,128)} %convert.1, pred[]{:T(512)S(6)} %ge.15), kind=kLoop, calls=%fused_computation.7 | loop fusion | flops 1048576 | bytes 4194305 | tf_op jit(solution)/shard_map/jit(_where)/select_n | solution.py:258
  150.1 1.6 add_select_fusion.1
  151.8 1.7 gather_fusion
  154.0 2.8 %gather_fusion.2 = bf16[4,256,512]{2,1,0:T(8,128)(2,1)} fusion(bf16[4,256,512]{2,1,0:T(8,128)(2,1)} %bitcast.28, s32[1024]{0:T(1024)S(1)} %pad_clamp_fusion), kind=kCustom, calls=%fused_computation.2 | custom fusion | bytes 2097168 | tf_op jit(solution)/shard_map/jit(_take)/gather | solution.py:272
  156.8 2.1 slice.42
  159.9 3.3 %fusion.6 = bf16[4,256,512]{2,1,0:T(8,128)(2,1)S(1)} fusion(f32[4,256,512]{2,1,0:T(8,128)} %add_select_fusion.1, f32[256]{0:T(256)S(1)} %minimum_convert_fusion, pred[]{:T(512)S(6)} %ge.12, bf16[4,256,512]{2,1,0:T(8,128)(2,1)} %bitcast.5), kind=kLoop, calls=%fused_computation.21 | loop fusion | flops 3145728 | bytes 4195329 | tf_op jit(solution)/shard_map/convert_element_type | solution.py:263
  163.2 2.0 convolution_multiply_fusion
  165.2 3.2 %collective-permute-done.2 = bf16[1024,512]{1,0:T(8,128)(2,1)} collective-permute-done((bf16[1024,512]{1,0:T(8,128)(2,1)}, bf16[1024,512]{1,0:T(8,128)(2,1)}, u32[]{:S(2)}, u32[]{:S(2)}) %collective-permute-start.2) | collective-permute-done | bytes 1048608 | tf_op jit(solution)/shard_map/ppermute | solution.py:248
  168.4 16.3 %collective-permute-done.1 = bf16[1024,512]{1,0:T(8,128)(2,1)} collective-permute-done((bf16[1024,512]{1,0:T(8,128)(2,1)}, bf16[1024,512]{1,0:T(8,128)(2,1)}, u32[]{:S(2)}, u32[]{:S(2)}) %collective-permute-start.1) | collective-permute-done | bytes 1048608 | tf_op jit(solution)/shard_map/ppermute | solution.py:247
  184.7 2.9 %collective-permute-done = bf16[1024,512]{1,0:T(8,128)(2,1)} collective-permute-done((bf16[1024,512]{1,0:T(8,128)(2,1)}, bf16[1024,512]{1,0:T(8,128)(2,1)}, u32[]{:S(2)}, u32[]{:S(2)}) %collective-permute-start) | collective-permute-done | bytes 1048608 | tf_op jit(solution)/shard_map/ppermute | solution.py:246
  187.6 4.3 %fusion.9.gate_ref = f32[1024,2]{1,0:T(8,128)} fusion(bf16[2048,2]{0,1:T(2,128)(2,1)S(1)} %bitcast.25, bf16[1024,512]{1,0:T(8,128)(2,1)} %collective-permute-done.2, bf16[1024,512]{1,0:T(8,128)(2,1)} %collective-permute-done.1, bf16[1024,512]{1,0:T(8,128)(2,1)} %collective-permute-done, bf16[1024,512]{1,0:T(8,128)(2,1)} %fusion.2), kind=kOutput, calls=%fused_computation.29 | convolution fusion | flops 25171968 | bytes 4210688 | tf_op jit(solution)/shard_map/dot_general | solution.py:280
  191.9 4.2 %convolution_convert_fusion.query_ref = bf16[1024,256]{1,0:T(8,128)(2,1)} fusion(bf16[2048,256]{1,0:T(8,128)(2,1)S(1)} %bitcast.29, bf16[1024,512]{1,0:T(8,128)(2,1)} %collective-permute-done.2, bf16[1024,512]{1,0:T(8,128)(2,1)} %collective-permute-done.1, bf16[1024,512]{1,0:T(8,128)(2,1)} %collective-permute-done, bf16[1024,512]{1,0:T(8,128)(2,1)} %fusion.2), kind=kOutput, calls=%fused_computation.25 | convolution fusion | flops 1090781184 | bytes 5767168 | tf_op jit(solution)/shard_map/dot_general | solution.py:277
  196.2 29.3 %all-to-all-done.1.table_ref = bf16[32,32,1024]{2,1,0:T(8,128)(2,1)S(1)} async-done(((bf16[32,32,1024]{2,1,0:T(8,128)(2,1)}), bf16[32,32,1024]{2,1,0:T(8,128)(2,1)S(1)}, u32[]{:S(2)}, u32[]{:S(2)}) %all-to-all-start.1) | async-done | bytes 2097184 | tf_op jit(solution)/shard_map/all_to_all | solution.py:228
  226.8 3.2 %attend.3 = bf16[512,256]{1,0:T(8,128)(2,1)} custom-call(bf16[1024,256]{1,0:T(8,128)(2,1)} %convolution_convert_fusion.query_ref, f32[1024,2]{1,0:T(8,128)} %fusion.9.gate_ref, bf16[32,32,1024]{2,1,0:T(8,128)(2,1)} %copy-done.1), custom_call_target="tpu_custom_call" | custom-call | tf_op jit(solution)/shard_map/attend/pallas_call | solution.py:182
  230.0 3.2 %collective-permute-start.6 = (bf16[512,256]{1,0:T(8,128)(2,1)}, bf16[512,256]{1,0:T(8,128)(2,1)}, u32[]{:S(2)}, u32[]{:S(2)}) collective-permute-start(bf16[512,256]{1,0:T(8,128)(2,1)} %attend.3), channel_id=1, source_target_pairs={{0,3},{1,0},{2,1},{3,2},{4,7},{5,4},{6,5},{7,6},{8,11},{9,8},{10,9... | collective-permute-start | bytes 786440 | tf_op jit(solution)/shard_map/ppermute | solution.py:297
  233.1 2.3 slice.44.table_ref
  235.4 3.1 %attend.2 = bf16[512,256]{1,0:T(8,128)(2,1)} custom-call(bf16[1024,256]{1,0:T(8,128)(2,1)} %convolution_convert_fusion.query_ref, f32[1024,2]{1,0:T(8,128)} %fusion.9.gate_ref, bf16[32,16,1024]{2,1,0:T(8,128)(2,1)} %slice.44.table_ref), custom_call_target="tpu_custom_call" | custom-call | tf_op jit(solution)/shard_map/attend/pallas_call | solution.py:182
  238.6 3.2 %collective-permute-start.4 = (bf16[512,256]{1,0:T(8,128)(2,1)}, bf16[512,256]{1,0:T(8,128)(2,1)S(1)}, u32[]{:S(2)}, u32[]{:S(2)}) collective-permute-start(bf16[512,256]{1,0:T(8,128)(2,1)} %attend.2), channel_id=1, source_target_pairs={{0,3},{1,0},{2,1},{3,2},{4,7},{5,4},{6,5},{7,6},{8,11},{9,8},{10,9... | collective-permute-start | bytes 786440 | tf_op jit(solution)/shard_map/ppermute | solution.py:294
  241.8 3.2 %collective-permute-start.8 = (bf16[512,256]{1,0:T(8,128)(2,1)}, bf16[512,256]{1,0:T(8,128)(2,1)S(1)}, u32[]{:S(2)}, u32[]{:S(2)}) collective-permute-start(bf16[512,256]{1,0:T(8,128)(2,1)} %collective-permute-done.6), channel_id=1, source_target_pairs={{0,3},{1,0},{2,1},{3,2},{4,7},{5,4},{6,5},{7,6},{8,11},{9,8},{10,9... | collective-permute-start | bytes 786440 | tf_op jit(solution)/shard_map/ppermute | solution.py:299
  245.1 4.1 %collective-permute-done.3 = bf16[512,256]{1,0:T(8,128)(2,1)S(1)} collective-permute-done((bf16[512,256]{1,0:T(8,128)(2,1)}, bf16[512,256]{1,0:T(8,128)(2,1)S(1)}, u32[]{:S(2)}, u32[]{:S(2)}) %collective-permute-start.3) | collective-permute-done | bytes 262176 | tf_op jit(solution)/shard_map/ppermute | solution.py:293
  249.2 1.8 convolution_add_fusion.1
  251.0 3.8 %collective-permute-done.5 = bf16[512,256]{1,0:T(8,128)(2,1)S(1)} collective-permute-done((bf16[512,256]{1,0:T(8,128)(2,1)}, bf16[512,256]{1,0:T(8,128)(2,1)S(1)}, u32[]{:S(2)}, u32[]{:S(2)}) %collective-permute-start.5) | collective-permute-done | bytes 262176 | tf_op jit(solution)/shard_map/ppermute | solution.py:296
  254.8 1.5 convolution_add_fusion
  256.4 1.8 collective-permute-done.7
  (37 shorter events, 9.1 us)
Async XLA Ops:
  0.0 151.8 %copy-start = (bf16[2048,256]{1,0:T(8,128)(2,1)S(1)}, bf16[2048,256]{1,0:T(8,128)(2,1)}, u32[]{:S(2)}) copy-start(bf16[2048,256]{1,0:T(8,128)(2,1)} %param.17) | copy-start | bytes 3145732
  119.8 105.6 %all-to-all-start.1 = ((bf16[32,32,1024]{2,1,0:T(8,128)(2,1)}), bf16[32,32,1024]{2,1,0:T(8,128)(2,1)S(1)}, u32[]{:S(2)}, u32[]{:S(2)}) async-start(bf16[32,32,1024]{2,1,0:T(8,128)(2,1)} %bitcast.26), calls=%async_computation.1 | async-start | bytes 4194304 | tf_op jit(solution)/shard_map/all_to_all | solution.py:228
  140.5 5.8 %copy-start.8 = (s32[4]{0:T(128)S(1)}, s32[4]{0:T(128)}, u32[]{:S(2)}) copy-start(s32[4]{0:T(128)} %constant.44.clone) | copy-start | bytes 52
  140.5 27.9 %collective-permute-start.2 = (bf16[1024,512]{1,0:T(8,128)(2,1)}, bf16[1024,512]{1,0:T(8,128)(2,1)}, u32[]{:S(2)}, u32[]{:S(2)}) collective-permute-start(bf16[1024,512]{1,0:T(8,128)(2,1)} %fusion.2), channel_id=1, source_target_pairs={{0,2},{1,3},{2,0},{3,1},{4,6},{5,7},{6,4},{7,5},{8,10},{9,11},{10,... | collective-permute-start | bytes 3145736 | tf_op jit(solution)/shard_map/ppermute | solution.py:248
  141.4 43.4 %collective-permute-start.1 = (bf16[1024,512]{1,0:T(8,128)(2,1)}, bf16[1024,512]{1,0:T(8,128)(2,1)}, u32[]{:S(2)}, u32[]{:S(2)}) collective-permute-start(bf16[1024,512]{1,0:T(8,128)(2,1)} %fusion.2), channel_id=1, source_target_pairs={{0,3},{1,0},{2,1},{3,2},{4,7},{5,4},{6,5},{7,6},{8,11},{9,8},{10,9... | collective-permute-start | bytes 3145736 | tf_op jit(solution)/shard_map/ppermute | solution.py:247
  142.7 45.0 %collective-permute-start = (bf16[1024,512]{1,0:T(8,128)(2,1)}, bf16[1024,512]{1,0:T(8,128)(2,1)}, u32[]{:S(2)}, u32[]{:S(2)}) collective-permute-start(bf16[1024,512]{1,0:T(8,128)(2,1)} %fusion.2), channel_id=1, source_target_pairs={{0,1},{1,2},{2,3},{3,0},{4,5},{5,6},{6,7},{7,4},{8,9},{9,10},{10,1... | collective-permute-start | bytes 3145736 | tf_op jit(solution)/shard_map/ppermute | solution.py:246
  159.9 3.3 %copy-start.5 = (bf16[1,512,512]{2,1,0:T(8,128)(2,1)S(1)}, bf16[1,512,512]{2,1,0:T(8,128)(2,1)}, u32[]{:S(2)}) copy-start(bf16[1,512,512]{2,1,0:T(8,128)(2,1)} %param.15) | copy-start | bytes 1572868
  159.9 3.3 %copy-start.7 = (f32[512]{0:T(512)S(1)}, f32[512]{0:T(512)}, u32[]{:S(2)}) copy-start(f32[512]{0:T(512)} %param.16) | copy-start | bytes 6148
  187.6 4.3 %copy-start.3 = (bf16[4,512,256]{2,1,0:T(8,128)(2,1)S(1)}, bf16[4,512,256]{2,1,0:T(8,128)(2,1)}, u32[]{:S(2)}) copy-start(bf16[4,512,256]{2,1,0:T(8,128)(2,1)} %gather_fusion) | copy-start | bytes 3145732
  225.4 1.3 copy-start.1
  230.0 19.2 %copy-start.2 = (f32[1024,512]{1,0:T(8,128)S(1)}, f32[1024,512]{1,0:T(8,128)}, u32[]{:S(2)}) copy-start(f32[1024,512]{1,0:T(8,128)} %convolution_multiply_fusion) | copy-start | bytes 6291460
  230.0 11.9 %collective-permute-start.6 = (bf16[512,256]{1,0:T(8,128)(2,1)}, bf16[512,256]{1,0:T(8,128)(2,1)}, u32[]{:S(2)}, u32[]{:S(2)}) collective-permute-start(bf16[512,256]{1,0:T(8,128)(2,1)} %attend.3), channel_id=1, source_target_pairs={{0,3},{1,0},{2,1},{3,2},{4,7},{5,4},{6,5},{7,6},{8,11},{9,8},{10,9... | collective-permute-start | bytes 786440 | tf_op jit(solution)/shard_map/ppermute | solution.py:297
  238.6 16.2 %copy-start.4 = (bf16[3,256,512]{2,1,0:T(8,128)(2,1)S(1)}, bf16[3,256,512]{2,1,0:T(8,128)(2,1)}, u32[]{:S(2)}) copy-start(bf16[3,256,512]{2,1,0:T(8,128)(2,1)} %slice.42) | copy-start | bytes 2359300
  238.6 16.2 %copy-start.6 = (bf16[512,256]{1,0:T(8,128)(2,1)S(1)}, bf16[512,256]{1,0:T(8,128)(2,1)}, u32[]{:S(2)}) copy-start(bf16[512,256]{1,0:T(8,128)(2,1)} %attend.3) | copy-start | bytes 786436
  238.6 10.6 %collective-permute-start.3 = (bf16[512,256]{1,0:T(8,128)(2,1)}, bf16[512,256]{1,0:T(8,128)(2,1)S(1)}, u32[]{:S(2)}, u32[]{:S(2)}) collective-permute-start(bf16[512,256]{1,0:T(8,128)(2,1)} %attend.2), channel_id=1, source_target_pairs={{0,1},{1,2},{2,3},{3,0},{4,5},{5,6},{6,7},{7,4},{8,9},{9,10},{10,1... | collective-permute-start | bytes 786440 | tf_op jit(solution)/shard_map/ppermute | solution.py:293
  238.6 10.6 %collective-permute-start.4 = (bf16[512,256]{1,0:T(8,128)(2,1)}, bf16[512,256]{1,0:T(8,128)(2,1)S(1)}, u32[]{:S(2)}, u32[]{:S(2)}) collective-permute-start(bf16[512,256]{1,0:T(8,128)(2,1)} %attend.2), channel_id=1, source_target_pairs={{0,3},{1,0},{2,1},{3,2},{4,7},{5,4},{6,5},{7,6},{8,11},{9,8},{10,9... | collective-permute-start | bytes 786440 | tf_op jit(solution)/shard_map/ppermute | solution.py:294
  241.8 13.0 %collective-permute-start.5 = (bf16[512,256]{1,0:T(8,128)(2,1)}, bf16[512,256]{1,0:T(8,128)(2,1)S(1)}, u32[]{:S(2)}, u32[]{:S(2)}) collective-permute-start(bf16[512,256]{1,0:T(8,128)(2,1)} %attend.3), channel_id=1, source_target_pairs={{0,1},{1,2},{2,3},{3,0},{4,5},{5,6},{6,7},{7,4},{8,9},{9,10},{10,1... | collective-permute-start | bytes 786440 | tf_op jit(solution)/shard_map/ppermute | solution.py:296
  241.8 14.5 %collective-permute-start.8 = (bf16[512,256]{1,0:T(8,128)(2,1)}, bf16[512,256]{1,0:T(8,128)(2,1)S(1)}, u32[]{:S(2)}, u32[]{:S(2)}) collective-permute-start(bf16[512,256]{1,0:T(8,128)(2,1)} %collective-permute-done.6), channel_id=1, source_target_pairs={{0,3},{1,0},{2,1},{3,2},{4,7},{5,4},{6,5},{7,6},{8,11},{9,8},{10,9... | collective-permute-start | bytes 786440 | tf_op jit(solution)/shard_map/ppermute | solution.py:299
  249.2 8.9 %collective-permute-start.7 = (bf16[512,256]{1,0:T(8,128)(2,1)S(1)}, bf16[512,256]{1,0:T(8,128)(2,1)S(1)}, u32[]{:S(2)}, u32[]{:S(2)}) collective-permute-start(bf16[512,256]{1,0:T(8,128)(2,1)S(1)} %collective-permute-done.3), channel_id=1, source_target_pairs={{0,1},{1,2},{2,3},{3,0},{4,5},{5,6},{6,7},{7,4},{8,9},{9,10},{10,1... | collective-permute-start | bytes 786440 | tf_op jit(solution)/shard_map/ppermute | solution.py:298

commit v10 on v9

--- a/solution.py
+++ b/solution.py
@@ -178,14 +178,13 @@
     rows, width = queries.shape
     rows = rows // 2
     holders, slots, both = table.shape
-    span = rows // BLK * NPB
     return pl.pallas_call(
         attend_kernel,
         grid=(1,),
         in_specs=[
             pl.BlockSpec((rows, width), lambda i: (half, 0)),
             pl.BlockSpec((rows, gates.shape[1]), lambda i: (half, 0)),
-            pl.BlockSpec((holders, span, both), lambda i: (0, slots // span - 1, 0)),
+            pl.BlockSpec((holders, slots // 2, both), lambda i: (0, half, 0)),
         ],
         out_specs=pl.BlockSpec((rows, width), lambda i: (0, 0)),
         out_shape=jax.ShapeDtypeStruct((rows, width), jnp.bfloat16),
@@ -289,7 +288,7 @@
         (queries, gating, base, near, weights[3])
     )
 
-    low = attend(queries, gating, returned[:, : returned.shape[1] // 2], 0)
+    low = attend(queries, gating, returned, 0)
     low_before = lax.ppermute(low, "tp", up)
     low_after = lax.ppermute(low, "tp", down)
     high = attend(queries, gating, returned, 1)

time: 260 us -> 258 us (level)
    ppermute x1, waiting for transfers between devices: 2.88 us -> 21.7 us  [per_device(): before = lax.ppermute(normed, 'tp', up)]
    ppermute x1, waiting for transfers between devices: 16.3 us -> 0.01 us  [per_device(): after = lax.ppermute(normed, 'tp', down)]
    ppermute x1, waiting for transfers between devices: 3.17 us -> 0.01 us  [per_device(): far = lax.ppermute(normed, 'tp', across)]
  transfers between devices with their start and end apart: 10 -> 10, of which waited for: 7 -> 5; matrix products, arithmetic and copies ran while one was open for 16% -> 15% of each run, Pallas kernels for 1% -> 1%
where the time goes in v10:
time: 258 us; the launch traced here: 257 us
  blocking collectives  117 us (45%)
  waiting for transfers between devices  62.8 us (24%)
  Pallas kernels  20.4 us (8%)
  starting transfers between devices  16.9 us (7%)
  other arithmetic  14.9 us (6%)
  matrix products  14.4 us (6%)
  local copies, waits for them, and re-layouts  11 us (4%)
    all_to_all x1, blocking collectives, per_device(): held = lax.all_to_all(spread, 'st', split_axis=0, concat_axis=0, tiled=True)  106 us
    all_to_all x1, waiting for transfers between devices, per_device(): lax.all_to_all(packed.reshape(st_count, -1, shares * width_both), 'st', s...  29.6 us
    ppermute x1, waiting for transfers between devices, per_device(): before = lax.ppermute(normed, 'tp', up)  21.7 us
    psum x1, blocking collectives, per_device(): square_sums = lax.psum(jnp.sum(wide_tokens * wide_tokens, axis=1), 'tp')  10.9 us
    pallas_call x1, Pallas kernels, spread_store(): pl.pallas_call(spread_kernel, grid=(groups, length // holders), in_specs=...  8.9 us
    pallas_call x2, Pallas kernels, attend(): pl.pallas_call(attend_kernel, grid=(1,), in_specs=[pl.BlockSpec((rows, wi...  6.33 us
    ppermute x1, waiting for transfers between devices, per_device(): high_before = lax.ppermute(high, 'tp', up)  5.61 us
    pallas_call x1, Pallas kernels, select_rows(): pl.pallas_call(lambda *refs: select_kernel(blocks, shares, *refs), grid=(...  5.21 us
  transfers between devices with their start and end apart: 10, of which 5 were waited for; matrix products, arithmetic and copies ran while one was open for 15% of the time, Pallas kernels for 1%

profile of v10, /device:TPU:40, one launch (start us, length us, event | category | flops | bytes accessed | tf_op | source)
XLA Modules:
  0.0 257.2 jit_solution(8303903989836753622)
XLA Ops:
  0.0 8.9 %spread_store.1 = bf16[32,200,128]{2,1,0:T(8,128)(2,1)} custom-call(s32[4,8]{1,0:T(4,128)} %bitcast.33, bf16[24,64,2048]{2,1,0:T(8,128)(2,1)} %store_ref.1, f32[1,2048]{1,0:T(1,128)} %bitcast.32, bf16[2048,256]{1,0:T(8,128)(2,1)} %key_ref.1, bf16[2048,256]{1,0:T(8,128)(2,1)} %value_ref.1), custom_call_target="tpu_custom_call" | custom-call | tf_op jit(solution)/shard_map/spread_store/pallas_call | solution.py:68
  8.9 105.7 %all_to_all.10.refs_0_ = bf16[32,200,128]{2,1,0:T(8,128)(2,1)} all-to-all(bf16[32,200,128]{2,1,0:T(8,128)(2,1)} %spread_store.1), channel_id=1, replica_groups=mesh['grp'=2,'st'=32,'tp'=4] {'st'}, dimensions={0} | all-to-all | bytes 3276800 | tf_op jit(solution)/shard_map/all_to_all | solution.py:224
  114.6 5.2 %select_rows.1 = bf16[1024,1024]{1,0:T(8,128)(2,1)} custom-call(bf16[32,200,128]{2,1,0:T(8,128)(2,1)} %all_to_all.10.refs_0_), custom_call_target="tpu_custom_call" | custom-call | tf_op jit(solution)/shard_map/select_rows/pallas_call | solution.py:125
  119.8 4.9 %all-to-all-start.1 = ((bf16[32,32,1024]{2,1,0:T(8,128)(2,1)}), bf16[32,32,1024]{2,1,0:T(8,128)(2,1)S(1)}, u32[]{:S(2)}, u32[]{:S(2)}) async-start(bf16[32,32,1024]{2,1,0:T(8,128)(2,1)} %bitcast.26), calls=%async_computation.1 | async-start | bytes 4194304 | tf_op jit(solution)/shard_map/all_to_all | solution.py:227
  125.5 1.5 fusion
  127.0 10.9 %psum.7 = f32[1024]{0:T(1024)S(1)} all-reduce(f32[1024]{0:T(1024)S(1)} %fusion), channel_id=1, replica_groups=mesh['grp'=2,'st'=32,'tp'=4] {'tp'}, use_global_device_ids=true, to_apply=%region_1.0 | all-reduce | flops 1024 | bytes 8192 | tf_op jit(solution)/shard_map/psum | solution.py:236
  138.0 2.5 fusion.2
  140.5 3.2 %collective-permute-start.1 = (bf16[1024,512]{1,0:T(8,128)(2,1)}, bf16[1024,512]{1,0:T(8,128)(2,1)}, u32[]{:S(2)}, u32[]{:S(2)}) collective-permute-start(bf16[1024,512]{1,0:T(8,128)(2,1)} %fusion.2), channel_id=1, source_target_pairs={{0,3},{1,0},{2,1},{3,2},{4,7},{5,4},{6,5},{7,6},{8,11},{9,8},{10,9... | collective-permute-start | bytes 3145736 | tf_op jit(solution)/shard_map/ppermute | solution.py:246
  143.8 2.9 %convert.1 = f32[4,256,512]{2,1,0:T(8,128)} convert(bf16[4,256,512]{2,1,0:T(8,128)(2,1)} %bitcast.5) | non-fusion elementwise | flops 524288 | bytes 3145728 | tf_op jit(solution)/shard_map/reshape | solution.py:252
  147.5 2.7 %add_select_fusion.3 = f32[4,256,512]{2,1,0:T(8,128)S(1)} fusion(f32[4,256,512]{2,1,0:T(8,128)} %convert.1, pred[]{:T(512)S(6)} %ge.15), kind=kLoop, calls=%fused_computation.7 | loop fusion | flops 1048576 | bytes 4194305 | tf_op jit(solution)/shard_map/jit(_where)/select_n | solution.py:257
  150.5 1.6 add_select_fusion.1
  152.7 1.7 gather_fusion
  154.4 2.8 %gather_fusion.2 = bf16[4,256,512]{2,1,0:T(8,128)(2,1)} fusion(bf16[4,256,512]{2,1,0:T(8,128)(2,1)} %bitcast.28, s32[1024]{0:T(1024)S(1)} %pad_clamp_fusion), kind=kCustom, calls=%fused_computation.2 | custom fusion | bytes 2097168 | tf_op jit(solution)/shard_map/jit(_take)/gather | solution.py:271
  157.2 2.1 slice.38
  159.3 1.0 slice_bitcast_fusion
  160.3 3.3 %fusion.6 = bf16[4,256,512]{2,1,0:T(8,128)(2,1)S(1)} fusion(f32[4,256,512]{2,1,0:T(8,128)} %add_select_fusion.1, f32[256]{0:T(256)S(1)} %minimum_convert_fusion, pred[]{:T(512)S(6)} %ge.12, bf16[4,256,512]{2,1,0:T(8,128)(2,1)} %bitcast.5), kind=kLoop, calls=%fused_computation.21 | loop fusion | flops 3145728 | bytes 4195329 | tf_op jit(solution)/shard_map/convert_element_type | solution.py:262
  163.6 2.0 convolution_multiply_fusion
  165.6 21.7 %collective-permute-done = bf16[1024,512]{1,0:T(8,128)(2,1)} collective-permute-done((bf16[1024,512]{1,0:T(8,128)(2,1)}, bf16[1024,512]{1,0:T(8,128)(2,1)}, u32[]{:S(2)}, u32[]{:S(2)}) %collective-permute-start) | collective-permute-done | bytes 1048608 | tf_op jit(solution)/shard_map/ppermute | solution.py:245
  187.3 4.3 %fusion.9.gate_ref = f32[1024,2]{1,0:T(8,128)} fusion(bf16[2048,2]{0,1:T(2,128)(2,1)S(1)} %bitcast.25, bf16[1024,512]{1,0:T(8,128)(2,1)} %collective-permute-done.2, bf16[1024,512]{1,0:T(8,128)(2,1)} %collective-permute-done.1, bf16[1024,512]{1,0:T(8,128)(2,1)} %collective-permute-done, bf16[1024,512]{1,0:T(8,128)(2,1)} %fusion.2), kind=kOutput, calls=%fused_computation.29 | convolution fusion | flops 25171968 | bytes 4210688 | tf_op jit(solution)/shard_map/dot_general | solution.py:279
  191.7 4.2 %convolution_convert_fusion.query_ref = bf16[1024,256]{1,0:T(8,128)(2,1)} fusion(bf16[2048,256]{1,0:T(8,128)(2,1)S(1)} %bitcast.29, bf16[1024,512]{1,0:T(8,128)(2,1)} %collective-permute-done.2, bf16[1024,512]{1,0:T(8,128)(2,1)} %collective-permute-done.1, bf16[1024,512]{1,0:T(8,128)(2,1)} %collective-permute-done, bf16[1024,512]{1,0:T(8,128)(2,1)} %fusion.2), kind=kOutput, calls=%fused_computation.25 | convolution fusion | flops 1090781184 | bytes 5767168 | tf_op jit(solution)/shard_map/dot_general | solution.py:276
  195.9 29.6 %all-to-all-done.1.table_ref = bf16[32,32,1024]{2,1,0:T(8,128)(2,1)S(1)} async-done(((bf16[32,32,1024]{2,1,0:T(8,128)(2,1)}), bf16[32,32,1024]{2,1,0:T(8,128)(2,1)S(1)}, u32[]{:S(2)}, u32[]{:S(2)}) %all-to-all-start.1) | async-done | bytes 2097184 | tf_op jit(solution)/shard_map/all_to_all | solution.py:227
  225.4 1.3 copy-done.1
  226.8 3.2 %attend.3 = bf16[512,256]{1,0:T(8,128)(2,1)} custom-call(bf16[1024,256]{1,0:T(8,128)(2,1)} %convolution_convert_fusion.query_ref, f32[1024,2]{1,0:T(8,128)} %fusion.9.gate_ref, bf16[32,32,1024]{2,1,0:T(8,128)(2,1)} %copy-done.1), custom_call_target="tpu_custom_call" | custom-call | tf_op jit(solution)/shard_map/attend/pallas_call | solution.py:181
  229.9 3.2 %collective-permute-start.6 = (bf16[512,256]{1,0:T(8,128)(2,1)}, bf16[512,256]{1,0:T(8,128)(2,1)}, u32[]{:S(2)}, u32[]{:S(2)}) collective-permute-start(bf16[512,256]{1,0:T(8,128)(2,1)} %attend.3), channel_id=1, source_target_pairs={{0,3},{1,0},{2,1},{3,2},{4,7},{5,4},{6,5},{7,6},{8,11},{9,8},{10,9... | collective-permute-start | bytes 786440 | tf_op jit(solution)/shard_map/ppermute | solution.py:296
  233.1 3.2 %attend.2 = bf16[512,256]{1,0:T(8,128)(2,1)} custom-call(bf16[1024,256]{1,0:T(8,128)(2,1)} %convolution_convert_fusion.query_ref, f32[1024,2]{1,0:T(8,128)} %fusion.9.gate_ref, bf16[32,32,1024]{2,1,0:T(8,128)(2,1)} %copy-done.1), custom_call_target="tpu_custom_call" | custom-call | tf_op jit(solution)/shard_map/attend/pallas_call | solution.py:181
  237.0 2.7 %collective-permute-start.4 = (bf16[512,256]{1,0:T(8,128)(2,1)}, bf16[512,256]{1,0:T(8,128)(2,1)S(1)}, u32[]{:S(2)}, u32[]{:S(2)}) collective-permute-start(bf16[512,256]{1,0:T(8,128)(2,1)} %attend.2), channel_id=1, source_target_pairs={{0,3},{1,0},{2,1},{3,2},{4,7},{5,4},{6,5},{7,6},{8,11},{9,8},{10,9... | collective-permute-start | bytes 786440 | tf_op jit(solution)/shard_map/ppermute | solution.py:293
  239.6 2.2 collective-permute-start.8
  241.8 5.1 %collective-permute-done.3 = bf16[512,256]{1,0:T(8,128)(2,1)S(1)} collective-permute-done((bf16[512,256]{1,0:T(8,128)(2,1)}, bf16[512,256]{1,0:T(8,128)(2,1)S(1)}, u32[]{:S(2)}, u32[]{:S(2)}) %collective-permute-start.3) | collective-permute-done | bytes 262176 | tf_op jit(solution)/shard_map/ppermute | solution.py:292
  246.9 5.6 %collective-permute-done.5 = bf16[512,256]{1,0:T(8,128)(2,1)S(1)} collective-permute-done((bf16[512,256]{1,0:T(8,128)(2,1)}, bf16[512,256]{1,0:T(8,128)(2,1)S(1)}, u32[]{:S(2)}, u32[]{:S(2)}) %collective-permute-start.5) | collective-permute-done | bytes 262176 | tf_op jit(solution)/shard_map/ppermute | solution.py:295
  252.5 1.9 convolution_add_fusion
  255.0 0.8 collective-permute-done.7
  255.8 1.4 fusion.5
  (36 shorter events, 3.8 us)
Async XLA Ops:
  0.0 152.7 %copy-start = (bf16[2048,256]{1,0:T(8,128)(2,1)S(1)}, bf16[2048,256]{1,0:T(8,128)(2,1)}, u32[]{:S(2)}) copy-start(bf16[2048,256]{1,0:T(8,128)(2,1)} %param.17) | copy-start | bytes 3145732
  119.8 105.6 %all-to-all-start.1 = ((bf16[32,32,1024]{2,1,0:T(8,128)(2,1)}), bf16[32,32,1024]{2,1,0:T(8,128)(2,1)S(1)}, u32[]{:S(2)}, u32[]{:S(2)}) async-start(bf16[32,32,1024]{2,1,0:T(8,128)(2,1)} %bitcast.26), calls=%async_computation.1 | async-start | bytes 4194304 | tf_op jit(solution)/shard_map/all_to_all | solution.py:227
  140.5 6.1 %copy-start.8 = (s32[4]{0:T(128)S(1)}, s32[4]{0:T(128)}, u32[]{:S(2)}) copy-start(s32[4]{0:T(128)} %constant.44.clone) | copy-start | bytes 52
  140.5 46.8 %collective-permute-start = (bf16[1024,512]{1,0:T(8,128)(2,1)}, bf16[1024,512]{1,0:T(8,128)(2,1)}, u32[]{:S(2)}, u32[]{:S(2)}) collective-permute-start(bf16[1024,512]{1,0:T(8,128)(2,1)} %fusion.2), channel_id=1, source_target_pairs={{0,1},{1,2},{2,3},{3,0},{4,5},{5,6},{6,7},{7,4},{8,9},{9,10},{10,1... | collective-permute-start | bytes 3145736 | tf_op jit(solution)/shard_map/ppermute | solution.py:245
  140.5 46.8 %collective-permute-start.1 = (bf16[1024,512]{1,0:T(8,128)(2,1)}, bf16[1024,512]{1,0:T(8,128)(2,1)}, u32[]{:S(2)}, u32[]{:S(2)}) collective-permute-start(bf16[1024,512]{1,0:T(8,128)(2,1)} %fusion.2), channel_id=1, source_target_pairs={{0,3},{1,0},{2,1},{3,2},{4,7},{5,4},{6,5},{7,6},{8,11},{9,8},{10,9... | collective-permute-start | bytes 3145736 | tf_op jit(solution)/shard_map/ppermute | solution.py:246
  143.7 43.6 %collective-permute-start.2 = (bf16[1024,512]{1,0:T(8,128)(2,1)}, bf16[1024,512]{1,0:T(8,128)(2,1)}, u32[]{:S(2)}, u32[]{:S(2)}) collective-permute-start(bf16[1024,512]{1,0:T(8,128)(2,1)} %fusion.2), channel_id=1, source_target_pairs={{0,2},{1,3},{2,0},{3,1},{4,6},{5,7},{6,4},{7,5},{8,10},{9,11},{10,... | collective-permute-start | bytes 3145736 | tf_op jit(solution)/shard_map/ppermute | solution.py:247
  160.3 3.3 %copy-start.5 = (bf16[1,512,512]{2,1,0:T(8,128)(2,1)S(1)}, bf16[1,512,512]{2,1,0:T(8,128)(2,1)}, u32[]{:S(2)}) copy-start(bf16[1,512,512]{2,1,0:T(8,128)(2,1)} %param.15) | copy-start | bytes 1572868
  160.3 3.3 %copy-start.7 = (f32[512]{0:T(512)S(1)}, f32[512]{0:T(512)}, u32[]{:S(2)}) copy-start(f32[512]{0:T(512)} %param.16) | copy-start | bytes 6148
  187.3 4.3 %copy-start.3 = (bf16[4,512,256]{2,1,0:T(8,128)(2,1)S(1)}, bf16[4,512,256]{2,1,0:T(8,128)(2,1)}, u32[]{:S(2)}) copy-start(bf16[4,512,256]{2,1,0:T(8,128)(2,1)} %gather_fusion) | copy-start | bytes 3145732
  225.4 1.3 copy-start.1
  229.9 22.6 %copy-start.2 = (f32[1024,512]{1,0:T(8,128)S(1)}, f32[1024,512]{1,0:T(8,128)}, u32[]{:S(2)}) copy-start(f32[1024,512]{1,0:T(8,128)} %convolution_multiply_fusion) | copy-start | bytes 6291460
  229.9 9.7 %collective-permute-start.6 = (bf16[512,256]{1,0:T(8,128)(2,1)}, bf16[512,256]{1,0:T(8,128)(2,1)}, u32[]{:S(2)}, u32[]{:S(2)}) collective-permute-start(bf16[512,256]{1,0:T(8,128)(2,1)} %attend.3), channel_id=1, source_target_pairs={{0,3},{1,0},{2,1},{3,2},{4,7},{5,4},{6,5},{7,6},{8,11},{9,8},{10,9... | collective-permute-start | bytes 786440 | tf_op jit(solution)/shard_map/ppermute | solution.py:296
  236.3 18.1 %copy-start.4 = (bf16[3,256,512]{2,1,0:T(8,128)(2,1)S(1)}, bf16[3,256,512]{2,1,0:T(8,128)(2,1)}, u32[]{:S(2)}) copy-start(bf16[3,256,512]{2,1,0:T(8,128)(2,1)} %slice.38) | copy-start | bytes 2359300
  236.3 18.1 %copy-start.6 = (bf16[512,256]{1,0:T(8,128)(2,1)S(1)}, bf16[512,256]{1,0:T(8,128)(2,1)}, u32[]{:S(2)}) copy-start(bf16[512,256]{1,0:T(8,128)(2,1)} %attend.2) | copy-start | bytes 786436
  236.3 10.6 %collective-permute-start.3 = (bf16[512,256]{1,0:T(8,128)(2,1)}, bf16[512,256]{1,0:T(8,128)(2,1)S(1)}, u32[]{:S(2)}, u32[]{:S(2)}) collective-permute-start(bf16[512,256]{1,0:T(8,128)(2,1)} %attend.2), channel_id=1, source_target_pairs={{0,1},{1,2},{2,3},{3,0},{4,5},{5,6},{6,7},{7,4},{8,9},{9,10},{10,1... | collective-permute-start | bytes 786440 | tf_op jit(solution)/shard_map/ppermute | solution.py:292
  236.3 16.2 %collective-permute-start.5 = (bf16[512,256]{1,0:T(8,128)(2,1)}, bf16[512,256]{1,0:T(8,128)(2,1)S(1)}, u32[]{:S(2)}, u32[]{:S(2)}) collective-permute-start(bf16[512,256]{1,0:T(8,128)(2,1)} %attend.3), channel_id=1, source_target_pairs={{0,1},{1,2},{2,3},{3,0},{4,5},{5,6},{6,7},{7,4},{8,9},{9,10},{10,1... | collective-permute-start | bytes 786440 | tf_op jit(solution)/shard_map/ppermute | solution.py:295
  237.0 17.4 %collective-permute-start.4 = (bf16[512,256]{1,0:T(8,128)(2,1)}, bf16[512,256]{1,0:T(8,128)(2,1)S(1)}, u32[]{:S(2)}, u32[]{:S(2)}) collective-permute-start(bf16[512,256]{1,0:T(8,128)(2,1)} %attend.2), channel_id=1, source_target_pairs={{0,3},{1,0},{2,1},{3,2},{4,7},{5,4},{6,5},{7,6},{8,11},{9,8},{10,9... | collective-permute-start | bytes 786440 | tf_op jit(solution)/shard_map/ppermute | solution.py:293
  239.6 15.3 %collective-permute-start.8 = (bf16[512,256]{1,0:T(8,128)(2,1)}, bf16[512,256]{1,0:T(8,128)(2,1)S(1)}, u32[]{:S(2)}, u32[]{:S(2)}) collective-permute-start(bf16[512,256]{1,0:T(8,128)(2,1)} %collective-permute-done.6), channel_id=1, source_target_pairs={{0,3},{1,0},{2,1},{3,2},{4,7},{5,4},{6,5},{7,6},{8,11},{9,8},{10,9... | collective-permute-start | bytes 786440 | tf_op jit(solution)/shard_map/ppermute | solution.py:298
  246.9 9.0 %collective-permute-start.7 = (bf16[512,256]{1,0:T(8,128)(2,1)S(1)}, bf16[512,256]{1,0:T(8,128)(2,1)S(1)}, u32[]{:S(2)}, u32[]{:S(2)}) collective-permute-start(bf16[512,256]{1,0:T(8,128)(2,1)S(1)} %collective-permute-done.3), channel_id=1, source_target_pairs={{0,1},{1,2},{2,3},{3,0},{4,5},{5,6},{6,7},{7,4},{8,9},{9,10},{10,1... | collective-permute-start | bytes 786440 | tf_op jit(solution)/shard_map/ppermute | solution.py:297
